TPU v7x, 512 devices: a 8x2x16 block of a 8x8x16 slice. The times are simulated.
512 devices in a mesh: grp: 2 (over y), sp: 16 (over z), dp: 16 (over x, core).
Axes of the slice: x: 8, y: 2, z: 16, core: 2. Of those that a mesh axis runs over, the one named last changes fastest.
The devices are a block of a 8x8x16 slice.
Arguments:
- mixer_source_array: bfloat16 [32, 3072, 2048], P(('grp', 'dp'), 'sp'), parts along dimension 0, may hold values from -6 to 6
- source_projection: bfloat16 [2048, 1024], P('dp'), may hold values from -0.125 to 0.125
- gating_projection: bfloat16 [2048, 1024], P('dp'), may hold values from -0.125 to 0.125
- entry_mapping_projection: bfloat16 [2048, 256], replicated, may hold values from -0.0390625 to 0.0390625
- readout_mapping_projection: bfloat16 [2048, 256], replicated, may hold values from -0.0390625 to 0.0390625
- increment_projection: bfloat16 [2048, 16], replicated, may hold values from -0.125 to 0.125
- source_conv_taps: float32 [4, 1024], replicated, may hold values from -3 to 3
- entry_mapping_taps: float32 [4, 256], replicated, may hold values from -3 to 3
- readout_mapping_taps: float32 [4, 256], replicated, may hold values from -3 to 3
- increment_offsets: float32 [16], replicated, may hold values from -1 to 1
- channel_damping_rate: float32 [16], replicated, may hold values from 0 to 1
- bypass_coefficients: float32 [16], replicated, may hold values from 0.5 to 1.5
- stride_multiplier: float32 [32, 3072], P(('grp', 'dp')), parts along dimension 0, may hold values from 0.5 to 2
- added_log_damping: float32 [32, 3072, 16], P(('grp', 'dp')), parts along dimension 0, may hold values from -2.1 to 0
- norm_scale_factor: float32 [1024], replicated, may hold values from 0.1 to 1.9
- final_projection: bfloat16 [1024, 2048], P(None, 'dp'), may hold values from -0.1875 to 0.1875
Outputs:
- output: bfloat16 [32, 3072, 2048], P(('grp', 'dp'), 'sp'), parts along dimension 0
There are 2 independent parts, one for each index of `grp`. A program takes and returns all parts, laid end to end along the dimension named above; an argument that names none is the same for every part. Nothing has to cross between parts.
All inputs are finite; a program needn't handle non-finite values.
Results may differ from a plain program's by a relative error of at most 0.015.
Values may be sent and summed in bfloat16 or wider, within the bound.
No kernel may reach another device: no remote copies, remote signals or barrier semaphores. Data moves between devices by JAX's collectives and lax.ppermute only.
A program may use at most 64 MiB of HBM per device.

v0:
```python
import jax
import jax.numpy as jnp
from jax import lax
from jax.sharding import PartitionSpec as P

P_SIZE = 64
N = 128
G = 2
CONV_W = 4
BLK = 64


EPSILON = 1e-06


def sent_together(arrays, axis, dim, along):
    widths = [a.shape[along] for a in arrays]
    both = jnp.concatenate(arrays, axis=along)
    out = lax.all_gather(both, axis, axis=dim, tiled=True)
    return tuple(jnp.split(out, [sum(widths[:k]) for k in range(1, len(widths))], axis=along))


def conv_silu(padded, taps):
    width = taps.shape[0]
    length = padded.shape[0] - width + 1
    total = taps[0][None, :] * padded[0:length]
    for shift_pos in range(1, width):
        total = total + taps[shift_pos][None, :] * padded[shift_pos : shift_pos + length]
    return jax.nn.silu(total).astype(jnp.bfloat16)


def block_parts(x_blocks, b_blocks, c_blocks, step_width_value, logarithm_retain):
    cumulative = jnp.cumsum(logarithm_retain, axis=1)
    scaled = (x_blocks.astype(jnp.float32) * step_width_value[..., None]).astype(jnp.bfloat16)
    intersection = jnp.einsum(
        "kign,kjgn->kgij", c_blocks, b_blocks, preferred_element_type=jnp.float32
    )
    by_row = jnp.transpose(cumulative, (0, 2, 3, 1))
    log_gap = by_row[..., :, None] - by_row[..., None, :]
    length = log_gap.shape[-1]
    lower = jnp.tril(jnp.ones((length, length), bool))
    mixing = (intersection[:, :, None] * jnp.exp(jnp.where(lower, log_gap, -jnp.inf))).astype(
        jnp.bfloat16
    )
    inner = jnp.einsum("kgrij,kjgrp->kigrp", mixing, scaled, preferred_element_type=jnp.float32)
    to_end = jnp.exp(cumulative[:, -1:] - cumulative)
    weighted = (b_blocks[:, :, :, None, :].astype(jnp.float32) * to_end[..., None]).astype(
        jnp.bfloat16
    )
    states = jnp.einsum("kjgrn,kjgrp->kgrnp", weighted, scaled, preferred_element_type=jnp.float32)
    return (inner, states, cumulative[:, -1], cumulative)


def block_carry(states, block_total):
    incl_sum = jnp.cumsum(block_total, axis=0)
    excl_sum = incl_sum - block_total
    count = block_total.shape[0]
    log_gap = excl_sum[:, None] - incl_sum[None, :]
    before = (jnp.arange(count)[None, :] < jnp.arange(count)[:, None])[:, :, None, None]
    factors = jnp.exp(jnp.where(before, log_gap, -jnp.inf))
    carried = jnp.einsum("kjgr,jgrnp->kgrnp", factors, states)
    final_factor = jnp.exp(incl_sum[-1][None] - incl_sum)
    final_state = jnp.einsum("jgr,jgrnp->grnp", final_factor, states)
    return (carried, final_state, excl_sum, incl_sum[-1])


def block_finish(inner, c_blocks, cumulative, carried, x_blocks, skip):
    reached = jnp.einsum("kign,kgrnp->kigrp", c_blocks.astype(jnp.float32), carried)
    return (
        inner
        + reached * jnp.exp(cumulative)[..., None]
        + skip[..., None] * x_blocks.astype(jnp.float32)
    )


def heads_mixer(
    proj_x,
    proj_b,
    proj_c,
    step_raw,
    source_conv_taps,
    entry_mapping_taps,
    readout_mapping_taps,
    increment_offsets,
    channel_damping_rate,
    bypass_coefficients,
    tempo_row_values,
    surge_row_values,
):
    tok_rows = proj_x.shape[0]
    head_count = step_raw.shape[1]
    per_group = head_count // G
    shard_head_count = head_count // lax.axis_size("sp")
    leading_head_index = lax.axis_index("sp") * shard_head_count
    b_heads = jnp.broadcast_to(
        proj_b.reshape(tok_rows, G, 1, N), (tok_rows, G, per_group, N)
    ).reshape(tok_rows, head_count, N)
    c_heads = jnp.broadcast_to(
        proj_c.reshape(tok_rows, G, 1, N), (tok_rows, G, per_group, N)
    ).reshape(tok_rows, head_count, N)
    pairs = jnp.stack([b_heads, c_heads], axis=2).reshape(tok_rows, head_count * 2 * N)
    x_arrived, pairs_arrived, step_arrived = (
        lax.all_to_all(proj_x, "sp", split_axis=1, concat_axis=0, tiled=True),
        lax.all_to_all(pairs, "sp", split_axis=1, concat_axis=0, tiled=True),
        lax.all_to_all(step_raw, "sp", split_axis=1, concat_axis=0, tiled=True),
    )
    length = x_arrived.shape[0]
    head_ids = leading_head_index + jnp.arange(shard_head_count)
    group_pick = ((head_ids // per_group)[:, None] == jnp.arange(G)[None, :]).astype(jnp.float32)
    taps_x = lax.dynamic_slice_in_dim(
        source_conv_taps, leading_head_index * P_SIZE, shard_head_count * P_SIZE, 1
    )
    taps_b = jnp.einsum(
        "hg,wgn->whn", group_pick, entry_mapping_taps.reshape(CONV_W, G, N)
    ).reshape(CONV_W, shard_head_count * N)
    taps_c = jnp.einsum(
        "hg,wgn->whn", group_pick, readout_mapping_taps.reshape(CONV_W, G, N)
    ).reshape(CONV_W, shard_head_count * N)
    pair_parts = pairs_arrived.reshape(length, shard_head_count, 2, N)
    xs = conv_silu(
        jnp.concatenate(
            [
                jnp.zeros((CONV_W - 1, shard_head_count * P_SIZE), jnp.float32),
                x_arrived.astype(jnp.float32),
            ],
            0,
        ),
        taps_x,
    )
    b_rows = pair_parts[:, :, 0, :].reshape(length, shard_head_count * N).astype(jnp.float32)
    c_rows = pair_parts[:, :, 1, :].reshape(length, shard_head_count * N).astype(jnp.float32)
    bm = conv_silu(
        jnp.concatenate([jnp.zeros((CONV_W - 1, shard_head_count * N), jnp.float32), b_rows], 0),
        taps_b,
    )
    cm = conv_silu(
        jnp.concatenate([jnp.zeros((CONV_W - 1, shard_head_count * N), jnp.float32), c_rows], 0),
        taps_c,
    )
    bias_heads = lax.dynamic_slice_in_dim(
        increment_offsets, leading_head_index, shard_head_count, 0
    )
    speed_per_head = lax.dynamic_slice_in_dim(
        channel_damping_rate, leading_head_index, shard_head_count, 0
    )
    skip_heads = lax.dynamic_slice_in_dim(
        bypass_coefficients, leading_head_index, shard_head_count, 0
    )
    surge_head_values = lax.dynamic_slice_in_dim(
        surge_row_values, leading_head_index, shard_head_count, 1
    )
    step_width_value = jax.nn.softplus(step_arrived.astype(jnp.float32) + bias_heads[None, :])
    logarithm_retain = (
        -speed_per_head[None, :] * step_width_value * tempo_row_values[:, None] + surge_head_values
    )
    blocks = length // BLK
    x_blocks = xs.reshape(blocks, BLK, shard_head_count, 1, P_SIZE)
    b_blocks = bm.reshape(blocks, BLK, shard_head_count, N)
    c_blocks = cm.reshape(blocks, BLK, shard_head_count, N)
    inner, states, block_total, cumulative = block_parts(
        x_blocks,
        b_blocks,
        c_blocks,
        step_width_value.reshape(blocks, BLK, shard_head_count, 1),
        logarithm_retain.reshape(blocks, BLK, shard_head_count, 1),
    )
    carried, final_state, excl_sum, whole_total = block_carry(states, block_total)
    mixed = block_finish(
        inner, c_blocks, cumulative, carried, x_blocks, skip_heads.reshape(shard_head_count, 1)
    )
    mixed = mixed.astype(jnp.bfloat16).reshape(length, shard_head_count * P_SIZE)
    return lax.all_to_all(mixed, "sp", split_axis=0, concat_axis=1, tiled=True)


def shards(
    mixer_source_array,
    source_projection,
    gating_projection,
    entry_mapping_projection,
    readout_mapping_projection,
    increment_projection,
    source_conv_taps,
    entry_mapping_taps,
    readout_mapping_taps,
    increment_offsets,
    channel_damping_rate,
    bypass_coefficients,
    stride_multiplier,
    added_log_damping,
    norm_scale_factor,
    final_projection,
):
    hidden_width = mixer_source_array[0]
    tok_rows = hidden_width.shape[0]
    width_x = source_projection.shape[1]
    pieces = sent_together((source_projection, gating_projection), "dp", 0, 1)
    acc_x = jnp.dot(hidden_width, pieces[0], preferred_element_type=jnp.float32)
    acc_z = jnp.dot(hidden_width, pieces[1], preferred_element_type=jnp.float32)
    proj_x = acc_x.astype(jnp.bfloat16)
    gate_z = acc_z.astype(jnp.bfloat16)
    proj_b = jnp.dot(
        hidden_width, entry_mapping_projection, preferred_element_type=jnp.float32
    ).astype(jnp.bfloat16)
    proj_c = jnp.dot(
        hidden_width, readout_mapping_projection, preferred_element_type=jnp.float32
    ).astype(jnp.bfloat16)
    step_raw = jnp.dot(
        hidden_width, increment_projection, preferred_element_type=jnp.float32
    ).astype(jnp.bfloat16)
    mixed = heads_mixer(
        proj_x,
        proj_b,
        proj_c,
        step_raw,
        source_conv_taps,
        entry_mapping_taps,
        readout_mapping_taps,
        increment_offsets,
        channel_damping_rate,
        bypass_coefficients,
        stride_multiplier[0],
        added_log_damping[0],
    )
    gated = mixed.astype(jnp.float32) * jax.nn.silu(gate_z.astype(jnp.float32))
    grouped = gated.reshape(tok_rows, G, width_x // G)
    normed = grouped * lax.rsqrt(jnp.mean(grouped * grouped, axis=-1, keepdims=True) + EPSILON)
    normed = (normed.reshape(tok_rows, width_x) * norm_scale_factor[None, :]).astype(jnp.bfloat16)
    output = jnp.dot(
        normed,
        lax.all_gather(final_projection, "dp", axis=1, tiled=True),
        preferred_element_type=jnp.float32,
    ).astype(jnp.bfloat16)
    return output[None]


def solution(mesh):
    return jax.shard_map(
        shards,
        mesh=mesh,
        in_specs=(
            P(("grp", "dp"), "sp", None),
            P("dp", None),
            P("dp", None),
            P(),
            P(),
            P(),
            P(),
            P(),
            P(),
            P(),
            P(),
            P(),
            P(("grp", "dp"), None),
            P(("grp", "dp"), None, None),
            P(),
            P(None, "dp"),
        ),
        out_specs=P(("grp", "dp"), "sp", None),
        check_vma=False,
    )
```

profile of v0, /device:TPU:88, one launch (start us, length us, event | category | flops | bytes accessed | tf_op | source)
XLA Modules:
  0.0 266.3 jit_solution(5397178726338997820)
XLA Ops:
  6.6 2.0 pad_maximum_fusion.1
  9.0 0.6 copy.100
  9.6 43.7 %all-to-all-start.1 = ((bf16[192,16,1]{0,2,1:T(2,128)(2,1)}), bf16[192,16,1]{0,2,1:T(2,128)(2,1)S(1)}, u32[]{:S(2)}, u32[]{:S(2)}) async-start(bf16[192,16,1]{0,2,1:T(2,128)(2,1)} %copy.100), calls=%async_computation.1 | async-start | bytes 32768 | tf_op jit(solution)/shard_map/all_to_all | solution.py:105
  54.6 1.6 copy.118
  56.2 2.3 reshape.411
  58.5 7.0 %all-to-all-done.1 = bf16[192,16,1]{0,2,1:T(2,128)(2,1)S(1)} async-done(((bf16[192,16,1]{0,2,1:T(2,128)(2,1)}), bf16[192,16,1]{0,2,1:T(2,128)(2,1)S(1)}, u32[]{:S(2)}, u32[]{:S(2)}) %all-to-all-start.1) | async-done | bytes 6176 | tf_op jit(solution)/shard_map/all_to_all | solution.py:105
  65.6 5.2 %all-to-all-start.2 = ((bf16[192,16,256]{2,0,1:T(8,128)(2,1)}), bf16[192,16,256]{2,0,1:T(8,128)(2,1)}, u32[]{:S(2)}, u32[]{:S(2)}) async-start(bf16[192,16,256]{2,0,1:T(8,128)(2,1)} %reshape.411), calls=%async_computation.2 | async-start | bytes 3145728 | tf_op jit(solution)/shard_map/all_to_all | solution.py:104
  70.8 0.7 all-gather.5.cloned.1.call-update
  71.6 0.6 dynamic_slice.18
  72.2 0.9 dynamic-slice_reduce_fusion
  73.2 0.6 dynamic_slice.19
  74.3 0.5 broadcast.200
  74.9 0.7 reduce.15
  75.6 0.6 dynamic_slice.22
  76.2 0.8 constant_dynamic-slice_fusion
  77.2 0.6 slice_bitcast_fusion.7
  77.8 0.6 bitcast_reduce_fusion
  78.5 1.8 copy.104
  80.3 1.6 fusion.75
  81.9 0.6 copy.105
  83.3 61.0 %all-to-all-done.2 = bf16[192,16,256]{2,0,1:T(8,128)(2,1)} async-done(((bf16[192,16,256]{2,0,1:T(8,128)(2,1)}), bf16[192,16,256]{2,0,1:T(8,128)(2,1)}, u32[]{:S(2)}, u32[]{:S(2)}) %all-to-all-start.2) | async-done | bytes 1572896 | tf_op jit(solution)/shard_map/all_to_all | solution.py:104
  144.3 2.4 reshape.391
  146.7 3.4 %slice_convert_fusion = (f32[3072,1,1,128]{3,2,0,1:T(1,128)}, bf16[3072,1,1,128]{3,2,0,1:T(2,128)(2,1)}) fusion(bf16[3072,1,2,128]{3,2,0,1:T(2,128)(2,1)S(1)} %reshape.391), kind=kLoop, calls=%fused_computation.6 | loop fusion | flops 393216 | bytes 3932160 | tf_op jit(solution)/shard_map/convert_element_type | solution.py:130
  150.1 4.0 %fusion.28 = bf16[192,1024]{1,0:T(8,128)(2,1)} fusion(bf16[2048,2048]{1,0:T(8,128)(2,1)} %all-gather.3.cloned.1.call-done, bf16[1,192,2048]{2,1,0:T(8,128)(2,1)S(1)} %copy-done.1), kind=kOutput, calls=%fused_computation.30 | convolution fusion | flops 805502976 | bytes 5373952 | tf_op jit(solution)/shard_map/dot_general | solution.py:197
  154.1 2.1 copy.98
  156.2 6.5 %all-to-all-start = ((bf16[192,16,64]{0,2,1:T(8,128)(2,1)}), bf16[192,16,64]{0,2,1:T(8,128)(2,1)}, u32[]{:S(2)}, u32[]{:S(2)}) async-start(bf16[192,16,64]{0,2,1:T(8,128)(2,1)} %bitcast.3), calls=%async_computation | async-start | bytes 1048576 | tf_op jit(solution)/shard_map/all_to_all | solution.py:103
  162.9 1.2 copy-done.4
  164.2 1.0 multiply_convert_fusion.2
  165.2 1.0 multiply_convert_fusion.3
  166.2 25.6 %all-to-all-done = bf16[192,16,64]{0,2,1:T(8,128)(2,1)} async-done(((bf16[192,16,64]{0,2,1:T(8,128)(2,1)}), bf16[192,16,64]{0,2,1:T(8,128)(2,1)}, u32[]{:S(2)}, u32[]{:S(2)}) %all-to-all-start) | async-done | bytes 393248 | tf_op jit(solution)/shard_map/all_to_all | solution.py:103
  191.7 1.1 convert_bitcast_fusion
  192.9 1.7 copy.99
  194.6 1.6 reshape.396
  196.2 2.4 broadcast_multiply_fusion
  198.6 2.8 %reshape.397 = f32[48,64,64]{1,0,2:T(8,128)} reshape(f32[3072,64]{0,1:T(8,128)} %get-tuple-element.8) | data formatting | bytes 1572864 | tf_op jit(solution)/shard_map/convert_element_type | solution.py:34
  201.4 1.6 mul.308
  202.9 1.5 multiply_convert_fusion.4
  204.5 0.6 fusion.32
  205.1 0.7 fusion.13
  205.8 1.7 fusion.7
  207.5 3.7 %fusion.5 = bf16[48,64,1,1,64]{1,4,0,3,2:T(8,128)(2,1)} fusion(f32[48,64,64]{2,1,0:T(8,128)} %fusion.7, f32[48,64,1,1,64]{1,0,4,3,2:T(8,128)} %mul.308, bf16[48,64,128]{2,1,0:T(8,128)(2,1)S(1)} %bitcast.145, bf16[48,64,128]{2,1,0:T(8,128)(2,1)S(1)} %bitcast.143, f32[48,64]{1,0:T(8,128)S(1)} %get-tuple-element.11, f32[48,64]{1,0:T(8,128)S(1)} %bitcast.150, ...), kind=kOutput, calls=%fused_computation.9 | convolution fusion | flops 77070336 | bytes 3960832 | tf_op jit(solution)/shard_map/kgrij,kjgrp->kigrp/dot_general | solution.py:45
  211.2 1.6 copy.113
  212.8 0.7 all_to_all.49
  213.7 35.4 %all_to_all.55 = bf16[16,192,64]{1,2,0:T(8,128)(2,1)S(1)} all-to-all(bf16[16,192,64]{1,2,0:T(8,128)(2,1)S(1)} %copy.114), channel_id=1, replica_groups=mesh['grp'=2,'sp'=16,'dp'=16] {'sp'}, dimensions={0} | all-to-all | bytes 786432 | tf_op jit(solution)/shard_map/all_to_all | solution.py:172
  249.2 1.2 copy.115
  250.4 3.5 %fusion.74 = (f32[192,1024]{1,0:T(8,128)S(1)}, f32[192,1024]{1,0:T(8,128)S(1)}) fusion(f32[192,1024]{1,0:T(8,128)} %copy.115, bf16[2048,2048]{1,0:T(8,128)(2,1)} %all-gather.3.cloned.1.call-done, bf16[1,192,2048]{2,1,0:T(8,128)(2,1)S(1)} %copy-done.2), kind=kOutput, calls=%fused_computation.107 | convolution fusion | flops 806879232 | bytes 7340032 | tf_op jit(solution)/shard_map/dot_general | solution.py:198
  253.9 0.7 mul.312
  255.4 4.1 %fusion.4 = bf16[1,192,2048]{2,1,0:T(8,128)(2,1)} fusion(bf16[1024,2048]{1,0:T(8,128)(2,1)} %all-gather.5.cloned.1.call-done, f32[192,1024]{1,0:T(8,128)S(1)} %get-tuple-element.26, f32[192,1024]{1,0:T(8,128)S(1)} %bitcast.149, f32[1024]{0:T(1024)S(1)} %copy-done.11), kind=kOutput, calls=%fused_computation.5 | convolution fusion | flops 806289408 | bytes 6557696 | tf_op jit(solution)/shard_map/dot_general | solution.py:228
  (74 shorter events, 4.2 us)
Async XLA Ops:
  6.5 46.7 %copy-start = (bf16[2048,256]{1,0:T(8,128)(2,1)S(1)}, bf16[2048,256]{1,0:T(8,128)(2,1)}, u32[]{:S(2)}) copy-start(bf16[2048,256]{1,0:T(8,128)(2,1)} %param.19) | copy-start | bytes 3145732
  6.6 2.1 copy-start.1
  6.6 2.1 copy-start.7
  6.6 143.6 %all-gather.3.cloned.1.call-start = ((), (), s32[]{:S(2)}) async-start(), calls=%async_computation.4 | async-start | bytes 8912896 | tf_op jit(solution)/shard_map/all_gather | solution.py:19
  8.6 45.1 %copy-start.6 = (bf16[2048,256]{1,0:T(8,128)(2,1)S(1)}, bf16[2048,256]{1,0:T(8,128)(2,1)}, u32[]{:S(2)}) copy-start(bf16[2048,256]{1,0:T(8,128)(2,1)} %param.20) | copy-start | bytes 3145732
  9.6 56.0 %all-to-all-start.1 = ((bf16[192,16,1]{0,2,1:T(2,128)(2,1)}), bf16[192,16,1]{0,2,1:T(2,128)(2,1)S(1)}, u32[]{:S(2)}, u32[]{:S(2)}) async-start(bf16[192,16,1]{0,2,1:T(2,128)(2,1)} %copy.100), calls=%async_computation.1 | async-start | bytes 32768 | tf_op jit(solution)/shard_map/all_to_all | solution.py:105
  58.5 13.1 %copy-start.9 = (f32[4,256]{1,0:T(4,128)S(1)}, f32[4,256]{1,0:T(4,128)}, u32[]{:S(2)}) copy-start(f32[4,256]{1,0:T(4,128)} %param.23) | copy-start | bytes 12292
  58.5 13.1 %copy-start.16 = (f32[16]{0:T(128)S(1)}, f32[16]{0:T(128)}, u32[]{:S(2)}) copy-start(f32[16]{0:T(128)} %param.25) | copy-start | bytes 196
  58.5 14.7 %copy-start.17 = (f32[16]{0:T(128)S(1)}, f32[16]{0:T(128)}, u32[]{:S(2)}) copy-start(f32[16]{0:T(128)} %param.26) | copy-start | bytes 196
  58.5 16.3 %copy-start.8 = (f32[1,3072]{1,0:T(1,128)S(1)}, f32[1,3072]{1,0:T(1,128)}, u32[]{:S(2)}) copy-start(f32[1,3072]{1,0:T(1,128)} %param.28) | copy-start | bytes 36868
  58.5 17.1 %copy-start.18 = (f32[16]{0:T(128)S(1)}, f32[16]{0:T(128)}, u32[]{:S(2)}) copy-start(f32[16]{0:T(128)} %param.27) | copy-start | bytes 196
  58.5 17.6 %copy-start.10 = (f32[4,256]{1,0:T(4,128)S(1)}, f32[4,256]{1,0:T(4,128)}, u32[]{:S(2)}) copy-start(f32[4,256]{1,0:T(4,128)} %param.24) | copy-start | bytes 12292
  65.6 78.7 %all-to-all-start.2 = ((bf16[192,16,256]{2,0,1:T(8,128)(2,1)}), bf16[192,16,256]{2,0,1:T(8,128)(2,1)}, u32[]{:S(2)}, u32[]{:S(2)}) async-start(bf16[192,16,256]{2,0,1:T(8,128)(2,1)} %reshape.411), calls=%async_computation.2 | async-start | bytes 3145728 | tf_op jit(solution)/shard_map/all_to_all | solution.py:104
  70.7 184.6 %all-gather.5.cloned.1.call-start = ((), (), s32[]{:S(2)}) async-start(), calls=%async_computation.5 | async-start | bytes 4456448 | tf_op jit(solution)/shard_map/all_gather | solution.py:230
  154.1 8.6 %copy-start.3 = (bf16[3072,1,1,128]{3,2,0,1:T(2,128)(2,1)S(1)}, bf16[3072,1,1,128]{3,2,0,1:T(2,128)(2,1)}, u32[]{:S(2)}) copy-start(bf16[3072,1,1,128]{3,2,0,1:T(2,128)(2,1)} %get-tuple-element.10) | copy-start | bytes 2359300
  156.2 35.5 %all-to-all-start = ((bf16[192,16,64]{0,2,1:T(8,128)(2,1)}), bf16[192,16,64]{0,2,1:T(8,128)(2,1)}, u32[]{:S(2)}, u32[]{:S(2)}) async-start(bf16[192,16,64]{0,2,1:T(8,128)(2,1)} %bitcast.3), calls=%async_computation | async-start | bytes 1048576 | tf_op jit(solution)/shard_map/all_to_all | solution.py:103
  162.7 1.4 copy-start.4
  162.9 2.3 copy-start.12
  162.9 2.3 copy-start.13
  162.9 2.3 copy-start.14
  162.9 2.3 copy-start.15
  198.6 2.8 %copy-start.5 = (f32[3072,64]{0,1:T(8,128)S(1)}, f32[3072,64]{0,1:T(8,128)}, u32[]{:S(2)}) copy-start(f32[3072,64]{0,1:T(8,128)} %get-tuple-element.7) | copy-start | bytes 2359300
  249.1 1.3 copy-start.2
  254.6 0.8 copy-start.11
Sparse Core Ops, SparseCore 0:
  9.5 91.6 all-gather.2
  103.3 53.3 all-gather.4
where the time goes:
time: 267 us; the launch traced here: 266 us
  waiting for transfers between devices  94.4 us (35%)
  starting transfers between devices  55.4 us (21%)
  blocking collectives  35.4 us (13%)
  local copies, waits for them, and re-layouts  30.4 us (11%)
  matrix products  19.6 us (7%)
  other arithmetic  16.7 us (6%)
  between operations  14.4 us (5%)
    all_to_all x1, waiting for transfers between devices, heads_mixer(): lax.all_to_all(pairs, 'sp', split_axis=1, concat_axis=0, tiled=True)  61 us
    all_to_all x1, starting transfers between devices, heads_mixer(): lax.all_to_all(step_raw, 'sp', split_axis=1, concat_axis=0, tiled=True)  43.7 us
    all_to_all x1, blocking collectives, heads_mixer(): return lax.all_to_all(mixed, 'sp', split_axis=0, concat_axis=1, tiled=True)  35.4 us
    all_to_all x1, waiting for transfers between devices, heads_mixer(): lax.all_to_all(proj_x, 'sp', split_axis=1, concat_axis=0, tiled=True)  25.6 us
    all_to_all x1, waiting for transfers between devices, heads_mixer(): lax.all_to_all(step_raw, 'sp', split_axis=1, concat_axis=0, tiled=True)  7.02 us
    all_to_all x1, starting transfers between devices, heads_mixer(): lax.all_to_all(proj_x, 'sp', split_axis=1, concat_axis=0, tiled=True)  6.49 us
  transfers between devices with their start and end apart: 5, of which 3 were waited for; matrix products, arithmetic and copies ran while one was open for 22% of the time, Pallas kernels for 0%

commit v1 on v0

v1 whole, which is shorter than its diff:
```python
import functools
import jax
import jax.numpy as jnp
from jax import lax
from jax.experimental import pallas as pl
from jax.experimental.pallas import tpu as pltpu
from jax.sharding import PartitionSpec as P

P_SIZE = 64
N = 128
G = 2
CONV_W = 4
HALO = 16
LANES = 128
EPSILON = 1e-06

F32 = jnp.float32
BF16 = jnp.bfloat16


def silu(x):
    return 0.5 * x * (1.0 + jnp.tanh(0.5 * x))


def rounded_dot(a, b):
    return jnp.dot(a, b, preferred_element_type=F32).astype(BF16).astype(F32)


def conv_silu(padded, taps):
    width = taps.shape[0]
    total = taps[0:1, :] * pltpu.roll(padded, width - 1, 0)[HALO:]
    for k in range(1, width):
        shifted = padded if k == width - 1 else pltpu.roll(padded, width - 1 - k, 0)
        total = total + taps[k : k + 1, :] * shifted[HALO:]
    return silu(total)


def per_head(values, pair, lane):
    return jnp.where(
        lane < P_SIZE, values[:, 2 * pair : 2 * pair + 1], values[:, 2 * pair + 1 : 2 * pair + 2]
    )


def maps_kernel(
    halo, hidden, w_in, w_out, w_step, taps_in, taps_out, offsets, rates, stride, added,
    in_t, out_maps, mixing, step_wide, end_wide, reach_wide, total,
    *, heads,
):
    rows = jnp.concatenate([halo[...], hidden[...]], axis=0)
    length = hidden.shape[0]
    in_maps = conv_silu(rounded_dot(rows, w_in[...]), taps_in[...]).astype(BF16)
    out_m = conv_silu(rounded_dot(rows, w_out[...]), taps_out[...]).astype(BF16)
    out_maps[...] = out_m
    in_tr = in_maps.astype(F32).T.astype(BF16)
    in_t[...] = in_tr
    raw = rounded_dot(hidden[...], w_step[...]) + offsets[...]
    step = jnp.maximum(raw, 0.0) + jnp.log1p(jnp.exp(-jnp.abs(raw)))
    cum = -rates[...] * step * stride[...] + added[...]
    row = lax.broadcasted_iota(jnp.int32, cum.shape, 0)
    shift = 1
    while shift < length:
        cum = cum + jnp.where(row >= shift, pltpu.roll(cum, shift, 0), 0.0)
        shift *= 2
    last = cum[length - 1 : length, :]
    total[...] = last
    to_end = step * jnp.exp(last - cum)
    reach = jnp.exp(cum)
    lane = lax.broadcasted_iota(jnp.int32, (length, LANES), 1)
    for pair in range(heads // 2):
        at = slice(pair * LANES, (pair + 1) * LANES)
        step_wide[:, at] = per_head(step, pair, lane)
        end_wide[:, at] = per_head(to_end, pair, lane)
        reach_wide[:, at] = per_head(reach, pair, lane)
    cum_t = cum.T
    lower = lax.broadcasted_iota(jnp.int32, (length, length), 0) >= lax.broadcasted_iota(
        jnp.int32, (length, length), 1
    )
    per_group = heads // G
    for g in range(G):
        inter = jnp.dot(
            out_m[:, g * N : (g + 1) * N],
            in_tr[g * N : (g + 1) * N, :],
            preferred_element_type=F32,
        )
        for h in range(g * per_group, (g + 1) * per_group):
            gap = cum[:, h : h + 1] - cum_t[h : h + 1, :]
            mixing[h] = (inter * jnp.exp(jnp.where(lower, gap, -jnp.inf))).astype(BF16)


def source_kernel(
    halo, hidden, w_x, taps, step_wide, end_wide, in_t, factors, xs_out, scaled_out, states
):
    rows = jnp.concatenate([halo[...], hidden[...]], axis=0)
    xs = conv_silu(rounded_dot(rows, w_x[...]), taps[...]).astype(BF16)
    xs_out[...] = xs
    xs = xs.astype(F32)
    scaled_out[...] = (xs * step_wide[...]).astype(BF16)
    weighted = (xs * end_wide[...]).astype(BF16)
    states[...] = jnp.dot(in_t[...], weighted, preferred_element_type=F32).astype(BF16)


def inner_kernel(mixing, scaled, xs, skip, base):
    length = scaled.shape[0]
    lane = lax.broadcasted_iota(jnp.int32, (length, LANES), 1)
    for pair in range(scaled.shape[1] // LANES):
        at = slice(pair * LANES, (pair + 1) * LANES)
        both = scaled[:, at]
        first = jnp.dot(mixing[2 * pair], both, preferred_element_type=F32)
        second = jnp.dot(mixing[2 * pair + 1], both, preferred_element_type=F32)
        base[:, at] = jnp.where(lane < P_SIZE, first, second) + skip[:, at] * xs[:, at].astype(F32)


def scan_kernel(states, factors, carried):
    count = factors.shape[0]
    rows = states.shape[0] // count
    acc = jnp.zeros((rows, states.shape[1]), F32)
    for k in range(count):
        at = slice(k * rows, (k + 1) * rows)
        carried[at, :] = acc.astype(BF16)
        acc = acc * factors[k : k + 1, :] + states[at, :].astype(F32)


def gate_kernel(hidden, w_z, after, gate):
    w = jnp.concatenate([w_z[d] for d in range(w_z.shape[0])], axis=0)
    gate[...] = silu(rounded_dot(hidden[...], w))


def finish_kernel(out_maps, carried, reach_wide, base, gate, gain, w_o, output, normed):
    width = base.shape[1] // G

    @pl.when(pl.program_id(0) == 0)
    def _():
        for g in range(G):
            at = slice(g * width, (g + 1) * width)
            reached = jnp.dot(
                out_maps[:, g * N : (g + 1) * N],
                carried[g * N : (g + 1) * N, :],
                preferred_element_type=F32,
            )
            mixed = (base[:, at] + reached * reach_wide[:, at]).astype(BF16).astype(F32)
            gated = mixed * gate[:, at]
            mean = jnp.mean(gated * gated, axis=1, keepdims=True)
            normed[:, at] = (gated * lax.rsqrt(mean + EPSILON) * gain[:, at]).astype(BF16)

    rows = w_o.shape[1]
    w = jnp.concatenate(
        [
            jnp.concatenate(
                [w_o[d, :, b * LANES : (b + 1) * LANES] for b in range(w_o.shape[2] // LANES)], 0
            )
            for d in range(w_o.shape[0])
        ],
        axis=1,
    )
    output[...] = jnp.dot(normed[...], w, preferred_element_type=F32).astype(BF16)


def whole(a):
    nd = len(a.shape)
    return pl.BlockSpec(a.shape, lambda *_: (0,) * nd)


def call(kernel, outs, *args, flops=0, nbytes=0, name=None, **kw):
    return pl.pallas_call(
        kernel,
        out_shape=outs,
        name=name,
        cost_estimate=pl.CostEstimate(flops=flops, transcendentals=0, bytes_accessed=nbytes),
        **kw,
    )(*args)


def shape(dims, kind=F32):
    return jax.ShapeDtypeStruct(dims, kind)


def shards(
    mixer_source_array,
    source_projection,
    gating_projection,
    entry_mapping_projection,
    readout_mapping_projection,
    increment_projection,
    source_conv_taps,
    entry_mapping_taps,
    readout_mapping_taps,
    increment_offsets,
    channel_damping_rate,
    bypass_coefficients,
    stride_multiplier,
    added_log_damping,
    norm_scale_factor,
    final_projection,
):
    hidden = mixer_source_array[0]
    length, d_model = hidden.shape
    width = source_projection.shape[1]
    heads = width // P_SIZE
    k_rows = source_projection.shape[0]
    sp = lax.axis_size("sp")
    dp = lax.axis_size("dp")
    me = lax.axis_index("sp")
    rows_own = G * N // sp

    w_x = lax.all_gather(source_projection, "dp", axis=0, tiled=True)
    halo = lax.ppermute(hidden[length - HALO :], "sp", [(i, i + 1) for i in range(sp - 1)])

    out_cols = final_projection.shape[1]
    w_o_own = jnp.concatenate(
        [final_projection[b * k_rows : (b + 1) * k_rows] for b in range(width // k_rows)], axis=1
    )
    own_zo = jnp.concatenate([gating_projection, w_o_own], axis=0)
    w_zo = lax.all_gather(own_zo, "dp", axis=0, tiled=False)

    pad = LANES - heads
    stride = lax.dynamic_slice_in_dim(stride_multiplier[0], me * length, length, 0)[:, None]
    added = jnp.pad(
        lax.dynamic_slice_in_dim(added_log_damping[0], me * length, length, 0), ((0, 0), (0, pad))
    )
    in_t, out_maps, mixing, step_wide, end_wide, reach_wide, total = call(
        functools.partial(maps_kernel, heads=heads),
        (
            shape((G * N, length), BF16),
            shape((length, G * N), BF16),
            shape((heads, length, length), BF16),
            shape((length, width)),
            shape((length, width)),
            shape((length, width)),
            shape((1, LANES)),
        ),
        halo,
        hidden,
        entry_mapping_projection,
        readout_mapping_projection,
        jnp.pad(increment_projection, ((0, 0), (0, pad))),
        entry_mapping_taps,
        readout_mapping_taps,
        jnp.pad(increment_offsets, (0, pad))[None],
        jnp.pad(channel_damping_rate, (0, pad))[None],
        stride,
        added,
        flops=2 * length * d_model * 5 * LANES * 4,
        name="maps",
    )
    totals = lax.all_gather(total[0], "sp", axis=0, tiled=False)
    own_group = me * rows_own // N
    per_group = heads // G
    factors = jnp.repeat(
        lax.dynamic_slice_in_dim(jnp.exp(totals), own_group * per_group, per_group, 1),
        P_SIZE,
        axis=1,
    )

    cols = 256
    steps = width // cols
    per = steps // G
    xs, scaled, states = call(
        source_kernel,
        (
            shape((length, width), BF16),
            shape((length, width), BF16),
            shape((G * N, width // G), BF16),
        ),
        halo,
        hidden,
        w_x,
        source_conv_taps,
        step_wide,
        end_wide,
        in_t,
        factors,
        grid=(steps,),
        in_specs=[
            whole(halo),
            whole(hidden),
            pl.BlockSpec((d_model, cols), lambda c: (0, c)),
            pl.BlockSpec((CONV_W, cols), lambda c: (0, c)),
            pl.BlockSpec((length, cols), lambda c: (0, c)),
            pl.BlockSpec((length, cols), lambda c: (0, c)),
            pl.BlockSpec((N, length), lambda c: (c // per, 0)),
            whole(factors),
        ],
        out_specs=[
            pl.BlockSpec((length, cols), lambda c: (0, c)),
            pl.BlockSpec((length, cols), lambda c: (0, c)),
            pl.BlockSpec((N, cols), lambda c: (c // per, c % per)),
        ],
        flops=2 * length * d_model * width,
        name="source",
    )
    arrived = lax.all_to_all(states, "sp", split_axis=0, concat_axis=0, tiled=True)

    skip_wide = jnp.repeat(bypass_coefficients, P_SIZE)[None]
    base = call(
        inner_kernel,
        shape((length, width)),
        mixing,
        scaled,
        xs,
        skip_wide,
        flops=2 * length * length * width * 16,
        name="inner",
    )
    own_carried = call(
        scan_kernel, shape(arrived.shape, BF16), arrived, factors, flops=1000, name="scan"
    )
    carried = lax.all_to_all(own_carried, "sp", split_axis=0, concat_axis=0, tiled=True)

    gate = call(
        gate_kernel,
        shape((length, width)),
        hidden,
        w_zo,
        factors,
        grid=(steps,),
        in_specs=[
            whole(hidden),
            pl.BlockSpec((dp, k_rows, cols), lambda c: (0, 0, c)),
            whole(factors),
        ],
        out_specs=pl.BlockSpec((length, cols), lambda c: (0, c)),
        flops=2 * length * d_model * width,
        name="gate",
    )
    two = 2
    output = call(
        finish_kernel,
        shape((length, dp * out_cols), BF16),
        out_maps,
        carried,
        reach_wide,
        base,
        gate,
        norm_scale_factor[None],
        w_zo,
        grid=(dp // two,),
        in_specs=[
            whole(out_maps),
            whole(carried),
            whole(reach_wide),
            whole(base),
            whole(gate),
            pl.BlockSpec((1, width), lambda i: (0, 0)),
            pl.BlockSpec((two, k_rows, width), lambda i: (i, 1, 0)),
        ],
        out_specs=pl.BlockSpec((length, two * out_cols), lambda i: (0, i)),
        scratch_shapes=[pltpu.VMEM((length, width), BF16)],
        flops=2 * length * width * d_model,
        name="finish",
    )
    return output[None]


def solution(mesh):
    return jax.shard_map(
        shards,
        mesh=mesh,
        in_specs=(
            P(("grp", "dp"), "sp", None),
            P("dp", None),
            P("dp", None),
            P(),
            P(),
            P(),
            P(),
            P(),
            P(),
            P(),
            P(),
            P(),
            P(("grp", "dp"), None),
            P(("grp", "dp"), None, None),
            P(),
            P(None, "dp"),
        ),
        out_specs=P(("grp", "dp"), "sp", None),
        check_vma=False,
    )
```

time: 267 us -> 178 us (0.67)
  the two profiles are of different devices: /device:TPU:88 before, /device:TPU:65 now
where the time goes in v1:
time: 178 us; the launch traced here: 176 us
  blocking collectives  83.4 us (47%)
  Pallas kernels  30.7 us (17%)
  starting transfers between devices  17 us (10%)
  local copies, waits for them, and re-layouts  14.9 us (8%)
  waiting for transfers between devices  14.9 us (8%)
  between operations  13.5 us (8%)
  other arithmetic  1.82 us (1%)
    all_gather x1, blocking collectives, shards(): totals = lax.all_gather(total[0], 'sp', axis=0, tiled=False)  59.1 us
    pallas_call x6, Pallas kernels, call(): pl.pallas_call(kernel, out_shape=outs, name=name, cost_estimate=pl.CostEs...  30.7 us
    all_to_all x1, blocking collectives, shards(): lax.all_to_all(states, 'sp', split_axis=0, concat_axis=0, tiled=True)  24.3 us
    all_gather x1, waiting for transfers between devices, shards(): w_zo = lax.all_gather(own_zo, 'dp', axis=0, tiled=False)  14.1 us
    all_to_all x1, starting transfers between devices, shards(): lax.all_to_all(own_carried, 'sp', split_axis=0, concat_axis=0, tiled=True)  10.4 us
    unnamed x20, local copies, waits for them, and re-layouts  7.84 us
    ppermute x1, starting transfers between devices, shards(): lax.ppermute(hidden[length - HALO:], 'sp', [(i, i + 1) for i in range(sp...  6.55 us
  transfers between devices with their start and end apart: 4, of which 1 were waited for; matrix products, arithmetic and copies ran while one was open for 9% of the time, Pallas kernels for 13%

profile of v1, /device:TPU:65, one launch (start us, length us, event | category | flops | bytes accessed | tf_op | source)
XLA Modules:
  0.0 176.3 jit_solution(16061344098532099922)
XLA Ops:
  6.5 0.0 copy-start
  6.6 0.0 copy-start.4
  6.6 0.0 all-gather.5.cloned.1.call-start
  6.6 0.7 all-gather.5.cloned.1.call-update
  7.3 0.1 all-gather.7.cloned.1.call-start
  7.4 0.8 slice_dynamic-update-slice_fusion.7
  8.1 0.8 slice_dynamic-update-slice_fusion.6
  8.9 0.8 slice_dynamic-update-slice_fusion.5
  9.7 0.8 slice_dynamic-update-slice_fusion.4
  10.5 0.8 slice_dynamic-update-slice_fusion.3
  11.2 0.8 slice_dynamic-update-slice_fusion.2
  12.0 0.8 slice_dynamic-update-slice_fusion.1
  12.8 0.8 slice_dynamic-update-slice_fusion
  13.6 1.8 %pad_maximum_fusion = bf16[256,1024]{1,0:T(8,128)(2,1)} fusion(bf16[128,1024]{1,0:T(8,128)(2,1)S(1)} %slice_dynamic-update-slice_fusion, bf16[128,1024]{1,0:T(8,128)(2,1)} %param.18), kind=kLoop, calls=%fused_computation | loop fusion | flops 1048576 | bytes 1048576 | tf_op jit(solution)/shard_map/concatenate | solution.py:212
  15.4 0.1 all-gather.7.cloned.1.call-update
  15.4 0.8 slice_bitcast_fusion
  16.3 6.6 %collective-permute-start = (bf16[16,2048]{1,0:T(8,128)(2,1)S(1)}, bf16[16,2048]{1,0:T(8,128)(2,1)S(1)}, u32[]{:S(2)}, u32[]{:S(2)}) collective-permute-start(bf16[16,2048]{1,0:T(8,128)(2,1)S(1)} %slice_bitcast_fusion), channel_id=1, source_target_pairs={{0,16},{16,32},{32,48},{48,64},{64,80},{80,96},{96,112},{112,128},... | collective-permute-start | bytes 196616 | tf_op jit(solution)/shard_map/ppermute | solution.py:206
  22.9 1.1 copy.31
  24.0 0.8 dynamic-slice_bitcast_fusion
  24.7 0.8 copy.33.stride
  25.5 0.0 copy-done
  25.5 0.1 constant_dynamic-slice_fusion
  25.6 0.1 copy.32
  25.7 0.9 pad.15.w_step
  26.6 0.6 pad.18.added
  27.3 0.0 copy-done.4
  27.3 0.0 copy-done.5
  27.3 0.5 pad_bitcast_fusion
  27.8 0.0 collective-permute-done.halo
  27.8 0.6 copy-done.2
  28.5 6.8 %maps.1 = (bf16[256,192]{1,0:T(8,128)(2,1)}, bf16[192,256]{1,0:T(8,128)(2,1)}, bf16[16,192,192]{2,1,0:T(8,128)(2,1)}, f32[192,1024]{1,0:T(8,128)}, f32[192,1024]...) custom-call(bf16[16,2048]{1,0:T(8,128)(2,1)} %copy-done.2, bf16[192,2048]{1,0:T(8,128)(2,1)} %bitcast.23, ...), custom_call_target="tpu_custom_call" | custom-call | flops 2013265920 | tf_op jit(solution)/shard_map/maps/pallas_call | solution.py:164
  35.2 59.1 %all-gather.1 = f32[16,1,128]{2,1,0:T(1,128)S(1)} all-gather(f32[1,1,128]{2,1,0:T(1,128)} %bitcast.33), channel_id=1, replica_groups=mesh['grp'=2,'sp'=16,'dp'=16] {'sp'}, dimensions={0}, use_global_device_ids=true | all-gather | bytes 8704 | tf_op jit(solution)/shard_map/all_gather | solution.py:245
  94.3 0.1 fusion
  94.4 0.1 broadcast_in_dim.24
  94.4 0.7 reshape.11.factors.after
  95.1 6.0 %source.1 = (bf16[192,1024]{1,0:T(8,128)(2,1)}, bf16[192,1024]{1,0:T(8,128)(2,1)}, bf16[256,512]{1,0:T(8,128)(2,1)}) custom-call(bf16[16,2048]{1,0:T(8,128)(2,1)} %copy-done.2, bf16[192,2048]{1,0:T(8,128)(2,1)} %bitcast.24, bf16[2048,1024]{1,0:T(8,128)(2,1)} %all-gather.5.cloned.1.call-done.w_x, f32[4,1024]{1,0:T(4,128)} %taps.1, ...), custom_call_target="tpu_custom_call" | custom-call | flops 805306368 | tf_op jit(solution)/shard_map/source/pallas_call | solution.py:164
  101.2 24.3 %all_to_all.22 = bf16[16,16,512]{2,1,0:T(8,128)(2,1)} all-to-all(bf16[16,16,512]{2,1,0:T(8,128)(2,1)} %bitcast.30), channel_id=1, replica_groups=mesh['grp'=2,'sp'=16,'dp'=16] {'sp'}, dimensions={0} | all-to-all | bytes 524288 | tf_op jit(solution)/shard_map/all_to_all | solution.py:291
  125.5 1.7 scan.1
  127.2 10.4 %all-to-all-start.1 = ((bf16[16,16,512]{2,1,0:T(8,128)(2,1)}), bf16[16,16,512]{2,1,0:T(8,128)(2,1)S(1)}, u32[]{:S(2)}, u32[]{:S(2)}) async-start(bf16[16,16,512]{2,1,0:T(8,128)(2,1)} %bitcast.27), calls=%async_computation.1 | async-start | bytes 524288 | tf_op jit(solution)/shard_map/all_to_all | solution.py:307
  137.6 0.0 copy-done.3
  137.6 0.1 broadcast_in_dim.25
  137.7 0.7 broadcast_in_dim_reshape.3.skip
  138.4 3.2 %inner.1.base = f32[192,1024]{1,0:T(8,128)} custom-call(bf16[16,192,192]{2,1,0:T(8,128)(2,1)} %get-tuple-element.22.mixing, bf16[192,1024]{1,0:T(8,128)(2,1)} %get-tuple-element.23.scaled, bf16[192,1024]{1,0:T(8,128)(2,1)} %get-tuple-element.24.xs, f32[1,1024]{1,0:T(1,128)} %broadcast_in_dim_reshape.3.skip), custom_call_target="tpu_custom_call" | custom-call | flops 1207959552 | tf_op jit(solution)/shard_map/inner/pallas_call | solution.py:164
  141.6 14.1 %all-gather.7.cloned.1.call-done = bf16[4096,1024]{1,0:T(8,128)(2,1)} async-done(((bf16[256,1024]{1,0:T(8,128)(2,1)}), bf16[4096,1024]{1,0:T(8,128)(2,1)}) %all-gather.7.cloned.1.call-update) | async-done | bytes 8388624 | tf_op jit(solution)/shard_map/all_gather | solution.py:213
  155.7 5.0 %gate.1 = f32[192,1024]{1,0:T(8,128)} custom-call(bf16[192,2048]{1,0:T(8,128)(2,1)} %bitcast.25, bf16[16,256,1024]{2,1,0:T(8,128)(2,1)} %bitcast.21, f32[16,512]{1,0:T(8,128)} %reshape.11.factors.after), custom_call_target="tpu_custom_call" | custom-call | flops 805306368 | tf_op jit(solution)/shard_map/gate/pallas_call | solution.py:164
  160.7 0.0 all-to-all-done.1
  160.7 0.7 copy-done.1
  161.4 8.0 %finish.1 = bf16[192,2048]{1,0:T(8,128)(2,1)} custom-call(bf16[192,256]{1,0:T(8,128)(2,1)} %get-tuple-element.15.out_maps, bf16[256,512]{1,0:T(8,128)(2,1)} %bitcast.26, f32[192,1024]{1,0:T(8,128)} %get-tuple-element.21.reach_wide, f32[192,1024]{1,0:T(8,128)} %inner.1.base, f32[192,1024]{1,0:T(8,128)} %gate.1, f32[1,1024]{1,0:T(1,128)} %bitcast.32, ...), custom_call_target="tpu_custom_call" | custom-call | flops 805306368 | tf_op jit(solution)/shard_map/finish/pallas_call | solution.py:164
  (5 shorter events, 0.0 us)
Async XLA Ops:
  6.5 19.0 %copy-start = (f32[1,3072,16]{1,2,0:T(8,128)S(1)}, f32[1,3072,16]{1,2,0:T(8,128)}, u32[]{:S(2)}) copy-start(f32[1,3072,16]{1,2,0:T(8,128)} %param.29) | copy-start | bytes 589828
  6.6 20.7 %copy-start.4 = (f32[16]{0:T(128)S(1)}, f32[16]{0:T(128)}, u32[]{:S(2)}) copy-start(f32[16]{0:T(128)} %param.26) | copy-start | bytes 196
  6.6 20.7 %copy-start.5 = (f32[16]{0:T(128)S(1)}, f32[16]{0:T(128)}, u32[]{:S(2)}) copy-start(f32[16]{0:T(128)} %param.25) | copy-start | bytes 196
  6.6 88.6 %all-gather.5.cloned.1.call-start = ((), (), s32[]{:S(2)}) async-start(), calls=%async_computation.2 | async-start | bytes 4456448 | tf_op jit(solution)/shard_map/all_gather | solution.py:205
  7.3 148.4 %all-gather.7.cloned.1.call-start = ((), (), s32[]{:S(2)}) async-start(), calls=%async_computation.3 | async-start | bytes 8912896 | tf_op jit(solution)/shard_map/all_gather | solution.py:213
  16.3 11.6 %collective-permute-start = (bf16[16,2048]{1,0:T(8,128)(2,1)S(1)}, bf16[16,2048]{1,0:T(8,128)(2,1)S(1)}, u32[]{:S(2)}, u32[]{:S(2)}) collective-permute-start(bf16[16,2048]{1,0:T(8,128)(2,1)S(1)} %slice_bitcast_fusion), channel_id=1, source_target_pairs={{0,16},{16,32},{32,48},{48,64},{64,80},{80,96},{96,112},{112,128},... | collective-permute-start | bytes 196616 | tf_op jit(solution)/shard_map/ppermute | solution.py:206
  27.8 0.6 copy-start.2
  95.1 42.5 %copy-start.3 = (f32[16]{0:T(128)S(1)}, f32[16]{0:T(128)}, u32[]{:S(2)}) copy-start(f32[16]{0:T(128)} %param.27) | copy-start | bytes 196
  127.2 33.5 %all-to-all-start.1 = ((bf16[16,16,512]{2,1,0:T(8,128)(2,1)}), bf16[16,16,512]{2,1,0:T(8,128)(2,1)S(1)}, u32[]{:S(2)}, u32[]{:S(2)}) async-start(bf16[16,16,512]{2,1,0:T(8,128)(2,1)} %bitcast.27), calls=%async_computation.1 | async-start | bytes 524288 | tf_op jit(solution)/shard_map/all_to_all | solution.py:307
  160.7 0.7 copy-start.1
Sparse Core Ops, SparseCore 0:
  9.5 83.0 all-gather.4
  94.8 60.8 all-gather.6

commit v2 on v1

--- a/solution.py
+++ b/solution.py
@@ -120,39 +120,54 @@
         acc = acc * factors[k : k + 1, :] + states[at, :].astype(F32)
 
 
-def gate_kernel(hidden, w_z, after, gate):
-    w = jnp.concatenate([w_z[d] for d in range(w_z.shape[0])], axis=0)
-    gate[...] = silu(rounded_dot(hidden[...], w))
-
-
-def finish_kernel(out_maps, carried, reach_wide, base, gate, gain, w_o, output, normed):
+def blend_kernel(out_maps, carried, reach_wide, base, mixed):
     width = base.shape[1] // G
-
-    @pl.when(pl.program_id(0) == 0)
+    for g in range(G):
+        at = slice(g * width, (g + 1) * width)
+        reached = jnp.dot(
+            out_maps[:, g * N : (g + 1) * N],
+            carried[g * N : (g + 1) * N, :],
+            preferred_element_type=F32,
+        )
+        mixed[:, at] = (base[:, at] + reached * reach_wide[:, at]).astype(BF16)
+
+
+def tail_kernel(hidden, mixed, gain, w_z, w_o, output, gated, normed, *, gate_steps):
+    step = pl.program_id(0)
+    width = mixed.shape[1] // G
+
+    @pl.when(step < gate_steps)
+    def _():
+        w = jnp.concatenate([w_z[d] for d in range(w_z.shape[0])], axis=0)
+        gate = silu(rounded_dot(hidden[...], w))
+        for k in range(gate_steps):
+
+            @pl.when(step == k)
+            def _():
+                at = slice(k * w.shape[1], (k + 1) * w.shape[1])
+                gated[:, at] = mixed[:, at].astype(F32) * gate
+
+    @pl.when(step == gate_steps)
     def _():
         for g in range(G):
             at = slice(g * width, (g + 1) * width)
-            reached = jnp.dot(
-                out_maps[:, g * N : (g + 1) * N],
-                carried[g * N : (g + 1) * N, :],
-                preferred_element_type=F32,
-            )
-            mixed = (base[:, at] + reached * reach_wide[:, at]).astype(BF16).astype(F32)
-            gated = mixed * gate[:, at]
-            mean = jnp.mean(gated * gated, axis=1, keepdims=True)
-            normed[:, at] = (gated * lax.rsqrt(mean + EPSILON) * gain[:, at]).astype(BF16)
-
-    rows = w_o.shape[1]
-    w = jnp.concatenate(
-        [
-            jnp.concatenate(
-                [w_o[d, :, b * LANES : (b + 1) * LANES] for b in range(w_o.shape[2] // LANES)], 0
-            )
-            for d in range(w_o.shape[0])
-        ],
-        axis=1,
-    )
-    output[...] = jnp.dot(normed[...], w, preferred_element_type=F32).astype(BF16)
+            own = gated[:, at]
+            mean = jnp.mean(own * own, axis=1, keepdims=True)
+            normed[:, at] = (own * lax.rsqrt(mean + EPSILON) * gain[:, at]).astype(BF16)
+
+    @pl.when(step >= gate_steps)
+    def _():
+        w = jnp.concatenate(
+            [
+                jnp.concatenate(
+                    [w_o[d, :, b * LANES : (b + 1) * LANES] for b in range(w_o.shape[2] // LANES)],
+                    0,
+                )
+                for d in range(w_o.shape[0])
+            ],
+            axis=1,
+        )
+        output[...] = jnp.dot(normed[...], w, preferred_element_type=F32).astype(BF16)
 
 
 def whole(a):
@@ -306,47 +321,39 @@
     )
     carried = lax.all_to_all(own_carried, "sp", split_axis=0, concat_axis=0, tiled=True)
 
-    gate = call(
-        gate_kernel,
-        shape((length, width)),
-        hidden,
-        w_zo,
-        factors,
-        grid=(steps,),
-        in_specs=[
-            whole(hidden),
-            pl.BlockSpec((dp, k_rows, cols), lambda c: (0, 0, c)),
-            whole(factors),
-        ],
-        out_specs=pl.BlockSpec((length, cols), lambda c: (0, c)),
-        flops=2 * length * d_model * width,
-        name="gate",
-    )
-    two = 2
-    output = call(
-        finish_kernel,
-        shape((length, dp * out_cols), BF16),
+    mixed = call(
+        blend_kernel,
+        shape((length, width), BF16),
         out_maps,
         carried,
         reach_wide,
         base,
-        gate,
+        flops=2 * length * N * width,
+        name="blend",
+    )
+    two = 2
+    output = call(
+        functools.partial(tail_kernel, gate_steps=steps),
+        shape((length, dp * out_cols), BF16),
+        hidden,
+        mixed,
         norm_scale_factor[None],
         w_zo,
-        grid=(dp // two,),
+        w_zo,
+        grid=(steps + dp // two,),
         in_specs=[
-            whole(out_maps),
-            whole(carried),
-            whole(reach_wide),
-            whole(base),
-            whole(gate),
+            whole(hidden),
+            whole(mixed),
             pl.BlockSpec((1, width), lambda i: (0, 0)),
-            pl.BlockSpec((two, k_rows, width), lambda i: (i, 1, 0)),
+            pl.BlockSpec((dp, k_rows, cols), lambda i: (0, 0, jnp.minimum(i, steps - 1))),
+            pl.BlockSpec((two, k_rows, width), lambda i: (jnp.maximum(i - steps, 0), 1, 0)),
         ],
-        out_specs=pl.BlockSpec((length, two * out_cols), lambda i: (0, i)),
-        scratch_shapes=[pltpu.VMEM((length, width), BF16)],
-        flops=2 * length * width * d_model,
-        name="finish",
+        out_specs=pl.BlockSpec(
+            (length, two * out_cols), lambda i: (0, jnp.maximum(i - steps, 0))
+        ),
+        scratch_shapes=[pltpu.VMEM((length, width), F32), pltpu.VMEM((length, width), BF16)],
+        flops=4 * length * width * d_model,
+        name="tail",
     )
     return output[None]
 

time: 178 us -> 177 us (level)
  the two profiles are of different devices: /device:TPU:65 before, /device:TPU:66 now
where the time goes in v2:
time: 177 us; the launch traced here: 176 us
  blocking collectives  87.3 us (49%)
  Pallas kernels  30.8 us (17%)
  waiting for transfers between devices  15.1 us (9%)
  local copies, waits for them, and re-layouts  14.9 us (8%)
  between operations  13.5 us (8%)
  starting transfers between devices  12.3 us (7%)
  other arithmetic  1.82 us (1%)
    all_gather x1, blocking collectives, shards(): totals = lax.all_gather(total[0], 'sp', axis=0, tiled=False)  63.7 us
    pallas_call x6, Pallas kernels, call(): pl.pallas_call(kernel, out_shape=outs, name=name, cost_estimate=pl.CostEs...  30.8 us
    all_to_all x1, blocking collectives, shards(): lax.all_to_all(states, 'sp', split_axis=0, concat_axis=0, tiled=True)  23.5 us
    all_to_all x1, waiting for transfers between devices, shards(): lax.all_to_all(own_carried, 'sp', split_axis=0, concat_axis=0, tiled=True)  14.3 us
    unnamed x20, local copies, waits for them, and re-layouts  7.84 us
    all_to_all x1, starting transfers between devices, shards(): lax.all_to_all(own_carried, 'sp', split_axis=0, concat_axis=0, tiled=True)  6.18 us
    ppermute x1, starting transfers between devices, shards(): lax.ppermute(hidden[length - HALO:], 'sp', [(i, i + 1) for i in range(sp...  6.02 us
  transfers between devices with their start and end apart: 4, of which 1 were waited for; matrix products, arithmetic and copies ran while one was open for 9% of the time, Pallas kernels for 11%

profile of v2, /device:TPU:66, one launch (start us, length us, event | category | flops | bytes accessed | tf_op | source)
XLA Modules:
  0.0 175.6 jit_solution(13233011367170572073)
XLA Ops:
  6.5 0.0 copy-start
  6.6 0.0 copy-start.5
  6.6 0.0 copy-start.4
  6.6 0.0 all-gather.5.cloned.1.call-start
  6.6 0.7 all-gather.5.cloned.1.call-update
  7.3 0.1 all-gather.7.cloned.1.call-start
  7.4 0.8 slice_dynamic-update-slice_fusion.7
  8.1 0.8 slice_dynamic-update-slice_fusion.6
  8.9 0.8 slice_dynamic-update-slice_fusion.5
  9.7 0.8 slice_dynamic-update-slice_fusion.4
  10.5 0.8 slice_dynamic-update-slice_fusion.3
  11.2 0.8 slice_dynamic-update-slice_fusion.2
  12.0 0.8 slice_dynamic-update-slice_fusion.1
  12.8 0.8 slice_dynamic-update-slice_fusion
  13.6 1.8 %pad_maximum_fusion = bf16[256,1024]{1,0:T(8,128)(2,1)} fusion(bf16[128,1024]{1,0:T(8,128)(2,1)S(1)} %slice_dynamic-update-slice_fusion, bf16[128,1024]{1,0:T(8,128)(2,1)} %param.18), kind=kLoop, calls=%fused_computation | loop fusion | flops 1048576 | bytes 1048576 | tf_op jit(solution)/shard_map/concatenate | solution.py:227
  15.4 0.1 all-gather.7.cloned.1.call-update
  15.4 0.8 slice_bitcast_fusion
  16.3 6.0 %collective-permute-start = (bf16[16,2048]{1,0:T(8,128)(2,1)S(1)}, bf16[16,2048]{1,0:T(8,128)(2,1)S(1)}, u32[]{:S(2)}, u32[]{:S(2)}) collective-permute-start(bf16[16,2048]{1,0:T(8,128)(2,1)S(1)} %slice_bitcast_fusion), channel_id=1, source_target_pairs={{0,16},{16,32},{32,48},{48,64},{64,80},{80,96},{96,112},{112,128},... | collective-permute-start | bytes 196616 | tf_op jit(solution)/shard_map/ppermute | solution.py:221
  22.3 0.0 copy-done
  22.3 0.1 constant_dynamic-slice_fusion
  22.4 0.1 copy.32
  22.5 0.8 dynamic-slice_bitcast_fusion
  23.3 0.8 copy.33.stride
  24.1 1.1 copy.31
  25.2 0.6 pad.18.added
  25.8 0.9 pad.15.w_step
  26.8 0.0 copy-done.5
  26.8 0.0 copy-done.4
  26.8 0.5 pad_bitcast_fusion
  27.3 0.0 collective-permute-done.halo
  27.3 0.6 copy-done.2
  27.9 6.8 %maps.1 = (bf16[256,192]{1,0:T(8,128)(2,1)}, bf16[192,256]{1,0:T(8,128)(2,1)}, bf16[16,192,192]{2,1,0:T(8,128)(2,1)}, f32[192,1024]{1,0:T(8,128)}, f32[192,1024]...) custom-call(bf16[16,2048]{1,0:T(8,128)(2,1)} %copy-done.2, bf16[192,2048]{1,0:T(8,128)(2,1)} %bitcast.23, ...), custom_call_target="tpu_custom_call" | custom-call | flops 2013265920 | tf_op jit(solution)/shard_map/maps/pallas_call | solution.py:179
  34.7 63.7 %all-gather.1 = f32[16,1,128]{2,1,0:T(1,128)S(1)} all-gather(f32[1,1,128]{2,1,0:T(1,128)} %bitcast.33), channel_id=1, replica_groups=mesh['grp'=2,'sp'=16,'dp'=16] {'sp'}, dimensions={0}, use_global_device_ids=true | all-gather | bytes 8704 | tf_op jit(solution)/shard_map/all_gather | solution.py:260
  98.4 0.1 fusion
  98.5 0.1 broadcast_in_dim.24
  98.6 0.7 reshape.11.factors
  99.3 6.0 %source.1 = (bf16[192,1024]{1,0:T(8,128)(2,1)}, bf16[192,1024]{1,0:T(8,128)(2,1)}, bf16[256,512]{1,0:T(8,128)(2,1)}) custom-call(bf16[16,2048]{1,0:T(8,128)(2,1)} %copy-done.2, bf16[192,2048]{1,0:T(8,128)(2,1)} %bitcast.24, bf16[2048,1024]{1,0:T(8,128)(2,1)} %all-gather.5.cloned.1.call-done.w_x, f32[4,1024]{1,0:T(4,128)} %taps.1, ...), custom_call_target="tpu_custom_call" | custom-call | flops 805306368 | tf_op jit(solution)/shard_map/source/pallas_call | solution.py:179
  105.3 23.5 %all_to_all.22 = bf16[16,16,512]{2,1,0:T(8,128)(2,1)} all-to-all(bf16[16,16,512]{2,1,0:T(8,128)(2,1)} %bitcast.30), channel_id=1, replica_groups=mesh['grp'=2,'sp'=16,'dp'=16] {'sp'}, dimensions={0} | all-to-all | bytes 524288 | tf_op jit(solution)/shard_map/all_to_all | solution.py:306
  128.8 1.7 scan.1
  130.6 6.2 %all-to-all-start.1 = ((bf16[16,16,512]{2,1,0:T(8,128)(2,1)}), bf16[16,16,512]{2,1,0:T(8,128)(2,1)S(1)}, u32[]{:S(2)}, u32[]{:S(2)}) async-start(bf16[16,16,512]{2,1,0:T(8,128)(2,1)} %bitcast.27), calls=%async_computation.1 | async-start | bytes 524288 | tf_op jit(solution)/shard_map/all_to_all | solution.py:322
  136.7 0.0 copy-done.3
  136.8 0.1 broadcast_in_dim.25
  136.8 0.7 broadcast_in_dim_reshape.3.skip
  137.5 3.1 %inner.1.base = f32[192,1024]{1,0:T(8,128)} custom-call(bf16[16,192,192]{2,1,0:T(8,128)(2,1)} %get-tuple-element.22.mixing, bf16[192,1024]{1,0:T(8,128)(2,1)} %get-tuple-element.23.scaled, bf16[192,1024]{1,0:T(8,128)(2,1)} %get-tuple-element.24.xs, f32[1,1024]{1,0:T(1,128)} %broadcast_in_dim_reshape.3.skip), custom_call_target="tpu_custom_call" | custom-call | flops 1207959552 | tf_op jit(solution)/shard_map/inner/pallas_call | solution.py:179
  140.6 14.3 %all-to-all-done.1 = bf16[16,16,512]{2,1,0:T(8,128)(2,1)S(1)} async-done(((bf16[16,16,512]{2,1,0:T(8,128)(2,1)}), bf16[16,16,512]{2,1,0:T(8,128)(2,1)S(1)}, u32[]{:S(2)}, u32[]{:S(2)}) %all-to-all-start.1) | async-done | bytes 262176 | tf_op jit(solution)/shard_map/all_to_all | solution.py:322
  154.9 0.7 copy-done.1
  155.6 2.5 %blend.1.mixed = bf16[192,1024]{1,0:T(8,128)(2,1)} custom-call(bf16[192,256]{1,0:T(8,128)(2,1)} %get-tuple-element.15.out_maps, bf16[256,512]{1,0:T(8,128)(2,1)} %bitcast.26, f32[192,1024]{1,0:T(8,128)} %get-tuple-element.21.reach_wide, f32[192,1024]{1,0:T(8,128)} %inner.1.base), custom_call_target="tpu_custom_call" | custom-call | flops 50331648 | tf_op jit(solution)/shard_map/blend/pallas_call | solution.py:179
  158.1 10.7 %tail.1 = bf16[192,2048]{1,0:T(8,128)(2,1)} custom-call(bf16[192,2048]{1,0:T(8,128)(2,1)} %bitcast.25, bf16[192,1024]{1,0:T(8,128)(2,1)} %blend.1.mixed, f32[1,1024]{1,0:T(1,128)} %bitcast.32, bf16[16,256,1024]{2,1,0:T(8,128)(2,1)} %bitcast.21, bf16[16,256,1024]{2,1,0:T(8,128)(2,1)} %bitcast.22), custom_call_target="tpu_custom_call" | custom-call | flops 1610612736 | tf_op jit(solution)/shard_map/tail/pallas_call | solution.py:179
  (5 shorter events, 0.0 us)
Async XLA Ops:
  6.5 15.8 %copy-start = (f32[1,3072,16]{1,2,0:T(8,128)S(1)}, f32[1,3072,16]{1,2,0:T(8,128)}, u32[]{:S(2)}) copy-start(f32[1,3072,16]{1,2,0:T(8,128)} %param.29) | copy-start | bytes 589828
  6.6 20.2 %copy-start.5 = (f32[16]{0:T(128)S(1)}, f32[16]{0:T(128)}, u32[]{:S(2)}) copy-start(f32[16]{0:T(128)} %param.25) | copy-start | bytes 196
  6.6 20.2 %copy-start.4 = (f32[16]{0:T(128)S(1)}, f32[16]{0:T(128)}, u32[]{:S(2)}) copy-start(f32[16]{0:T(128)} %param.26) | copy-start | bytes 196
  6.6 92.7 %all-gather.5.cloned.1.call-start = ((), (), s32[]{:S(2)}) async-start(), calls=%async_computation.2 | async-start | bytes 4456448 | tf_op jit(solution)/shard_map/all_gather | solution.py:220
  7.3 150.8 %all-gather.7.cloned.1.call-start = ((), (), s32[]{:S(2)}) async-start(), calls=%async_computation.3 | async-start | bytes 8912896 | tf_op jit(solution)/shard_map/all_gather | solution.py:228
  16.3 11.0 %collective-permute-start = (bf16[16,2048]{1,0:T(8,128)(2,1)S(1)}, bf16[16,2048]{1,0:T(8,128)(2,1)S(1)}, u32[]{:S(2)}, u32[]{:S(2)}) collective-permute-start(bf16[16,2048]{1,0:T(8,128)(2,1)S(1)} %slice_bitcast_fusion), channel_id=1, source_target_pairs={{0,16},{16,32},{32,48},{48,64},{64,80},{80,96},{96,112},{112,128},... | collective-permute-start | bytes 196616 | tf_op jit(solution)/shard_map/ppermute | solution.py:221
  27.3 0.6 copy-start.2
  99.3 37.5 %copy-start.3 = (f32[16]{0:T(128)S(1)}, f32[16]{0:T(128)}, u32[]{:S(2)}) copy-start(f32[16]{0:T(128)} %param.27) | copy-start | bytes 196
  130.6 24.3 %all-to-all-start.1 = ((bf16[16,16,512]{2,1,0:T(8,128)(2,1)}), bf16[16,16,512]{2,1,0:T(8,128)(2,1)S(1)}, u32[]{:S(2)}, u32[]{:S(2)}) async-start(bf16[16,16,512]{2,1,0:T(8,128)(2,1)} %bitcast.27), calls=%async_computation.1 | async-start | bytes 524288 | tf_op jit(solution)/shard_map/all_to_all | solution.py:322
  154.9 0.7 copy-start.1
Sparse Core Ops, SparseCore 0:
  9.5 81.6 all-gather.4
  93.4 59.6 all-gather.6

commit v3 on v1

v3 whole, which is shorter than its diff:
```python
import functools
import jax
import jax.numpy as jnp
from jax import lax
from jax.experimental import pallas as pl
from jax.experimental.pallas import tpu as pltpu
from jax.sharding import PartitionSpec as P

P_SIZE = 64
N = 128
G = 2
CONV_W = 4
HALO = 16
LANES = 128
EPSILON = 1e-06

F32 = jnp.float32
BF16 = jnp.bfloat16


def silu(x):
    return 0.5 * x * (1.0 + jnp.tanh(0.5 * x))


def rounded_dot(a, b):
    return jnp.dot(a, b, preferred_element_type=F32).astype(BF16).astype(F32)


def conv_silu(padded, taps):
    width = taps.shape[0]
    total = taps[0:1, :] * pltpu.roll(padded, width - 1, 0)[HALO:]
    for k in range(1, width):
        shifted = padded if k == width - 1 else pltpu.roll(padded, width - 1 - k, 0)
        total = total + taps[k : k + 1, :] * shifted[HALO:]
    return silu(total)


def per_head(values, pair, lane):
    return jnp.where(
        lane < P_SIZE, values[:, 2 * pair : 2 * pair + 1], values[:, 2 * pair + 1 : 2 * pair + 2]
    )


def pick_kernel(side, w_x, w_z, picked):
    rows = w_x.shape[0]
    picked[:rows, :] = w_x[...]
    picked[rows:, :] = w_z[...]


def maps_kernel(
    side, halo_a, halo_b, own, other, w_in, w_out, w_step, taps_in, taps_out, offsets, rates,
    stride, added, rows, in_t, out_maps, mixing, step_wide, end_wide, reach_wide, total,
    *, heads,
):
    part = own.shape[0]
    length = 2 * part
    rows[:HALO, :] = halo_a[...] + halo_b[...]
    mine = pl.multiple_of(HALO + side[0] * part, HALO)
    others = pl.multiple_of(HALO + (1 - side[0]) * part, HALO)
    rows[pl.ds(mine, part), :] = own[...]
    rows[pl.ds(others, part), :] = other[...]
    out_m = conv_silu(rounded_dot(rows[...], w_out[...]), taps_out[...]).astype(BF16)
    out_maps[...] = out_m
    in_m = conv_silu(rounded_dot(rows[...], w_in[...]), taps_in[...]).astype(BF16)
    in_tr = in_m.astype(F32).T.astype(BF16)
    in_t[...] = in_tr
    raw = rounded_dot(rows[HALO:, :], w_step[...]) + offsets[...]
    step = jnp.maximum(raw, 0.0) + jnp.log1p(jnp.exp(-jnp.abs(raw)))
    cum = -rates[...] * step * stride[...] + added[...]
    row = lax.broadcasted_iota(jnp.int32, cum.shape, 0)
    shift = 1
    while shift < length:
        cum = cum + jnp.where(row >= shift, pltpu.roll(cum, shift, 0), 0.0)
        shift *= 2
    last = cum[length - 1 : length, :]
    total[...] = jnp.broadcast_to(last[None], total.shape)
    to_end = step * jnp.exp(last - cum)
    reach = jnp.exp(cum)
    lane = lax.broadcasted_iota(jnp.int32, (length, LANES), 1)
    for pair in range(heads // 2):
        at = slice(pair * LANES, (pair + 1) * LANES)
        step_wide[:, at] = per_head(step, pair, lane)
        end_wide[:, at] = per_head(to_end, pair, lane)
        reach_wide[:, at] = per_head(reach, pair, lane)
    cum_t = cum.T
    lower = lax.broadcasted_iota(jnp.int32, (LANES, LANES), 0) >= lax.broadcasted_iota(
        jnp.int32, (LANES, LANES), 1
    )
    for i in range(length // LANES):
        to = slice(i * LANES, (i + 1) * LANES)
        for j in range(i + 1):
            frm = slice(j * LANES, (j + 1) * LANES)
            inter = jnp.dot(out_m[to, :], in_tr[:, frm], preferred_element_type=F32)
            for h in range(heads):
                gap = cum[to, h : h + 1] - cum_t[h : h + 1, frm]
                if i == j:
                    gap = jnp.where(lower, gap, -jnp.inf)
                mixing[h, to, frm] = (inter * jnp.exp(gap)).astype(BF16)


def gathered(w):
    return jnp.concatenate([w[d] for d in range(w.shape[0])], axis=0)


def source_kernel(
    side, rows, w_x, taps, step_wide, end_wide, in_t, factors, xs_out, scaled_out, states
):
    xs = conv_silu(rounded_dot(rows[...], gathered(w_x)), taps[...]).astype(BF16)
    xs_out[...] = xs
    xs = xs.astype(F32)
    scaled_out[...] = (xs * step_wide[...]).astype(BF16)
    weighted = (xs * end_wide[...]).astype(BF16)
    states[...] = jnp.dot(in_t[...], weighted, preferred_element_type=F32).astype(BF16)


def inner_kernel(mixing, scaled, xs, skip, base):
    length = scaled.shape[0]
    lane = lax.broadcasted_iota(jnp.int32, (LANES, LANES), 1)
    for pair in range(scaled.shape[1] // LANES):
        at = slice(pair * LANES, (pair + 1) * LANES)
        for i in range(length // LANES):
            to = slice(i * LANES, (i + 1) * LANES)
            seen = (i + 1) * LANES
            both = scaled[:seen, at]
            first = jnp.dot(mixing[2 * pair, to, :seen], both, preferred_element_type=F32)
            second = jnp.dot(mixing[2 * pair + 1, to, :seen], both, preferred_element_type=F32)
            base[to, at] = jnp.where(lane < P_SIZE, first, second) + skip[:, at] * xs[
                to, at
            ].astype(F32)


def scan_kernel(states, factors, carried):
    count = factors.shape[0]
    rows = states.shape[0] // count
    acc = jnp.zeros((rows, states.shape[1]), F32)
    for k in range(count):
        at = slice(k * rows, (k + 1) * rows)
        carried[at, :] = acc.astype(BF16)
        acc = acc * factors[k : k + 1, :] + states[at, :].astype(F32)


def gate_kernel(rows, w_z, gate):
    gate[...] = silu(rounded_dot(rows[HALO:, :], gathered(w_z)))


def blend_kernel(side, out_maps, carried, reach_wide, base, gate, gain, kept, sent, normed):
    part = kept.shape[0]
    reached = jnp.dot(out_maps[...], carried[...], preferred_element_type=F32)
    mixed = (base[...] + reached * reach_wide[...]).astype(BF16).astype(F32)
    gated = mixed * gate[...]
    mean = jnp.mean(gated * gated, axis=1, keepdims=True)
    normed[...] = (gated * lax.rsqrt(mean + EPSILON) * gain[...]).astype(BF16)
    kept[...] = normed[pl.ds(pl.multiple_of(side[0] * part, HALO), part), :]
    sent[...] = normed[pl.ds(pl.multiple_of((1 - side[0]) * part, HALO), part), :]


def output_kernel(side, kept, arrived, w_o, output, w, normed, out, sem_in, sem_out, *, parts):
    count = w_o.shape[0] // parts
    width = kept.shape[1]
    cols = count * LANES
    copies = [
        pltpu.make_async_copy(
            w_o.at[pl.ds(p * count, count)], w.at[pl.ds(p * count, count)], sem_in.at[p]
        )
        for p in range(parts)
    ]
    for c in copies:
        c.start()
    normed[:, pl.ds(pl.multiple_of(side[0] * width, LANES), width)] = kept[...]
    normed[:, pl.ds(pl.multiple_of((1 - side[0]) * width, LANES), width)] = arrived[...]
    outs = []
    for p in range(parts):
        copies[p].wait()
        block = jnp.concatenate([w[d] for d in range(p * count, (p + 1) * count)], axis=1)
        at = pl.ds(p * cols, cols)
        out[:, at] = jnp.dot(normed[...], block, preferred_element_type=F32).astype(BF16)
        outs.append(pltpu.make_async_copy(out.at[:, at], output.at[:, at], sem_out.at[p]))
        outs[-1].start()
    for c in outs:
        c.wait()


def shape(dims, kind=F32):
    return jax.ShapeDtypeStruct(dims, kind)


def block(dims, index):
    return pl.BlockSpec(dims, index)


def whole(dims):
    return pl.BlockSpec(dims, lambda *_: (0,) * len(dims))


def call(kernel, outs, *args, name, flops, ins, out_blocks, grid=(1,), scalars=0, scratch=()):
    return pl.pallas_call(
        kernel,
        out_shape=outs,
        name=name,
        grid_spec=pltpu.PrefetchScalarGridSpec(
            num_scalar_prefetch=scalars,
            grid=grid,
            in_specs=ins,
            out_specs=out_blocks,
            scratch_shapes=scratch,
        ),
        cost_estimate=pl.CostEstimate(flops=flops, transcendentals=0, bytes_accessed=0),
    )(*args)


def shards(
    mixer_source_array,
    source_projection,
    gating_projection,
    entry_mapping_projection,
    readout_mapping_projection,
    increment_projection,
    source_conv_taps,
    entry_mapping_taps,
    readout_mapping_taps,
    increment_offsets,
    channel_damping_rate,
    bypass_coefficients,
    stride_multiplier,
    added_log_damping,
    norm_scale_factor,
    final_projection,
):
    own = mixer_source_array[0]
    part, d_model = own.shape
    length = 2 * part
    k_rows = source_projection.shape[0]
    width = source_projection.shape[1] // G
    heads = width // P_SIZE
    sp = lax.axis_size("sp")
    dp = lax.axis_size("dp")
    me = lax.axis_index("sp")
    blocks = sp // 2
    side_index = me % 2
    side = side_index.astype(jnp.int32)[None]
    ranks = [list(range(0, sp, 2)), list(range(1, sp, 2))]
    swap = [(i, i ^ 1) for i in range(sp)]

    picked = call(
        pick_kernel,
        shape((2 * k_rows, width), BF16),
        side,
        source_projection,
        gating_projection,
        name="pick",
        flops=0,
        scalars=1,
        ins=[block((k_rows, width), lambda i, s: (0, s[0]))] * 2,
        out_blocks=whole((2 * k_rows, width)),
    )
    w_xz = lax.all_gather(picked, "dp", axis=0, tiled=False)
    w_o = lax.all_gather(final_projection, "dp", axis=0, tiled=False)

    other = lax.ppermute(own, "sp", swap)
    edge = own[part - HALO :]
    halo_a = lax.ppermute(edge, "sp", [(i, i + 1) for i in range(1, sp - 1, 2)])
    halo_b = lax.ppermute(edge, "sp", [(i, i + 2) for i in range(1, sp - 2, 2)])

    pad = LANES - heads
    first = (me // 2) * length
    head0 = side_index * heads
    zero = jnp.zeros_like(head0)
    w_step = jnp.pad(
        lax.dynamic_slice(increment_projection, (zero, head0), (d_model, heads)), ((0, 0), (0, pad))
    )
    stride = lax.dynamic_slice_in_dim(stride_multiplier[0], first, length, 0)[:, None]
    added = jnp.pad(
        lax.dynamic_slice(added_log_damping[0], (first, head0), (length, heads)), ((0, 0), (0, pad))
    )
    offsets = jnp.pad(lax.dynamic_slice_in_dim(increment_offsets, head0, heads, 0), (0, pad))[None]
    rates = jnp.pad(lax.dynamic_slice_in_dim(channel_damping_rate, head0, heads, 0), (0, pad))[None]

    wide = (length, width)
    out_shapes = (
        shape((HALO + length, d_model), BF16),
        shape((N, length), BF16),
        shape((length, N), BF16),
        shape((heads, length, length), BF16),
        shape(wide),
        shape(wide),
        shape(wide),
        shape((blocks, 8, LANES)),
    )
    rows, in_t, out_maps, mixing, step_wide, end_wide, reach_wide, total = call(
        functools.partial(maps_kernel, heads=heads),
        out_shapes,
        side,
        halo_a,
        halo_b,
        own,
        other,
        entry_mapping_projection,
        readout_mapping_projection,
        w_step,
        entry_mapping_taps,
        readout_mapping_taps,
        offsets,
        rates,
        stride,
        added,
        name="maps",
        flops=2 * length * d_model * LANES * 20,
        scalars=1,
        ins=[
            whole((HALO, d_model)),
            whole((HALO, d_model)),
            whole(own.shape),
            whole(own.shape),
            block((d_model, N), lambda i, s: (0, s[0])),
            block((d_model, N), lambda i, s: (0, s[0])),
            whole((d_model, LANES)),
            block((CONV_W, N), lambda i, s: (0, s[0])),
            block((CONV_W, N), lambda i, s: (0, s[0])),
            whole((1, LANES)),
            whole((1, LANES)),
            whole((length, 1)),
            whole((length, LANES)),
        ],
        out_blocks=[whole(o.shape) for o in out_shapes],
    )
    totals = lax.all_to_all(
        total, "sp", split_axis=0, concat_axis=0, tiled=True, axis_index_groups=ranks
    )
    factors = jnp.repeat(jnp.exp(totals[:, 0, :heads]), P_SIZE, axis=1)

    cols = 256
    steps = width // cols
    xs, scaled, states = call(
        source_kernel,
        (shape(wide, BF16), shape(wide, BF16), shape((N, width), BF16)),
        side,
        rows,
        w_xz,
        source_conv_taps,
        step_wide,
        end_wide,
        in_t,
        factors,
        name="source",
        flops=2 * length * d_model * width,
        grid=(steps,),
        scalars=1,
        ins=[
            whole(rows.shape),
            block((dp, k_rows, cols), lambda c, s: (0, 0, c)),
            block((CONV_W, cols), lambda c, s: (0, s[0] * steps + c)),
            block((length, cols), lambda c, s: (0, c)),
            block((length, cols), lambda c, s: (0, c)),
            whole(in_t.shape),
            whole(factors.shape),
        ],
        out_blocks=[
            block((length, cols), lambda c, s: (0, c)),
            block((length, cols), lambda c, s: (0, c)),
            block((N, cols), lambda c, s: (0, c)),
        ],
    )
    arrived = lax.all_to_all(
        states, "sp", split_axis=0, concat_axis=0, tiled=True, axis_index_groups=ranks
    )
    gate = call(
        gate_kernel,
        shape(wide),
        rows,
        w_xz,
        name="gate",
        flops=2 * length * d_model * width,
        grid=(steps,),
        ins=[whole(rows.shape), block((dp, k_rows, cols), lambda c: (0, 1, c))],
        out_blocks=block((length, cols), lambda c: (0, c)),
    )
    skip_wide = jnp.repeat(
        lax.dynamic_slice_in_dim(bypass_coefficients, head0, heads, 0), P_SIZE
    )[None]
    base = call(
        inner_kernel,
        shape(wide),
        mixing,
        scaled,
        xs,
        skip_wide,
        name="inner",
        flops=2 * length * d_model * width,
        ins=[whole(mixing.shape), whole(wide), whole(wide), whole((1, width))],
        out_blocks=whole(wide),
    )
    own_carried = call(
        scan_kernel,
        shape(arrived.shape, BF16),
        arrived,
        factors,
        name="scan",
        flops=1000,
        ins=[whole(arrived.shape), whole(factors.shape)],
        out_blocks=whole(arrived.shape),
    )
    carried = lax.all_to_all(
        own_carried, "sp", split_axis=0, concat_axis=0, tiled=True, axis_index_groups=ranks
    )
    kept, sent = call(
        blend_kernel,
        (shape((part, width), BF16), shape((part, width), BF16)),
        side,
        out_maps,
        carried,
        reach_wide,
        base,
        gate,
        norm_scale_factor[None],
        name="blend",
        flops=2 * length * N * width,
        scalars=1,
        ins=[
            whole((length, N)),
            whole((N, width)),
            whole(wide),
            whole(wide),
            whole(wide),
            block((1, width), lambda i, s: (0, s[0])),
        ],
        out_blocks=[whole((part, width)), whole((part, width))],
        scratch=[pltpu.VMEM(wide, BF16)],
    )
    arrived_half = lax.ppermute(sent, "sp", swap)
    parts = 4
    any_space = pl.BlockSpec(memory_space=pl.ANY)
    out_dims = (part, dp * final_projection.shape[1])
    output = call(
        functools.partial(output_kernel, parts=parts),
        shape(out_dims, BF16),
        side,
        kept,
        arrived_half,
        w_o,
        name="output",
        flops=4 * part * width * d_model,
        scalars=1,
        ins=[whole((part, width)), whole((part, width)), any_space],
        out_blocks=any_space,
        scratch=[
            pltpu.VMEM(w_o.shape, BF16),
            pltpu.VMEM((part, G * width), BF16),
            pltpu.VMEM(out_dims, BF16),
            pltpu.SemaphoreType.DMA((parts,)),
            pltpu.SemaphoreType.DMA((parts,)),
        ],
    )
    return output[None]


def solution(mesh):
    return jax.shard_map(
        shards,
        mesh=mesh,
        in_specs=(
            P(("grp", "dp"), "sp", None),
            P("dp", None),
            P("dp", None),
            P(),
            P(),
            P(),
            P(),
            P(),
            P(),
            P(),
            P(),
            P(),
            P(("grp", "dp"), None),
            P(("grp", "dp"), None, None),
            P(),
            P(None, "dp"),
        ),
        out_specs=P(("grp", "dp"), "sp", None),
        check_vma=False,
    )
```

time: 178 us -> 169 us (0.949)
  the two profiles are of different devices: /device:TPU:65 before, /device:TPU:66 now
where the time goes in v3:
time: 169 us; the launch traced here: 168 us
  blocking collectives  77.9 us (46%)
  Pallas kernels  30.4 us (18%)
  waiting for transfers between devices  21.1 us (12%)
  starting transfers between devices  13.9 us (8%)
  between operations  13.6 us (8%)
  local copies, waits for them, and re-layouts  11 us (7%)
    all_to_all x1, blocking collectives, shards(): lax.all_to_all(total, 'sp', split_axis=0, concat_axis=0, tiled=True, axis...  54.5 us
    pallas_call x8, Pallas kernels, call(): pl.pallas_call(kernel, out_shape=outs, name=name, grid_spec=pltpu.Prefetc...  30.4 us
    all_to_all x1, blocking collectives, shards(): lax.all_to_all(states, 'sp', split_axis=0, concat_axis=0, tiled=True, axi...  23.4 us
    ppermute x1, waiting for transfers between devices, shards(): other = lax.ppermute(own, 'sp', swap)  9.2 us
    all_to_all x1, waiting for transfers between devices, shards(): lax.all_to_all(own_carried, 'sp', split_axis=0, concat_axis=0, tiled=True...  6.26 us
    ppermute x1, starting transfers between devices, shards(): other = lax.ppermute(own, 'sp', swap)  6.03 us
    ppermute x1, waiting for transfers between devices, shards(): arrived_half = lax.ppermute(sent, 'sp', swap)  4.83 us
    all_to_all x1, starting transfers between devices, shards(): lax.all_to_all(own_carried, 'sp', split_axis=0, concat_axis=0, tiled=True...  3.57 us
  transfers between devices with their start and end apart: 7, of which 3 were waited for; matrix products, arithmetic and copies ran while one was open for 5% of the time, Pallas kernels for 14%

profile of v3, /device:TPU:66, one launch (start us, length us, event | category | flops | bytes accessed | tf_op | source)
XLA Modules:
  0.0 167.9 jit_solution(7996148070729628447)
XLA Ops:
  6.5 0.0 copy-start
  6.6 0.0 all-gather.5.cloned.1.call-start
  6.6 1.7 %pick.1 = bf16[256,512]{1,0:T(8,128)(2,1)} custom-call(s32[1]{0:T(128)} %bitcast.side, bf16[128,1024]{1,0:T(8,128)(2,1)} %w_x.1, bf16[128,1024]{1,0:T(8,128)(2,1)} %w_z.1), custom_call_target="tpu_custom_call" | custom-call | tf_op jit(solution)/shard_map/pick/pallas_call | solution.py:196
  8.3 0.1 all-gather.5.cloned.1.call-update
  8.3 0.1 all-gather.7.cloned.1.call-start
  8.4 0.7 all-gather.7.cloned.1.call-update
  9.2 6.0 %collective-permute-start.2 = (bf16[192,2048]{1,0:T(8,128)(2,1)}, bf16[192,2048]{1,0:T(8,128)(2,1)S(1)}, u32[]{:S(2)}, u32[]{:S(2)}) collective-permute-start(bf16[192,2048]{1,0:T(8,128)(2,1)} %bitcast.29), channel_id=1, source_target_pairs={{0,16},{16,0},{32,48},{48,32},{64,80},{80,64},{96,112},{112,96},{1... | collective-permute-start | bytes 2359304 | tf_op jit(solution)/shard_map/ppermute | solution.py:259
  15.2 0.9 slice_bitcast_fusion
  16.0 0.7 collective-permute-start
  16.7 0.7 collective-permute-start.1
  17.4 0.8 constant_dynamic-slice_fusion.1
  18.2 0.3 copy.22
  18.5 0.0 copy-done
  18.5 0.1 copy.20
  18.6 0.7 dynamic-slice_bitcast_fusion
  19.3 0.8 copy.21.stride
  20.1 0.7 dynamic_slice.21
  20.9 0.7 dynamic_slice.22
  21.6 0.9 pad.15.w_step
  22.5 0.7 pad.18.added
  23.2 0.6 pad_bitcast_fusion
  23.8 0.0 collective-permute-done.halo_a
  23.8 0.0 collective-permute-done.1.halo_b
  23.8 0.0 copy-start.5
  23.8 9.2 %collective-permute-done.2.other = bf16[192,2048]{1,0:T(8,128)(2,1)S(1)} collective-permute-done((bf16[192,2048]{1,0:T(8,128)(2,1)}, bf16[192,2048]{1,0:T(8,128)(2,1)S(1)}, u32[]{:S(2)}, u32[]{:S(2)}) %collective-permute-start.2) | collective-permute-done | bytes 786464 | tf_op jit(solution)/shard_map/ppermute | solution.py:259
  33.0 0.0 copy-done.4
  33.0 0.9 copy-done.3
  33.9 7.7 %maps.1 = (bf16[400,2048]{1,0:T(8,128)(2,1)}, bf16[128,384]{1,0:T(8,128)(2,1)}, bf16[384,128]{1,0:T(8,128)(2,1)}, bf16[8,384,384]{2,1,0:T(8,128)(2,1)}, f32[384,...) custom-call(s32[1]{0:T(128)} %bitcast.side, bf16[16,2048]{1,0:T(8,128)(2,1)} %copy-done.4, ...), custom_call_target="tpu_custom_call" | custom-call | flops 4026531840 | tf_op jit(solution)/shard_map/maps/pallas_call | solution.py:196
  41.5 54.5 %all_to_all.27 = f32[8,8,128]{2,1,0:T(8,128)S(1)} all-to-all(f32[8,8,128]{2,1,0:T(8,128)} %get-tuple-element.23), channel_id=1, replica_groups={{0,32,64,96,128,160,192,224},{16,48,80,112,144,176,208,240},{1,33,65,97..., dimensions={0} | all-to-all | bytes 65536 | tf_op jit(solution)/shard_map/all_to_all | solution.py:326
  96.1 0.1 broadcast_in_dim.28
  96.2 0.7 reshape.12.factors
  96.8 4.9 %source.1 = (bf16[384,512]{1,0:T(8,128)(2,1)}, bf16[384,512]{1,0:T(8,128)(2,1)}, bf16[128,512]{1,0:T(8,128)(2,1)}) custom-call(s32[1]{0:T(128)} %bitcast.side, bf16[400,2048]{1,0:T(8,128)(2,1)} %get-tuple-element.19.rows, bf16[16,256,512]{2,1,0:T(8,128)(2,1)} %bitcast.20, f32[4,1024]{1,0:T(4,128)} %taps.1, f32[384,512]{1,0:T(8,128)} %get-tuple-element.20.step_wide, ...), custom_call_target="tpu_custom_call" | custom-call | flops 805306368 | tf_op jit(solution)/shard_map/source/pallas_call | solution.py:196
  101.7 23.4 %all_to_all.28 = bf16[8,16,512]{2,1,0:T(8,128)(2,1)} all-to-all(bf16[8,16,512]{2,1,0:T(8,128)(2,1)} %bitcast.27), channel_id=1, replica_groups={{0,32,64,96,128,160,192,224},{16,48,80,112,144,176,208,240},{1,33,65,97..., dimensions={0} | all-to-all | bytes 262144 | tf_op jit(solution)/shard_map/all_to_all | solution.py:363
  125.1 1.6 scan.1
  126.7 3.6 %all-to-all-start.2 = ((bf16[8,16,512]{2,1,0:T(8,128)(2,1)}), bf16[8,16,512]{2,1,0:T(8,128)(2,1)S(1)}, u32[]{:S(2)}, u32[]{:S(2)}) async-start(bf16[8,16,512]{2,1,0:T(8,128)(2,1)} %bitcast.25), calls=%async_computation.2 | async-start | bytes 262144 | tf_op jit(solution)/shard_map/all_to_all | solution.py:402
  130.3 0.1 dynamic_slice.26
  130.4 0.1 broadcast_in_dim.29
  130.5 0.6 broadcast_in_dim_reshape.3.skip
  131.1 3.8 %gate.1 = f32[384,512]{1,0:T(8,128)} custom-call(bf16[400,2048]{1,0:T(8,128)(2,1)} %get-tuple-element.19.rows, bf16[16,256,512]{2,1,0:T(8,128)(2,1)} %bitcast.21), custom_call_target="tpu_custom_call" | custom-call | flops 805306368 | tf_op jit(solution)/shard_map/gate/pallas_call | solution.py:196
  134.9 3.3 %inner.1.base = f32[384,512]{1,0:T(8,128)} custom-call(bf16[8,384,384]{2,1,0:T(8,128)(2,1)} %get-tuple-element.26.mixing, bf16[384,512]{1,0:T(8,128)(2,1)} %get-tuple-element.27.scaled, bf16[384,512]{1,0:T(8,128)(2,1)} %get-tuple-element.28.xs, f32[1,512]{1,0:T(1,128)} %broadcast_in_dim_reshape.3.skip), custom_call_target="tpu_custom_call" | custom-call | flops 805306368 | tf_op jit(solution)/shard_map/inner/pallas_call | solution.py:196
  138.2 6.3 %all-to-all-done.2 = bf16[8,16,512]{2,1,0:T(8,128)(2,1)S(1)} async-done(((bf16[8,16,512]{2,1,0:T(8,128)(2,1)}), bf16[8,16,512]{2,1,0:T(8,128)(2,1)S(1)}, u32[]{:S(2)}, u32[]{:S(2)}) %all-to-all-start.2) | async-done | bytes 131104 | tf_op jit(solution)/shard_map/all_to_all | solution.py:402
  144.5 0.7 copy-done.1
  145.2 2.9 %blend.1 = (bf16[192,512]{1,0:T(8,128)(2,1)}, bf16[192,512]{1,0:T(8,128)(2,1)}) custom-call(s32[1]{0:T(128)} %bitcast.side, bf16[384,128]{1,0:T(8,128)(2,1)} %get-tuple-element.18.out_maps, bf16[128,512]{1,0:T(8,128)(2,1)} %bitcast.24, f32[384,512]{1,0:T(8,128)} %get-tuple-element.25.reach_wide, f32[384,512]{1,0:T(8,128)} %inner.1.base, f32[384,512]{1,0:T(8,128)} %gate.1, ...), custom_call_target="tpu_custom_call" | custom-call | flops 50331648 | tf_op jit(solution)/shard_map/blend/pallas_call | solution.py:196
  148.1 2.9 %collective-permute-start.3 = (bf16[192,512]{1,0:T(8,128)(2,1)}, bf16[192,512]{1,0:T(8,128)(2,1)S(1)}, u32[]{:S(2)}, u32[]{:S(2)}) collective-permute-start(bf16[192,512]{1,0:T(8,128)(2,1)} %get-tuple-element.30), channel_id=1, source_target_pairs={{0,16},{16,0},{32,48},{48,32},{64,80},{80,64},{96,112},{112,96},{1... | collective-permute-start | bytes 589832 | tf_op jit(solution)/shard_map/ppermute | solution.py:429
  151.0 0.0 all-gather.7.cloned.1.call-done
  151.0 4.8 %collective-permute-done.3.arrived = bf16[192,512]{1,0:T(8,128)(2,1)S(1)} collective-permute-done((bf16[192,512]{1,0:T(8,128)(2,1)}, bf16[192,512]{1,0:T(8,128)(2,1)S(1)}, u32[]{:S(2)}, u32[]{:S(2)}) %collective-permute-start.3) | collective-permute-done | bytes 196640 | tf_op jit(solution)/shard_map/ppermute | solution.py:429
  155.9 0.7 copy-done.2
  156.5 4.5 %output.1 = bf16[192,2048]{1,0:T(8,128)(2,1)} custom-call(s32[1]{0:T(128)} %bitcast.side, bf16[192,512]{1,0:T(8,128)(2,1)} %get-tuple-element.29.kept, bf16[192,512]{1,0:T(8,128)(2,1)} %copy-done.2, bf16[16,1024,128]{2,1,0:T(8,128)(2,1)} %bitcast.22), custom_call_target="tpu_custom_call" | custom-call | flops 805306368 | tf_op jit(solution)/shard_map/output/pallas_call | solution.py:196
  (10 shorter events, 0.0 us)
Async XLA Ops:
  6.5 11.9 %copy-start = (f32[1,3072,16]{1,2,0:T(8,128)S(1)}, f32[1,3072,16]{1,2,0:T(8,128)}, u32[]{:S(2)}) copy-start(f32[1,3072,16]{1,2,0:T(8,128)} %param.29) | copy-start | bytes 589828
  6.6 90.3 %all-gather.5.cloned.1.call-start = ((), (), s32[]{:S(2)}) async-start(), calls=%async_computation.3 | async-start | bytes 4456448 | tf_op jit(solution)/shard_map/all_gather | solution.py:256
  8.3 142.7 %all-gather.7.cloned.1.call-start = ((), (), s32[]{:S(2)}) async-start(), calls=%async_computation.4 | async-start | bytes 4456448 | tf_op jit(solution)/shard_map/all_gather | solution.py:257
  9.2 23.8 %collective-permute-start.2 = (bf16[192,2048]{1,0:T(8,128)(2,1)}, bf16[192,2048]{1,0:T(8,128)(2,1)S(1)}, u32[]{:S(2)}, u32[]{:S(2)}) collective-permute-start(bf16[192,2048]{1,0:T(8,128)(2,1)} %bitcast.29), channel_id=1, source_target_pairs={{0,16},{16,0},{32,48},{48,32},{64,80},{80,64},{96,112},{112,96},{1... | collective-permute-start | bytes 2359304 | tf_op jit(solution)/shard_map/ppermute | solution.py:259
  16.0 7.7 %collective-permute-start = (bf16[16,2048]{1,0:T(8,128)(2,1)S(1)}, bf16[16,2048]{1,0:T(8,128)(2,1)S(1)}, u32[]{:S(2)}, u32[]{:S(2)}) collective-permute-start(bf16[16,2048]{1,0:T(8,128)(2,1)S(1)} %slice_bitcast_fusion), channel_id=1, source_target_pairs={{16,32},{48,64},{80,96},{112,128},{144,160},{176,192},{208,224},{1... | collective-permute-start | bytes 196616 | tf_op jit(solution)/shard_map/ppermute | solution.py:261
  16.7 7.1 %collective-permute-start.1 = (bf16[16,2048]{1,0:T(8,128)(2,1)S(1)}, bf16[16,2048]{1,0:T(8,128)(2,1)S(1)}, u32[]{:S(2)}, u32[]{:S(2)}) collective-permute-start(bf16[16,2048]{1,0:T(8,128)(2,1)S(1)} %slice_bitcast_fusion), channel_id=1, source_target_pairs={{16,48},{48,80},{80,112},{112,144},{144,176},{176,208},{208,240},{... | collective-permute-start | bytes 196616 | tf_op jit(solution)/shard_map/ppermute | solution.py:262
  23.8 9.2 %copy-start.4 = (bf16[16,2048]{1,0:T(8,128)(2,1)}, bf16[16,2048]{1,0:T(8,128)(2,1)S(1)}, u32[]{:S(2)}) copy-start(bf16[16,2048]{1,0:T(8,128)(2,1)S(1)} %collective-permute-done.halo_a) | copy-start | bytes 196612
  23.8 9.2 %copy-start.5 = (bf16[16,2048]{1,0:T(8,128)(2,1)}, bf16[16,2048]{1,0:T(8,128)(2,1)S(1)}, u32[]{:S(2)}) copy-start(bf16[16,2048]{1,0:T(8,128)(2,1)S(1)} %collective-permute-done.1.halo_b) | copy-start | bytes 196612
  33.0 0.9 copy-start.3
  96.2 34.2 %copy-start.6 = (f32[16]{0:T(128)S(1)}, f32[16]{0:T(128)}, u32[]{:S(2)}) copy-start(f32[16]{0:T(128)} %param.27) | copy-start | bytes 196
  126.7 17.8 %all-to-all-start.2 = ((bf16[8,16,512]{2,1,0:T(8,128)(2,1)}), bf16[8,16,512]{2,1,0:T(8,128)(2,1)S(1)}, u32[]{:S(2)}, u32[]{:S(2)}) async-start(bf16[8,16,512]{2,1,0:T(8,128)(2,1)} %bitcast.25), calls=%async_computation.2 | async-start | bytes 262144 | tf_op jit(solution)/shard_map/all_to_all | solution.py:402
  144.5 0.7 copy-start.1
  148.1 7.8 %collective-permute-start.3 = (bf16[192,512]{1,0:T(8,128)(2,1)}, bf16[192,512]{1,0:T(8,128)(2,1)S(1)}, u32[]{:S(2)}, u32[]{:S(2)}) collective-permute-start(bf16[192,512]{1,0:T(8,128)(2,1)} %get-tuple-element.30), channel_id=1, source_target_pairs={{0,16},{16,0},{32,48},{48,32},{64,80},{80,64},{96,112},{112,96},{1... | collective-permute-start | bytes 589832 | tf_op jit(solution)/shard_map/ppermute | solution.py:429
  155.9 0.7 copy-start.2
Sparse Core Ops, SparseCore 0:
  9.5 81.6 all-gather.4
  93.4 47.0 all-gather.6

commit v4 on v3

v4 whole, which is shorter than its diff:
```python
import functools
import jax
import jax.numpy as jnp
from jax import lax
from jax.experimental import pallas as pl
from jax.experimental.pallas import tpu as pltpu
from jax.sharding import PartitionSpec as P

P_SIZE = 64
N = 128
G = 2
CONV_W = 4
HALO = 16
LANES = 128
EPSILON = 1e-06

F32 = jnp.float32
BF16 = jnp.bfloat16


def silu(x):
    return 0.5 * x * (1.0 + jnp.tanh(0.5 * x))


def rounded_dot(a, b):
    return jnp.dot(a, b, preferred_element_type=F32).astype(BF16).astype(F32)


def conv_silu(padded, taps):
    width = taps.shape[0]
    total = taps[0:1, :] * pltpu.roll(padded, width - 1, 0)[HALO:]
    for k in range(1, width):
        shifted = padded if k == width - 1 else pltpu.roll(padded, width - 1 - k, 0)
        total = total + taps[k : k + 1, :] * shifted[HALO:]
    return silu(total)


def per_head(values, pair, lane):
    return jnp.where(
        lane < P_SIZE, values[:, 2 * pair : 2 * pair + 1], values[:, 2 * pair + 1 : 2 * pair + 2]
    )


def pick_kernel(side, w_x, w_z, picked, sem):
    rows = w_x.shape[0]
    width = picked.shape[1]
    at = pl.ds(pl.multiple_of(side[0] * width, LANES), width)
    copies = [
        pltpu.make_async_copy(w.at[:, at], picked.at[pl.ds(k * rows, rows)], sem.at[k])
        for k, w in enumerate((w_x, w_z))
    ]
    for c in copies:
        c.start()
    for c in copies:
        c.wait()


def maps_kernel(
    side, halo_a, halo_b, own, other, w_in_all, w_out_all, w_step, taps_in, taps_out, offsets,
    rates, stride, added, rows, in_t, out_maps, mixing, step_wide, end_wide, reach_wide,
    w_in, w_out, sem, *, heads,
):
    part = own.shape[0]
    length = 2 * part
    group = pl.ds(pl.multiple_of(side[0] * N, LANES), N)
    copies = [
        pltpu.make_async_copy(src.at[:, group], dst, sem.at[k])
        for k, (src, dst) in enumerate(((w_out_all, w_out), (w_in_all, w_in)))
    ]
    for c in copies:
        c.start()
    rows[:HALO, :] = halo_a[...] + halo_b[...]
    mine = pl.multiple_of(HALO + side[0] * part, HALO)
    others = pl.multiple_of(HALO + (1 - side[0]) * part, HALO)
    rows[pl.ds(mine, part), :] = own[...]
    rows[pl.ds(others, part), :] = other[...]
    copies[0].wait()
    out_m = conv_silu(rounded_dot(rows[...], w_out[...]), taps_out[:, group]).astype(BF16)
    out_maps[...] = out_m
    copies[1].wait()
    in_m = conv_silu(rounded_dot(rows[...], w_in[...]), taps_in[:, group]).astype(BF16)
    in_tr = in_m.astype(F32).T.astype(BF16)
    in_t[...] = in_tr
    raw = rounded_dot(rows[HALO:, :], w_step[...]) + offsets[...]
    step = jnp.maximum(raw, 0.0) + jnp.log1p(jnp.exp(-jnp.abs(raw)))
    cum = -rates[...] * step * stride[...] + added[...]
    row = lax.broadcasted_iota(jnp.int32, cum.shape, 0)
    shift = 1
    while shift < length:
        cum = cum + jnp.where(row >= shift, pltpu.roll(cum, shift, 0), 0.0)
        shift *= 2
    last = cum[length - 1 : length, :]
    to_end = step * jnp.exp(last - cum)
    reach = jnp.exp(cum)
    lane = lax.broadcasted_iota(jnp.int32, (length, LANES), 1)
    for pair in range(heads // 2):
        at = slice(pair * LANES, (pair + 1) * LANES)
        step_wide[:, at] = per_head(step, pair, lane)
        end_wide[:, at] = per_head(to_end, pair, lane)
        reach_wide[:, at] = per_head(reach, pair, lane)
    cum_t = cum.T
    lower = lax.broadcasted_iota(jnp.int32, (LANES, LANES), 0) >= lax.broadcasted_iota(
        jnp.int32, (LANES, LANES), 1
    )
    for i in range(length // LANES):
        to = slice(i * LANES, (i + 1) * LANES)
        for j in range(i + 1):
            frm = slice(j * LANES, (j + 1) * LANES)
            inter = jnp.dot(out_m[to, :], in_tr[:, frm], preferred_element_type=F32)
            for h in range(heads):
                gap = cum[to, h : h + 1] - cum_t[h : h + 1, frm]
                if i == j:
                    gap = jnp.where(lower, gap, -jnp.inf)
                mixing[h, to, frm] = (inter * jnp.exp(gap)).astype(BF16)


def streamed_dot(rows, first, w_all, half, w, sem):
    parts = sem.shape[0]
    count = w_all.shape[0] // parts
    k_rows = w.shape[1]
    copies = [
        pltpu.make_async_copy(
            w_all.at[pl.ds(p * count, count), pl.ds(half * k_rows, k_rows)],
            w.at[pl.ds(p * count, count)],
            sem.at[p],
        )
        for p in range(parts)
    ]
    for c in copies:
        c.start()
    acc = None
    for p in range(parts):
        copies[p].wait()
        block = jnp.concatenate([w[d] for d in range(p * count, (p + 1) * count)], axis=0)
        lhs = rows[first:, p * count * k_rows : (p + 1) * count * k_rows]
        part = jnp.dot(lhs, block, preferred_element_type=F32)
        acc = part if acc is None else acc + part
    return acc.astype(BF16).astype(F32)


def source_kernel(
    side, rows, w_xz, taps, step_wide, end_wide, reach_wide, in_t, xs_out, scaled_out, states,
    w, sem,
):
    length, width = step_wide.shape
    raw = streamed_dot(rows, 0, w_xz, 0, w, sem)
    group = pl.ds(pl.multiple_of(side[0] * width, LANES), width)
    xs = conv_silu(raw, taps[:, group]).astype(BF16)
    xs_out[...] = xs
    xs = xs.astype(F32)
    weighted = (xs * end_wide[...]).astype(BF16)
    states[:, :width] = jnp.dot(in_t[...], weighted, preferred_element_type=F32).astype(BF16)
    rest = reach_wide[length - 1 : length, :]
    row = lax.broadcasted_iota(jnp.int32, (HALO, LANES), 0)
    pieces = jnp.zeros((HALO, LANES), F32)
    blocks = width // LANES
    for k in range(3):
        piece = rest.astype(BF16).astype(F32)
        rest = rest - piece
        for c in range(blocks):
            pieces = jnp.where(
                row == k * blocks + c, piece[:, c * LANES : (c + 1) * LANES], pieces
            )
    pieces = pieces.astype(BF16)
    for i in range(states.shape[0] // HALO):
        states[i * HALO : (i + 1) * HALO, width:] = pieces
    scaled_out[...] = (xs * step_wide[...]).astype(BF16)


def inner_kernel(mixing, scaled, xs, skip, base):
    length = scaled.shape[0]
    lane = lax.broadcasted_iota(jnp.int32, (LANES, LANES), 1)
    for pair in range(scaled.shape[1] // LANES):
        at = slice(pair * LANES, (pair + 1) * LANES)
        for i in range(length // LANES):
            to = slice(i * LANES, (i + 1) * LANES)
            seen = (i + 1) * LANES
            both = scaled[:seen, at]
            first = jnp.dot(mixing[2 * pair, to, :seen], both, preferred_element_type=F32)
            second = jnp.dot(mixing[2 * pair + 1, to, :seen], both, preferred_element_type=F32)
            base[to, at] = jnp.where(lane < P_SIZE, first, second) + skip[:, at] * xs[
                to, at
            ].astype(F32)


def scan_kernel(states, carried):
    rows = HALO
    width = carried.shape[1]
    blocks = width // LANES
    acc = jnp.zeros((rows, width), F32)
    for k in range(states.shape[0] // rows):
        at = slice(k * rows, (k + 1) * rows)
        carried[at, :] = acc.astype(BF16)
        pieces = states[at, width:].astype(F32)
        factor = jnp.concatenate(
            [
                pieces[c : c + 1] + pieces[blocks + c : blocks + c + 1]
                + pieces[2 * blocks + c : 2 * blocks + c + 1]
                for c in range(blocks)
            ],
            axis=1,
        )
        acc = acc * factor + states[at, :width].astype(F32)


def gate_kernel(rows, w_xz, gate, w, sem):
    gate[...] = silu(streamed_dot(rows, HALO, w_xz, 1, w, sem))


def blend_kernel(side, out_maps, carried, reach_wide, base, gate, gain, kept, sent, normed):
    part = kept.shape[0]
    reached = jnp.dot(out_maps[...], carried[...], preferred_element_type=F32)
    mixed = (base[...] + reached * reach_wide[...]).astype(BF16).astype(F32)
    gated = mixed * gate[...]
    mean = jnp.mean(gated * gated, axis=1, keepdims=True)
    own_gain = gain[:, pl.ds(pl.multiple_of(side[0] * base.shape[1], LANES), base.shape[1])]
    normed[...] = (gated * lax.rsqrt(mean + EPSILON) * own_gain).astype(BF16)
    sent[...] = normed[pl.ds(pl.multiple_of((1 - side[0]) * part, HALO), part), :]
    kept[...] = normed[pl.ds(pl.multiple_of(side[0] * part, HALO), part), :]


def joined(w, first, count):
    return jnp.concatenate([w[d] for d in range(first, first + count)], axis=1)


def own_half_kernel(side, kept, w_o, partial, w_other, w, sem):
    parts = sem.shape[0] - 1
    count = w_o.shape[0] // parts
    width = kept.shape[1]
    mine = pl.ds(pl.multiple_of(side[0] * width, LANES), width)
    others = pl.ds(pl.multiple_of((1 - side[0]) * width, LANES), width)
    copies = [
        pltpu.make_async_copy(
            w_o.at[pl.ds(p * count, count), mine], w.at[pl.ds(p * count, count)], sem.at[p]
        )
        for p in range(parts)
    ]
    copies.append(pltpu.make_async_copy(w_o.at[:, others], w_other, sem.at[parts]))
    for c in copies:
        c.start()
    for p in range(parts):
        copies[p].wait()
        at = slice(p * count * LANES, (p + 1) * count * LANES)
        partial[:, at] = jnp.dot(
            kept[...], joined(w, p * count, count), preferred_element_type=F32
        )
    copies[parts].wait()


def output_kernel(arrived, partial, w_other, output, out, sem):
    parts = sem.shape[0]
    count = w_other.shape[0] // parts
    outs = []
    for p in range(parts):
        at = pl.ds(p * count * LANES, count * LANES)
        half = jnp.dot(
            arrived[...], joined(w_other, p * count, count), preferred_element_type=F32
        )
        out[:, at] = (partial[:, at] + half).astype(BF16)
        outs.append(pltpu.make_async_copy(out.at[:, at], output.at[:, at], sem.at[p]))
        outs[-1].start()
    for c in outs:
        c.wait()


def shape(dims, kind=F32):
    return jax.ShapeDtypeStruct(dims, kind)


V = pl.BlockSpec(memory_space=pltpu.VMEM)
K = pl.BlockSpec(memory_space=pltpu.VMEM)
S = pl.BlockSpec(memory_space=pltpu.SMEM)
H = pl.BlockSpec(memory_space=pltpu.HBM)
MIB = 1 << 20


def held(dims, kind=F32):
    return pltpu.VMEM(dims, kind)


def call(kernel, outs, *args, name, flops, ins, out_blocks, scratch=(), limit=12):
    placed = [
        pltpu.with_memory_space_constraint(x, pltpu.HBM if spec is H else pltpu.VMEM)
        if spec is H or spec is K
        else x
        for x, spec in zip(args, ins, strict=True)
    ]
    return pl.pallas_call(
        kernel,
        out_shape=outs,
        name=name,
        in_specs=ins,
        out_specs=out_blocks,
        scratch_shapes=scratch,
        compiler_params=pltpu.CompilerParams(vmem_limit_bytes=limit * MIB),
        cost_estimate=pl.CostEstimate(flops=flops, transcendentals=0, bytes_accessed=4 * MIB),
    )(*placed)


def copies(count):
    return pltpu.SemaphoreType.DMA((count,))


def shards(
    mixer_source_array,
    source_projection,
    gating_projection,
    entry_mapping_projection,
    readout_mapping_projection,
    increment_projection,
    source_conv_taps,
    entry_mapping_taps,
    readout_mapping_taps,
    increment_offsets,
    channel_damping_rate,
    bypass_coefficients,
    stride_multiplier,
    added_log_damping,
    norm_scale_factor,
    final_projection,
):
    own = mixer_source_array[0]
    part, d_model = own.shape
    length = 2 * part
    k_rows = source_projection.shape[0]
    width = source_projection.shape[1] // G
    heads = width // P_SIZE
    sp = lax.axis_size("sp")
    dp = lax.axis_size("dp")
    me = lax.axis_index("sp")
    side_index = me % 2
    side = side_index.astype(jnp.int32)[None]
    ranks = [list(range(0, sp, 2)), list(range(1, sp, 2))]
    swap = [(i, i ^ 1) for i in range(sp)]

    picked = call(
        pick_kernel,
        shape((2 * k_rows, width), BF16),
        side,
        source_projection,
        gating_projection,
        name="pick",
        flops=0,
        ins=[S, H, H],
        out_blocks=H,
        scratch=[copies(2)],
    )
    w_xz = lax.all_gather(picked, "dp", axis=0, tiled=False)
    w_o = lax.all_gather(final_projection, "dp", axis=0, tiled=False)

    other = lax.ppermute(own, "sp", swap)
    edge = own[part - HALO :]
    halo_a = lax.ppermute(edge, "sp", [(i, i + 1) for i in range(1, sp - 1, 2)])
    halo_b = lax.ppermute(edge, "sp", [(i, i + 2) for i in range(1, sp - 2, 2)])

    pad = LANES - heads
    first = (me // 2) * length
    head0 = side_index * heads
    zero = jnp.zeros_like(head0)
    w_step = jnp.pad(
        lax.dynamic_slice(increment_projection, (zero, head0), (d_model, heads)), ((0, 0), (0, pad))
    )
    stride = lax.dynamic_slice_in_dim(stride_multiplier[0], first, length, 0)[:, None]
    added = jnp.pad(
        lax.dynamic_slice(added_log_damping[0], (first, head0), (length, heads)), ((0, 0), (0, pad))
    )
    offsets = jnp.pad(lax.dynamic_slice_in_dim(increment_offsets, head0, heads, 0), (0, pad))[None]
    rates = jnp.pad(lax.dynamic_slice_in_dim(channel_damping_rate, head0, heads, 0), (0, pad))[None]

    wide = (length, width)
    out_shapes = (
        held((HALO + length, d_model), BF16),
        held((N, length), BF16),
        held((length, N), BF16),
        held((heads, length, length), BF16),
        held(wide),
        held(wide),
        held(wide),
    )
    rows, in_t, out_maps, mixing, step_wide, end_wide, reach_wide = call(
        functools.partial(maps_kernel, heads=heads),
        out_shapes,
        side,
        halo_a,
        halo_b,
        own,
        other,
        entry_mapping_projection,
        readout_mapping_projection,
        w_step,
        entry_mapping_taps,
        readout_mapping_taps,
        offsets,
        rates,
        stride,
        added,
        name="maps",
        flops=2 * length * d_model * LANES * 20,
        ins=[S, V, V, V, V, H, H, V, V, V, V, V, V, V],
        out_blocks=[V] * 7,
        scratch=[pltpu.VMEM((d_model, N), BF16), pltpu.VMEM((d_model, N), BF16), copies(2)],
        limit=24,
    )

    w_half = pltpu.VMEM((dp, k_rows, width), BF16)
    xs, scaled, states = call(
        source_kernel,
        (held(wide, BF16), held(wide, BF16), shape((N, width + LANES), BF16)),
        side,
        rows,
        w_xz,
        source_conv_taps,
        step_wide,
        end_wide,
        reach_wide,
        in_t,
        name="source",
        flops=2 * length * d_model * width,
        ins=[S, K, H, V, K, K, K, K],
        out_blocks=[V, V, V],
        scratch=[w_half, copies(4)],
        limit=20,
    )
    arrived = lax.all_to_all(
        states, "sp", split_axis=0, concat_axis=0, tiled=True, axis_index_groups=ranks
    )
    gate = call(
        gate_kernel,
        held(wide),
        rows,
        w_xz,
        name="gate",
        flops=2 * length * d_model * width,
        ins=[K, H],
        out_blocks=V,
        scratch=[w_half, copies(4)],
    )
    skip_wide = jnp.repeat(
        lax.dynamic_slice_in_dim(bypass_coefficients, head0, heads, 0), P_SIZE
    )[None]
    base = call(
        inner_kernel,
        held(wide),
        mixing,
        scaled,
        xs,
        skip_wide,
        name="inner",
        flops=2 * length * d_model * width,
        ins=[K, K, K, V],
        out_blocks=V,
    )
    own_carried = call(
        scan_kernel,
        shape((N, width), BF16),
        arrived,
        name="scan",
        flops=1000,
        ins=[V],
        out_blocks=V,
    )
    carried = lax.all_to_all(
        own_carried, "sp", split_axis=0, concat_axis=0, tiled=True, axis_index_groups=ranks
    )
    kept, sent = call(
        blend_kernel,
        (held((part, width), BF16), shape((part, width), BF16)),
        side,
        out_maps,
        carried,
        reach_wide,
        base,
        gate,
        norm_scale_factor[None],
        name="blend",
        flops=2 * length * N * width,
        ins=[S, K, V, K, K, K, V],
        out_blocks=[V, V],
        scratch=[pltpu.VMEM(wide, BF16)],
    )
    arrived_half = lax.ppermute(sent, "sp", swap)
    out_dims = (part, dp * final_projection.shape[1])
    w_o_half = (dp, width, final_projection.shape[1])
    partial, w_other = call(
        own_half_kernel,
        (held(out_dims), held(w_o_half, BF16)),
        side,
        kept,
        w_o,
        name="own_half",
        flops=2 * part * width * d_model,
        ins=[S, K, H],
        out_blocks=[V, V],
        scratch=[pltpu.VMEM(w_o_half, BF16), copies(5)],
    )
    output = call(
        output_kernel,
        shape(out_dims, BF16),
        arrived_half,
        partial,
        w_other,
        name="output",
        flops=2 * part * width * d_model,
        ins=[V, K, K],
        out_blocks=H,
        scratch=[pltpu.VMEM(out_dims, BF16), copies(4)],
    )
    return output[None]


def solution(mesh):
    return jax.shard_map(
        shards,
        mesh=mesh,
        in_specs=(
            P(("grp", "dp"), "sp", None),
            P("dp", None),
            P("dp", None),
            P(),
            P(),
            P(),
            P(),
            P(),
            P(),
            P(),
            P(),
            P(),
            P(("grp", "dp"), None),
            P(("grp", "dp"), None, None),
            P(),
            P(None, "dp"),
        ),
        out_specs=P(("grp", "dp"), "sp", None),
        check_vma=False,
    )
```

time: 169 us -> 169 us (level)
  waiting for transfers between devices: 21.1 us -> 71.2 us
  blocking collectives: 77.9 us -> 29.9 us
  Pallas kernels: 30.4 us -> 24.8 us
  local copies, waits for them, and re-layouts: 11 us -> 16 us
    all_to_all x1 -> x0, blocking collectives: 54.5 us -> none  [shards(): lax.all_to_all(total, 'sp', split_axis=0, concat_axis=0, tiled=True, axis...]
    all_gather x1, waiting for transfers between devices: 0.01 us -> 43.7 us  [shards(): w_xz = lax.all_gather(picked, 'dp', axis=0, tiled=False)]
    unnamed x15 -> x53, local copies, waits for them, and re-layouts: 2.5 us -> 12.2 us
    all_to_all x1, blocking collectives: 23.4 us -> 29.9 us  [shards(): lax.all_to_all(states, 'sp', split_axis=0, concat_axis=0, tiled=True, axi...]
    all_to_all x1, waiting for transfers between devices: 6.26 us -> 12.1 us  [shards(): lax.all_to_all(own_carried, 'sp', split_axis=0, concat_axis=0, tiled=True...]
    pallas_call x8 -> x9, Pallas kernels: 30.4 us -> 24.8 us  [call(): pl.pallas_call(kernel, out_shape=outs, name=name, in_specs=ins, out_specs...]
    ppermute x1, waiting for transfers between devices: 9.2 us -> 11.2 us  [shards(): other = lax.ppermute(own, 'sp', swap)]
  transfers between devices with their start and end apart: 7 -> 7, of which waited for: 3 -> 4; matrix products, arithmetic and copies ran while one was open for 5% -> 2% of each run, Pallas kernels for 14% -> 9%
where the time goes in v4:
time: 169 us
  waiting for transfers between devices  71.2 us (42%)
  blocking collectives  29.9 us (18%)
  Pallas kernels  24.8 us (15%)
  local copies, waits for them, and re-layouts  16 us (9%)
  between operations  13.8 us (8%)
  starting transfers between devices  13 us (8%)
    all_gather x1, waiting for transfers between devices, shards(): w_xz = lax.all_gather(picked, 'dp', axis=0, tiled=False)  43.7 us
    all_to_all x1, blocking collectives, shards(): lax.all_to_all(states, 'sp', split_axis=0, concat_axis=0, tiled=True, axi...  29.9 us
    pallas_call x9, Pallas kernels, call(): pl.pallas_call(kernel, out_shape=outs, name=name, in_specs=ins, out_specs...  24.8 us
    unnamed x53, local copies, waits for them, and re-layouts  12.2 us
    all_to_all x1, waiting for transfers between devices, shards(): lax.all_to_all(own_carried, 'sp', split_axis=0, concat_axis=0, tiled=True...  12.1 us
    ppermute x1, waiting for transfers between devices, shards(): other = lax.ppermute(own, 'sp', swap)  11.2 us
    ppermute x1, starting transfers between devices, shards(): other = lax.ppermute(own, 'sp', swap)  6.03 us
    all_to_all x1, starting transfers between devices, shards(): lax.all_to_all(own_carried, 'sp', split_axis=0, concat_axis=0, tiled=True...  3.57 us
  transfers between devices with their start and end apart: 7, of which 4 were waited for; matrix products, arithmetic and copies ran while one was open for 2% of the time, Pallas kernels for 9%

profile of v4, /device:TPU:66, one launch (start us, length us, event | category | flops | bytes accessed | tf_op | source)
XLA Modules:
  0.0 168.7 jit_solution(3443289040222391809)
XLA Ops:
  6.6 0.1 all-gather.5.cloned.1.call-start
  6.6 9.1 %pick.1 = bf16[256,512]{1,0:T(8,128)(2,1)} custom-call(s32[1]{0:T(128)} %bitcast.side, bf16[128,1024]{1,0:T(8,128)(2,1)} %w_x.1, bf16[128,1024]{1,0:T(8,128)(2,1)} %w_z.1), custom_call_target="tpu_custom_call" | custom-call | bytes 4194304 | tf_op jit(solution)/shard_map/pick/pallas_call | solution.py:288
  15.7 0.1 all-gather.5.cloned.1.call-update
  15.8 0.1 all-gather.7.cloned.1.call-start
  15.8 0.7 all-gather.7.cloned.1.call-update
  16.6 6.0 %collective-permute-start.2 = (bf16[192,2048]{1,0:T(8,128)(2,1)}, bf16[192,2048]{1,0:T(8,128)(2,1)S(1)}, u32[]{:S(2)}, u32[]{:S(2)}) collective-permute-start(bf16[192,2048]{1,0:T(8,128)(2,1)} %bitcast.22), channel_id=1, source_target_pairs={{0,16},{16,0},{32,48},{48,32},{64,80},{80,64},{96,112},{112,96},{1... | collective-permute-start | bytes 2359304 | tf_op jit(solution)/shard_map/ppermute | solution.py:351
  22.6 0.9 slice_bitcast_fusion
  23.5 0.7 collective-permute-start
  24.1 0.7 collective-permute-start.1
  24.8 0.8 constant_dynamic-slice_fusion.1
  25.6 0.3 copy.22
  25.9 0.1 copy.20
  26.1 0.7 dynamic-slice_bitcast_fusion
  26.7 0.9 copy.21.stride
  27.6 0.1 dynamic_slice.21
  27.7 0.1 dynamic_slice.22
  27.8 0.1 pad.15.w_step
  27.9 0.6 copy-done.17
  28.5 0.6 copy-done.19
  29.2 11.2 %collective-permute-done.2.other = bf16[192,2048]{1,0:T(8,128)(2,1)S(1)} collective-permute-done((bf16[192,2048]{1,0:T(8,128)(2,1)}, bf16[192,2048]{1,0:T(8,128)(2,1)S(1)}, u32[]{:S(2)}, u32[]{:S(2)}) %collective-permute-start.2) | collective-permute-done | bytes 786464 | tf_op jit(solution)/shard_map/ppermute | solution.py:351
  40.4 0.9 copy-done.15
  41.3 0.9 copy-done.9
  42.2 1.1 copy-done.13
  43.4 1.1 copy-done.16
  44.5 0.8 copy-done.18
  45.4 0.8 copy-done.20
  46.2 4.8 %maps.1 = (bf16[400,2048]{1,0:T(8,128)(2,1)S(1)}, bf16[128,384]{1,0:T(8,128)(2,1)S(1)}, bf16[384,128]{1,0:T(8,128)(2,1)S(1)}, bf16[8,384,384]{2,1,0:T(8,128)(2,1...) custom-call(s32[1]{0:T(128)} %bitcast.side, bf16[16,2048]{1,0:T(8,128)(2,1)S(1)} %copy-done.18, ...), custom_call_target="tpu_custom_call" | custom-call | flops 4026531840 | bytes 4194304 | tf_op jit(solution)/shard_map/maps/pallas_call | solution.py:288
  51.0 1.4 copy-done.1
  52.4 0.9 copy-done.3
  53.3 0.6 copy-done.10
  53.9 43.7 %all-gather.5.cloned.1.call-done = bf16[4096,512]{1,0:T(8,128)(2,1)} async-done(((bf16[256,512]{1,0:T(8,128)(2,1)}), bf16[4096,512]{1,0:T(8,128)(2,1)}) %all-gather.5.cloned.1.call-update) | async-done | bytes 4194320 | tf_op jit(solution)/shard_map/all_gather | solution.py:348
  97.6 1.1 copy-done.4
  98.8 3.1 %source.1 = (bf16[384,512]{1,0:T(8,128)(2,1)S(1)}, bf16[384,512]{1,0:T(8,128)(2,1)S(1)}, bf16[128,640]{1,0:T(8,128)(2,1)S(1)}) custom-call(s32[1]{0:T(128)} %bitcast.side, bf16[400,2048]{1,0:T(8,128)(2,1)S(1)} %get-tuple-element.20.rows, bf16[16,256,512]{2,1,0:T(8,128)(2,1)} %bitcast.25, f32[4,1024]{1,0:T(4,128)S(1)} %copy-done.12, ...), custom_call_target="tpu_custom_call" | custom-call | flops 805306368 | bytes 4194304 | tf_op jit(solution)/shard_map/source/pallas_call | solution.py:288
  101.9 0.7 copy-done.7
  102.7 29.9 %all_to_all.22 = bf16[8,16,640]{2,1,0:T(8,128)(2,1)S(1)} all-to-all(bf16[8,16,640]{2,1,0:T(8,128)(2,1)S(1)} %bitcast.21), channel_id=1, replica_groups={{0,32,64,96,128,160,192,224},{16,48,80,112,144,176,208,240},{1,33,65,97..., dimensions={0} | all-to-all | bytes 327680 | tf_op jit(solution)/shard_map/all_to_all | solution.py:424
  132.6 0.7 scan.1
  133.3 3.6 %all-to-all-start.1 = ((bf16[8,16,512]{2,1,0:T(8,128)(2,1)}), bf16[8,16,512]{2,1,0:T(8,128)(2,1)S(1)}, u32[]{:S(2)}, u32[]{:S(2)}) async-start(bf16[8,16,512]{2,1,0:T(8,128)(2,1)} %bitcast.10), calls=%async_computation.1 | async-start | bytes 262144 | tf_op jit(solution)/shard_map/all_to_all | solution.py:462
  136.9 0.1 dynamic_slice.26
  137.0 0.1 broadcast_in_dim.25
  137.1 0.1 broadcast_in_dim_reshape.3.skip
  137.1 2.5 %gate.1 = f32[384,512]{1,0:T(8,128)S(1)} custom-call(bf16[400,2048]{1,0:T(8,128)(2,1)S(1)} %get-tuple-element.20.rows, bf16[16,256,512]{2,1,0:T(8,128)(2,1)} %bitcast.26), custom_call_target="tpu_custom_call" | custom-call | flops 805306368 | bytes 4194304 | tf_op jit(solution)/shard_map/gate/pallas_call | solution.py:288
  139.7 0.6 inner.1.base
  140.3 12.1 %all-to-all-done.1 = bf16[8,16,512]{2,1,0:T(8,128)(2,1)S(1)} async-done(((bf16[8,16,512]{2,1,0:T(8,128)(2,1)}), bf16[8,16,512]{2,1,0:T(8,128)(2,1)S(1)}, u32[]{:S(2)}, u32[]{:S(2)}) %all-to-all-start.1) | async-done | bytes 131104 | tf_op jit(solution)/shard_map/all_to_all | solution.py:462
  152.4 0.4 blend.1
  152.9 2.0 %collective-permute-start.3 = (bf16[192,512]{1,0:T(8,128)(2,1)S(1)}, bf16[192,512]{1,0:T(8,128)(2,1)S(1)}, u32[]{:S(2)}, u32[]{:S(2)}) collective-permute-start(bf16[192,512]{1,0:T(8,128)(2,1)S(1)} %get-tuple-element.29), channel_id=1, source_target_pairs={{0,16},{16,0},{32,48},{48,32},{64,80},{80,64},{96,112},{112,96},{1... | collective-permute-start | bytes 589832 | tf_op jit(solution)/shard_map/ppermute | solution.py:481
  154.8 2.3 %own_half.1 = (f32[192,2048]{1,0:T(8,128)S(1)}, bf16[16,512,128]{2,1,0:T(8,128)(2,1)S(1)}) custom-call(s32[1]{0:T(128)} %bitcast.side, bf16[192,512]{1,0:T(8,128)(2,1)S(1)} %get-tuple-element.30.kept, bf16[16,1024,128]{2,1,0:T(8,128)(2,1)} %bitcast.27), custom_call_target="tpu_custom_call" | custom-call | flops 402653184 | bytes 4194304 | tf_op jit(solution)/shard_map/own_half/pallas_call | solution.py:288
  157.1 3.3 %collective-permute-done.3.arrived = bf16[192,512]{1,0:T(8,128)(2,1)S(1)} collective-permute-done((bf16[192,512]{1,0:T(8,128)(2,1)S(1)}, bf16[192,512]{1,0:T(8,128)(2,1)S(1)}, u32[]{:S(2)}, u32[]{:S(2)}) %collective-permute-start.3) | collective-permute-done | bytes 196640 | tf_op jit(solution)/shard_map/ppermute | solution.py:481
  160.5 1.3 output.1
  (45 shorter events, 0.1 us)
Async XLA Ops:
  6.5 19.3 %copy-start = (f32[1,3072,16]{1,2,0:T(8,128)S(1)}, f32[1,3072,16]{1,2,0:T(8,128)}, u32[]{:S(2)}) copy-start(f32[1,3072,16]{1,2,0:T(8,128)} %param.29) | copy-start | bytes 589828
  6.6 21.1 %copy-start.23 = (f32[16]{0:T(128)S(1)}, f32[16]{0:T(128)}, u32[]{:S(2)}) copy-start(f32[16]{0:T(128)} %param.25) | copy-start | bytes 196
  6.6 21.1 %copy-start.24 = (f32[16]{0:T(128)S(1)}, f32[16]{0:T(128)}, u32[]{:S(2)}) copy-start(f32[16]{0:T(128)} %param.26) | copy-start | bytes 196
  6.6 34.8 %copy-start.21 = (f32[4,256]{1,0:T(4,128)S(1)}, f32[4,256]{1,0:T(4,128)}, u32[]{:S(2)}) copy-start(f32[4,256]{1,0:T(4,128)} %taps_in.1) | copy-start | bytes 12292
  6.6 34.8 %copy-start.22 = (f32[4,256]{1,0:T(4,128)S(1)}, f32[4,256]{1,0:T(4,128)}, u32[]{:S(2)}) copy-start(f32[4,256]{1,0:T(4,128)} %taps_out.1) | copy-start | bytes 12292
  6.6 91.1 %all-gather.5.cloned.1.call-start = ((), (), s32[]{:S(2)}) async-start(), calls=%async_computation.2 | async-start | bytes 4456448 | tf_op jit(solution)/shard_map/all_gather | solution.py:348
  15.8 139.1 %all-gather.7.cloned.1.call-start = ((), (), s32[]{:S(2)}) async-start(), calls=%async_computation.3 | async-start | bytes 4456448 | tf_op jit(solution)/shard_map/all_gather | solution.py:349
  16.6 23.8 %collective-permute-start.2 = (bf16[192,2048]{1,0:T(8,128)(2,1)}, bf16[192,2048]{1,0:T(8,128)(2,1)S(1)}, u32[]{:S(2)}, u32[]{:S(2)}) collective-permute-start(bf16[192,2048]{1,0:T(8,128)(2,1)} %bitcast.22), channel_id=1, source_target_pairs={{0,16},{16,0},{32,48},{48,32},{64,80},{80,64},{96,112},{112,96},{1... | collective-permute-start | bytes 2359304 | tf_op jit(solution)/shard_map/ppermute | solution.py:351
  23.5 4.4 %collective-permute-start = (bf16[16,2048]{1,0:T(8,128)(2,1)S(1)}, bf16[16,2048]{1,0:T(8,128)(2,1)S(1)}, u32[]{:S(2)}, u32[]{:S(2)}) collective-permute-start(bf16[16,2048]{1,0:T(8,128)(2,1)S(1)} %slice_bitcast_fusion), channel_id=1, source_target_pairs={{16,32},{48,64},{80,96},{112,128},{144,160},{176,192},{208,224},{1... | collective-permute-start | bytes 196616 | tf_op jit(solution)/shard_map/ppermute | solution.py:353
  24.1 4.4 %collective-permute-start.1 = (bf16[16,2048]{1,0:T(8,128)(2,1)S(1)}, bf16[16,2048]{1,0:T(8,128)(2,1)S(1)}, u32[]{:S(2)}, u32[]{:S(2)}) collective-permute-start(bf16[16,2048]{1,0:T(8,128)(2,1)S(1)} %slice_bitcast_fusion), channel_id=1, source_target_pairs={{16,48},{48,80},{80,112},{112,144},{144,176},{176,208},{208,240},{... | collective-permute-start | bytes 196616 | tf_op jit(solution)/shard_map/ppermute | solution.py:354
  27.9 0.6 copy-start.17
  28.5 0.6 copy-start.19
  40.4 0.9 copy-start.15
  41.3 0.9 copy-start.9
  42.2 1.1 copy-start.13
  43.4 1.1 copy-start.16
  44.5 0.8 copy-start.18
  45.4 0.8 copy-start.20
  46.2 51.4 %copy-start.12 = (f32[4,1024]{1,0:T(4,128)S(1)}, f32[4,1024]{1,0:T(4,128)}, u32[]{:S(2)}) copy-start(f32[4,1024]{1,0:T(4,128)} %taps.1) | copy-start | bytes 49156
  51.0 1.4 copy-start.1
  52.4 0.9 copy-start.3
  53.3 0.6 copy-start.10
  97.6 1.1 copy-start.4
  98.8 38.1 %copy-start.25 = (f32[16]{0:T(128)S(1)}, f32[16]{0:T(128)}, u32[]{:S(2)}) copy-start(f32[16]{0:T(128)} %param.27) | copy-start | bytes 196
  101.9 0.7 copy-start.7
  102.7 30.7 %copy-start.5 = (bf16[384,512]{1,0:T(8,128)(2,1)}, bf16[384,512]{1,0:T(8,128)(2,1)S(1)}, u32[]{:S(2)}) copy-start(bf16[384,512]{1,0:T(8,128)(2,1)S(1)} %get-tuple-element.28.xs) | copy-start | bytes 1179652
  133.3 19.1 %all-to-all-start.1 = ((bf16[8,16,512]{2,1,0:T(8,128)(2,1)}), bf16[8,16,512]{2,1,0:T(8,128)(2,1)S(1)}, u32[]{:S(2)}, u32[]{:S(2)}) async-start(bf16[8,16,512]{2,1,0:T(8,128)(2,1)} %bitcast.10), calls=%async_computation.1 | async-start | bytes 262144 | tf_op jit(solution)/shard_map/all_to_all | solution.py:462
  137.1 2.6 %copy-start.2 = (bf16[8,384,384]{2,1,0:T(8,128)(2,1)S(1)}, bf16[8,384,384]{2,1,0:T(8,128)(2,1)}, u32[]{:S(2)}) copy-start(bf16[8,384,384]{2,1,0:T(8,128)(2,1)} %copy-done.1) | copy-start | bytes 7077892
  137.1 2.6 %copy-start.6 = (bf16[384,512]{1,0:T(8,128)(2,1)S(1)}, bf16[384,512]{1,0:T(8,128)(2,1)}, u32[]{:S(2)}) copy-start(bf16[384,512]{1,0:T(8,128)(2,1)} %copy-done.5) | copy-start | bytes 1179652
  137.1 2.6 %copy-start.8 = (bf16[384,512]{1,0:T(8,128)(2,1)S(1)}, bf16[384,512]{1,0:T(8,128)(2,1)}, u32[]{:S(2)}) copy-start(bf16[384,512]{1,0:T(8,128)(2,1)} %copy-done.7) | copy-start | bytes 1179652
  139.7 12.7 %copy-start.11 = (bf16[384,128]{1,0:T(8,128)(2,1)S(1)}, bf16[384,128]{1,0:T(8,128)(2,1)}, u32[]{:S(2)}) copy-start(bf16[384,128]{1,0:T(8,128)(2,1)} %copy-done.10) | copy-start | bytes 294916
  139.7 12.7 %copy-start.14 = (f32[1024]{0:T(1024)S(1)}, f32[1024]{0:T(1024)}, u32[]{:S(2)}) copy-start(f32[1024]{0:T(1024)} %param.30) | copy-start | bytes 12292
  152.9 7.6 %collective-permute-start.3 = (bf16[192,512]{1,0:T(8,128)(2,1)S(1)}, bf16[192,512]{1,0:T(8,128)(2,1)S(1)}, u32[]{:S(2)}, u32[]{:S(2)}) collective-permute-start(bf16[192,512]{1,0:T(8,128)(2,1)S(1)} %get-tuple-element.29), channel_id=1, source_target_pairs={{0,16},{16,0},{32,48},{48,32},{64,80},{80,64},{96,112},{112,96},{1... | collective-permute-start | bytes 589832 | tf_op jit(solution)/shard_map/ppermute | solution.py:481
Sparse Core Ops, SparseCore 0:
  15.9 81.6 all-gather.4
  99.8 47.0 all-gather.6

commit v5 on v4

--- a/solution.py
+++ b/solution.py
@@ -41,17 +41,23 @@
     )
 
 
-def pick_kernel(side, w_x, w_z, picked, sem):
-    rows = w_x.shape[0]
-    width = picked.shape[1]
+def pick_kernel(side, w_x, w_z, picked, x, z, sem):
+    rows, width = x.shape
     at = pl.ds(pl.multiple_of(side[0] * width, LANES), width)
-    copies = [
-        pltpu.make_async_copy(w.at[:, at], picked.at[pl.ds(k * rows, rows)], sem.at[k])
-        for k, w in enumerate((w_x, w_z))
+    arrive = [
+        pltpu.make_async_copy(w.at[:, at], own, sem.at[k])
+        for k, (w, own) in enumerate(((w_x, x), (w_z, z)))
     ]
-    for c in copies:
+    leave = [
+        pltpu.make_async_copy(own, picked.at[pl.ds(k * rows, rows)], sem.at[2 + k])
+        for k, own in enumerate((x, z))
+    ]
+    for c in arrive:
         c.start()
-    for c in copies:
+    for c_in, c_out in zip(arrive, leave, strict=True):
+        c_in.wait()
+        c_out.start()
+    for c in leave:
         c.wait()
 
 
@@ -343,7 +349,7 @@
         flops=0,
         ins=[S, H, H],
         out_blocks=H,
-        scratch=[copies(2)],
+        scratch=[pltpu.VMEM((k_rows, width), BF16), pltpu.VMEM((k_rows, width), BF16), copies(4)],
     )
     w_xz = lax.all_gather(picked, "dp", axis=0, tiled=False)
     w_o = lax.all_gather(final_projection, "dp", axis=0, tiled=False)

time: 169 us -> 162 us (0.959)
  Pallas kernels: 24.8 us -> 17.5 us
    pallas_call x9, Pallas kernels: 24.8 us -> 17.5 us  [call(): pl.pallas_call(kernel, out_shape=outs, name=name, in_specs=ins, out_specs...]
  transfers between devices with their start and end apart: 7 -> 7, of which waited for: 4 -> 4; matrix products, arithmetic and copies ran while one was open for 2% -> 3% of each run, Pallas kernels for 9% -> 9%
where the time goes in v5:
time: 162 us; the launch traced here: 161 us
  waiting for transfers between devices  70.3 us (43%)
  blocking collectives  30 us (19%)
  Pallas kernels  17.5 us (11%)
  local copies, waits for them, and re-layouts  16 us (10%)
  between operations  13.8 us (9%)
  starting transfers between devices  13.4 us (8%)
    all_gather x1, waiting for transfers between devices, shards(): w_xz = lax.all_gather(picked, 'dp', axis=0, tiled=False)  44.7 us
    all_to_all x1, blocking collectives, shards(): lax.all_to_all(states, 'sp', split_axis=0, concat_axis=0, tiled=True, axi...  30 us
    pallas_call x9, Pallas kernels, call(): pl.pallas_call(kernel, out_shape=outs, name=name, in_specs=ins, out_specs...  17.5 us
    unnamed x53, local copies, waits for them, and re-layouts  12.2 us
    ppermute x1, waiting for transfers between devices, shards(): other = lax.ppermute(own, 'sp', swap)  11.2 us
    all_to_all x1, waiting for transfers between devices, shards(): lax.all_to_all(own_carried, 'sp', split_axis=0, concat_axis=0, tiled=True...  10.6 us
    ppermute x1, starting transfers between devices, shards(): other = lax.ppermute(own, 'sp', swap)  6.03 us
    all_to_all x1, starting transfers between devices, shards(): lax.all_to_all(own_carried, 'sp', split_axis=0, concat_axis=0, tiled=True...  3.57 us
  transfers between devices with their start and end apart: 7, of which 4 were waited for; matrix products, arithmetic and copies ran while one was open for 3% of the time, Pallas kernels for 9%

profile of v5, /device:TPU:66, one launch (start us, length us, event | category | flops | bytes accessed | tf_op | source)
XLA Modules:
  0.0 160.9 jit_solution(3797258800457510445)
XLA Ops:
  6.6 0.1 all-gather.5.cloned.1.call-start
  6.6 1.7 %pick.1 = bf16[256,512]{1,0:T(8,128)(2,1)} custom-call(s32[1]{0:T(128)} %bitcast.side, bf16[128,1024]{1,0:T(8,128)(2,1)} %w_x.1, bf16[128,1024]{1,0:T(8,128)(2,1)} %w_z.1), custom_call_target="tpu_custom_call" | custom-call | bytes 4194304 | tf_op jit(solution)/shard_map/pick/pallas_call | solution.py:294
  8.4 0.1 all-gather.5.cloned.1.call-update
  8.4 0.1 all-gather.7.cloned.1.call-start
  8.5 0.7 all-gather.7.cloned.1.call-update
  9.2 6.0 %collective-permute-start.2 = (bf16[192,2048]{1,0:T(8,128)(2,1)}, bf16[192,2048]{1,0:T(8,128)(2,1)S(1)}, u32[]{:S(2)}, u32[]{:S(2)}) collective-permute-start(bf16[192,2048]{1,0:T(8,128)(2,1)} %bitcast.22), channel_id=1, source_target_pairs={{0,16},{16,0},{32,48},{48,32},{64,80},{80,64},{96,112},{112,96},{1... | collective-permute-start | bytes 2359304 | tf_op jit(solution)/shard_map/ppermute | solution.py:357
  15.3 0.9 slice_bitcast_fusion
  16.1 0.7 collective-permute-start
  16.8 0.7 collective-permute-start.1
  17.5 0.8 constant_dynamic-slice_fusion.1
  18.2 0.3 copy.22
  18.6 0.1 copy.20
  18.7 0.7 dynamic-slice_bitcast_fusion
  19.4 0.9 copy.21.stride
  20.2 0.1 dynamic_slice.21
  20.3 0.1 dynamic_slice.22
  20.4 0.1 pad.15.w_step
  20.6 0.6 copy-done.17
  21.2 0.6 copy-done.19
  21.8 11.2 %collective-permute-done.2.other = bf16[192,2048]{1,0:T(8,128)(2,1)S(1)} collective-permute-done((bf16[192,2048]{1,0:T(8,128)(2,1)}, bf16[192,2048]{1,0:T(8,128)(2,1)S(1)}, u32[]{:S(2)}, u32[]{:S(2)}) %collective-permute-start.2) | collective-permute-done | bytes 786464 | tf_op jit(solution)/shard_map/ppermute | solution.py:357
  33.1 0.9 copy-done.15
  34.0 0.9 copy-done.9
  34.9 1.1 copy-done.13
  36.0 1.1 copy-done.16
  37.2 0.8 copy-done.18
  38.0 0.8 copy-done.20
  38.8 4.8 %maps.1 = (bf16[400,2048]{1,0:T(8,128)(2,1)S(1)}, bf16[128,384]{1,0:T(8,128)(2,1)S(1)}, bf16[384,128]{1,0:T(8,128)(2,1)S(1)}, bf16[8,384,384]{2,1,0:T(8,128)(2,1...) custom-call(s32[1]{0:T(128)} %bitcast.side, bf16[16,2048]{1,0:T(8,128)(2,1)S(1)} %copy-done.18, ...), custom_call_target="tpu_custom_call" | custom-call | flops 4026531840 | bytes 4194304 | tf_op jit(solution)/shard_map/maps/pallas_call | solution.py:294
  43.6 1.4 copy-done.1
  45.1 0.9 copy-done.3
  45.9 0.6 copy-done.10
  46.6 44.7 %all-gather.5.cloned.1.call-done = bf16[4096,512]{1,0:T(8,128)(2,1)} async-done(((bf16[256,512]{1,0:T(8,128)(2,1)}), bf16[4096,512]{1,0:T(8,128)(2,1)}) %all-gather.5.cloned.1.call-update) | async-done | bytes 4194320 | tf_op jit(solution)/shard_map/all_gather | solution.py:354
  91.3 1.1 copy-done.4
  92.4 3.1 %source.1 = (bf16[384,512]{1,0:T(8,128)(2,1)S(1)}, bf16[384,512]{1,0:T(8,128)(2,1)S(1)}, bf16[128,640]{1,0:T(8,128)(2,1)S(1)}) custom-call(s32[1]{0:T(128)} %bitcast.side, bf16[400,2048]{1,0:T(8,128)(2,1)S(1)} %get-tuple-element.20.rows, bf16[16,256,512]{2,1,0:T(8,128)(2,1)} %bitcast.25, f32[4,1024]{1,0:T(4,128)S(1)} %copy-done.12, ...), custom_call_target="tpu_custom_call" | custom-call | flops 805306368 | bytes 4194304 | tf_op jit(solution)/shard_map/source/pallas_call | solution.py:294
  95.6 0.7 copy-done.7
  96.3 30.0 %all_to_all.22 = bf16[8,16,640]{2,1,0:T(8,128)(2,1)S(1)} all-to-all(bf16[8,16,640]{2,1,0:T(8,128)(2,1)S(1)} %bitcast.21), channel_id=1, replica_groups={{0,32,64,96,128,160,192,224},{16,48,80,112,144,176,208,240},{1,33,65,97..., dimensions={0} | all-to-all | bytes 327680 | tf_op jit(solution)/shard_map/all_to_all | solution.py:430
  126.3 0.7 scan.1
  127.0 3.6 %all-to-all-start.1 = ((bf16[8,16,512]{2,1,0:T(8,128)(2,1)}), bf16[8,16,512]{2,1,0:T(8,128)(2,1)S(1)}, u32[]{:S(2)}, u32[]{:S(2)}) async-start(bf16[8,16,512]{2,1,0:T(8,128)(2,1)} %bitcast.10), calls=%async_computation.1 | async-start | bytes 262144 | tf_op jit(solution)/shard_map/all_to_all | solution.py:468
  130.6 0.1 dynamic_slice.26
  130.7 0.1 broadcast_in_dim.25
  130.8 0.1 broadcast_in_dim_reshape.3.skip
  130.9 2.6 %gate.1 = f32[384,512]{1,0:T(8,128)S(1)} custom-call(bf16[400,2048]{1,0:T(8,128)(2,1)S(1)} %get-tuple-element.20.rows, bf16[16,256,512]{2,1,0:T(8,128)(2,1)} %bitcast.26), custom_call_target="tpu_custom_call" | custom-call | flops 805306368 | bytes 4194304 | tf_op jit(solution)/shard_map/gate/pallas_call | solution.py:294
  133.5 0.6 inner.1.base
  134.0 10.6 %all-to-all-done.1 = bf16[8,16,512]{2,1,0:T(8,128)(2,1)S(1)} async-done(((bf16[8,16,512]{2,1,0:T(8,128)(2,1)}), bf16[8,16,512]{2,1,0:T(8,128)(2,1)S(1)}, u32[]{:S(2)}, u32[]{:S(2)}) %all-to-all-start.1) | async-done | bytes 131104 | tf_op jit(solution)/shard_map/all_to_all | solution.py:468
  144.7 0.4 blend.1
  145.1 2.4 %collective-permute-start.3 = (bf16[192,512]{1,0:T(8,128)(2,1)S(1)}, bf16[192,512]{1,0:T(8,128)(2,1)S(1)}, u32[]{:S(2)}, u32[]{:S(2)}) collective-permute-start(bf16[192,512]{1,0:T(8,128)(2,1)S(1)} %get-tuple-element.29), channel_id=1, source_target_pairs={{0,16},{16,0},{32,48},{48,32},{64,80},{80,64},{96,112},{112,96},{1... | collective-permute-start | bytes 589832 | tf_op jit(solution)/shard_map/ppermute | solution.py:487
  147.5 2.3 %own_half.1 = (f32[192,2048]{1,0:T(8,128)S(1)}, bf16[16,512,128]{2,1,0:T(8,128)(2,1)S(1)}) custom-call(s32[1]{0:T(128)} %bitcast.side, bf16[192,512]{1,0:T(8,128)(2,1)S(1)} %get-tuple-element.30.kept, bf16[16,1024,128]{2,1,0:T(8,128)(2,1)} %bitcast.27), custom_call_target="tpu_custom_call" | custom-call | flops 402653184 | bytes 4194304 | tf_op jit(solution)/shard_map/own_half/pallas_call | solution.py:294
  149.8 2.9 %collective-permute-done.3.arrived = bf16[192,512]{1,0:T(8,128)(2,1)S(1)} collective-permute-done((bf16[192,512]{1,0:T(8,128)(2,1)S(1)}, bf16[192,512]{1,0:T(8,128)(2,1)S(1)}, u32[]{:S(2)}, u32[]{:S(2)}) %collective-permute-start.3) | collective-permute-done | bytes 196640 | tf_op jit(solution)/shard_map/ppermute | solution.py:487
  152.7 1.3 output.1
  (45 shorter events, 0.1 us)
Async XLA Ops:
  6.5 12.0 %copy-start = (f32[1,3072,16]{1,2,0:T(8,128)S(1)}, f32[1,3072,16]{1,2,0:T(8,128)}, u32[]{:S(2)}) copy-start(f32[1,3072,16]{1,2,0:T(8,128)} %param.29) | copy-start | bytes 589828
  6.6 13.7 %copy-start.23 = (f32[16]{0:T(128)S(1)}, f32[16]{0:T(128)}, u32[]{:S(2)}) copy-start(f32[16]{0:T(128)} %param.25) | copy-start | bytes 196
  6.6 13.8 %copy-start.24 = (f32[16]{0:T(128)S(1)}, f32[16]{0:T(128)}, u32[]{:S(2)}) copy-start(f32[16]{0:T(128)} %param.26) | copy-start | bytes 196
  6.6 27.4 %copy-start.21 = (f32[4,256]{1,0:T(4,128)S(1)}, f32[4,256]{1,0:T(4,128)}, u32[]{:S(2)}) copy-start(f32[4,256]{1,0:T(4,128)} %taps_in.1) | copy-start | bytes 12292
  6.6 27.4 %copy-start.22 = (f32[4,256]{1,0:T(4,128)S(1)}, f32[4,256]{1,0:T(4,128)}, u32[]{:S(2)}) copy-start(f32[4,256]{1,0:T(4,128)} %taps_out.1) | copy-start | bytes 12292
  6.6 84.7 %all-gather.5.cloned.1.call-start = ((), (), s32[]{:S(2)}) async-start(), calls=%async_computation.2 | async-start | bytes 4456448 | tf_op jit(solution)/shard_map/all_gather | solution.py:354
  8.4 139.1 %all-gather.7.cloned.1.call-start = ((), (), s32[]{:S(2)}) async-start(), calls=%async_computation.3 | async-start | bytes 4456448 | tf_op jit(solution)/shard_map/all_gather | solution.py:355
  9.2 23.8 %collective-permute-start.2 = (bf16[192,2048]{1,0:T(8,128)(2,1)}, bf16[192,2048]{1,0:T(8,128)(2,1)S(1)}, u32[]{:S(2)}, u32[]{:S(2)}) collective-permute-start(bf16[192,2048]{1,0:T(8,128)(2,1)} %bitcast.22), channel_id=1, source_target_pairs={{0,16},{16,0},{32,48},{48,32},{64,80},{80,64},{96,112},{112,96},{1... | collective-permute-start | bytes 2359304 | tf_op jit(solution)/shard_map/ppermute | solution.py:357
  16.1 4.4 %collective-permute-start = (bf16[16,2048]{1,0:T(8,128)(2,1)S(1)}, bf16[16,2048]{1,0:T(8,128)(2,1)S(1)}, u32[]{:S(2)}, u32[]{:S(2)}) collective-permute-start(bf16[16,2048]{1,0:T(8,128)(2,1)S(1)} %slice_bitcast_fusion), channel_id=1, source_target_pairs={{16,32},{48,64},{80,96},{112,128},{144,160},{176,192},{208,224},{1... | collective-permute-start | bytes 196616 | tf_op jit(solution)/shard_map/ppermute | solution.py:359
  16.8 4.4 %collective-permute-start.1 = (bf16[16,2048]{1,0:T(8,128)(2,1)S(1)}, bf16[16,2048]{1,0:T(8,128)(2,1)S(1)}, u32[]{:S(2)}, u32[]{:S(2)}) collective-permute-start(bf16[16,2048]{1,0:T(8,128)(2,1)S(1)} %slice_bitcast_fusion), channel_id=1, source_target_pairs={{16,48},{48,80},{80,112},{112,144},{144,176},{176,208},{208,240},{... | collective-permute-start | bytes 196616 | tf_op jit(solution)/shard_map/ppermute | solution.py:360
  20.6 0.6 copy-start.17
  21.2 0.6 copy-start.19
  33.1 0.9 copy-start.15
  34.0 0.9 copy-start.9
  34.9 1.1 copy-start.13
  36.0 1.1 copy-start.16
  37.2 0.8 copy-start.18
  38.0 0.8 copy-start.20
  38.8 52.4 %copy-start.12 = (f32[4,1024]{1,0:T(4,128)S(1)}, f32[4,1024]{1,0:T(4,128)}, u32[]{:S(2)}) copy-start(f32[4,1024]{1,0:T(4,128)} %taps.1) | copy-start | bytes 49156
  43.6 1.4 copy-start.1
  45.1 0.9 copy-start.3
  45.9 0.6 copy-start.10
  91.3 1.1 copy-start.4
  92.4 38.2 %copy-start.25 = (f32[16]{0:T(128)S(1)}, f32[16]{0:T(128)}, u32[]{:S(2)}) copy-start(f32[16]{0:T(128)} %param.27) | copy-start | bytes 196
  95.5 0.7 copy-start.7
  96.3 30.7 %copy-start.5 = (bf16[384,512]{1,0:T(8,128)(2,1)}, bf16[384,512]{1,0:T(8,128)(2,1)S(1)}, u32[]{:S(2)}) copy-start(bf16[384,512]{1,0:T(8,128)(2,1)S(1)} %get-tuple-element.28.xs) | copy-start | bytes 1179652
  127.0 17.6 %all-to-all-start.1 = ((bf16[8,16,512]{2,1,0:T(8,128)(2,1)}), bf16[8,16,512]{2,1,0:T(8,128)(2,1)S(1)}, u32[]{:S(2)}, u32[]{:S(2)}) async-start(bf16[8,16,512]{2,1,0:T(8,128)(2,1)} %bitcast.10), calls=%async_computation.1 | async-start | bytes 262144 | tf_op jit(solution)/shard_map/all_to_all | solution.py:468
  130.8 2.6 %copy-start.2 = (bf16[8,384,384]{2,1,0:T(8,128)(2,1)S(1)}, bf16[8,384,384]{2,1,0:T(8,128)(2,1)}, u32[]{:S(2)}) copy-start(bf16[8,384,384]{2,1,0:T(8,128)(2,1)} %copy-done.1) | copy-start | bytes 7077892
  130.9 2.6 %copy-start.6 = (bf16[384,512]{1,0:T(8,128)(2,1)S(1)}, bf16[384,512]{1,0:T(8,128)(2,1)}, u32[]{:S(2)}) copy-start(bf16[384,512]{1,0:T(8,128)(2,1)} %copy-done.5) | copy-start | bytes 1179652
  130.9 2.6 %copy-start.8 = (bf16[384,512]{1,0:T(8,128)(2,1)S(1)}, bf16[384,512]{1,0:T(8,128)(2,1)}, u32[]{:S(2)}) copy-start(bf16[384,512]{1,0:T(8,128)(2,1)} %copy-done.7) | copy-start | bytes 1179652
  133.4 11.3 %copy-start.11 = (bf16[384,128]{1,0:T(8,128)(2,1)S(1)}, bf16[384,128]{1,0:T(8,128)(2,1)}, u32[]{:S(2)}) copy-start(bf16[384,128]{1,0:T(8,128)(2,1)} %copy-done.10) | copy-start | bytes 294916
  133.4 11.2 %copy-start.14 = (f32[1024]{0:T(1024)S(1)}, f32[1024]{0:T(1024)}, u32[]{:S(2)}) copy-start(f32[1024]{0:T(1024)} %param.30) | copy-start | bytes 12292
  145.1 7.6 %collective-permute-start.3 = (bf16[192,512]{1,0:T(8,128)(2,1)S(1)}, bf16[192,512]{1,0:T(8,128)(2,1)S(1)}, u32[]{:S(2)}, u32[]{:S(2)}) collective-permute-start(bf16[192,512]{1,0:T(8,128)(2,1)S(1)} %get-tuple-element.29), channel_id=1, source_target_pairs={{0,16},{16,0},{32,48},{48,32},{64,80},{80,64},{96,112},{112,96},{1... | collective-permute-start | bytes 589832 | tf_op jit(solution)/shard_map/ppermute | solution.py:487
Sparse Core Ops, SparseCore 0:
  9.5 81.6 all-gather.4
  93.4 47.0 all-gather.6

commit v6 on v5

--- a/solution.py
+++ b/solution.py
@@ -145,7 +145,7 @@
 
 
 def source_kernel(
-    side, rows, w_xz, taps, step_wide, end_wide, reach_wide, in_t, xs_out, scaled_out, states,
+    side, rows, w_xz, taps, step_wide, end_wide, in_t, xs_out, scaled_out, states, passed,
     w, sem,
 ):
     length, width = step_wide.shape
@@ -155,21 +155,9 @@
     xs_out[...] = xs
     xs = xs.astype(F32)
     weighted = (xs * end_wide[...]).astype(BF16)
-    states[:, :width] = jnp.dot(in_t[...], weighted, preferred_element_type=F32).astype(BF16)
-    rest = reach_wide[length - 1 : length, :]
-    row = lax.broadcasted_iota(jnp.int32, (HALO, LANES), 0)
-    pieces = jnp.zeros((HALO, LANES), F32)
-    blocks = width // LANES
-    for k in range(3):
-        piece = rest.astype(BF16).astype(F32)
-        rest = rest - piece
-        for c in range(blocks):
-            pieces = jnp.where(
-                row == k * blocks + c, piece[:, c * LANES : (c + 1) * LANES], pieces
-            )
-    pieces = pieces.astype(BF16)
-    for i in range(states.shape[0] // HALO):
-        states[i * HALO : (i + 1) * HALO, width:] = pieces
+    state = jnp.dot(in_t[...], weighted, preferred_element_type=F32)
+    states[...] = state
+    passed[...] = state.astype(BF16)
     scaled_out[...] = (xs * step_wide[...]).astype(BF16)
 
 
@@ -189,33 +177,24 @@
             ].astype(F32)
 
 
-def scan_kernel(states, carried):
-    rows = HALO
-    width = carried.shape[1]
-    blocks = width // LANES
-    acc = jnp.zeros((rows, width), F32)
-    for k in range(states.shape[0] // rows):
-        at = slice(k * rows, (k + 1) * rows)
-        carried[at, :] = acc.astype(BF16)
-        pieces = states[at, width:].astype(F32)
-        factor = jnp.concatenate(
-            [
-                pieces[c : c + 1] + pieces[blocks + c : blocks + c + 1]
-                + pieces[2 * blocks + c : 2 * blocks + c + 1]
-                for c in range(blocks)
-            ],
-            axis=1,
-        )
-        acc = acc * factor + states[at, :width].astype(F32)
+def pass_kernel(states, reach_wide, before, arrived, carried, passed):
+    length = reach_wide.shape[0]
+    entered = before[...] + arrived[...]
+    carried[...] = entered
+    decay = reach_wide[length - 1 : length, :]
+    passed[...] = (states[...] + decay * entered.astype(F32)).astype(BF16)
 
 
 def gate_kernel(rows, w_xz, gate, w, sem):
     gate[...] = silu(streamed_dot(rows, HALO, w_xz, 1, w, sem))
 
 
-def blend_kernel(side, out_maps, carried, reach_wide, base, gate, gain, kept, sent, normed):
+def blend_kernel(
+    side, out_maps, before, arrived, reach_wide, base, gate, gain, kept, sent, normed
+):
     part = kept.shape[0]
-    reached = jnp.dot(out_maps[...], carried[...], preferred_element_type=F32)
+    carried = before[...] + arrived[...]
+    reached = jnp.dot(out_maps[...], carried, preferred_element_type=F32)
     mixed = (base[...] + reached * reach_wide[...]).astype(BF16).astype(F32)
     gated = mixed * gate[...]
     mean = jnp.mean(gated * gated, axis=1, keepdims=True)
@@ -336,7 +315,6 @@
     me = lax.axis_index("sp")
     side_index = me % 2
     side = side_index.astype(jnp.int32)[None]
-    ranks = [list(range(0, sp, 2)), list(range(1, sp, 2))]
     swap = [(i, i ^ 1) for i in range(sp)]
 
     picked = call(
@@ -409,27 +387,41 @@
     )
 
     w_half = pltpu.VMEM((dp, k_rows, width), BF16)
-    xs, scaled, states = call(
+    carry = (N, width)
+    xs, scaled, states, passed = call(
         source_kernel,
-        (held(wide, BF16), held(wide, BF16), shape((N, width + LANES), BF16)),
+        (held(wide, BF16), held(wide, BF16), held(carry), shape(carry, BF16)),
         side,
         rows,
         w_xz,
         source_conv_taps,
         step_wide,
         end_wide,
-        reach_wide,
         in_t,
         name="source",
         flops=2 * length * d_model * width,
-        ins=[S, K, H, V, K, K, K, K],
-        out_blocks=[V, V, V],
+        ins=[S, K, H, V, K, K, K],
+        out_blocks=[V, V, V, V],
         scratch=[w_half, copies(4)],
         limit=20,
     )
-    arrived = lax.all_to_all(
-        states, "sp", split_axis=0, concat_axis=0, tiled=True, axis_index_groups=ranks
-    )
+    before = jnp.zeros(carry, BF16)
+    for k in range(sp // 2 - 1):
+        links = [(i, i + 2) for i in (2 * k, 2 * k + 1)]
+        arrived = lax.ppermute(passed, "sp", links)
+        if k < sp // 2 - 2:
+            before, passed = call(
+                pass_kernel,
+                (shape(carry, BF16), shape(carry, BF16)),
+                states,
+                reach_wide,
+                before,
+                arrived,
+                name="pass",
+                flops=1000,
+                ins=[K, K, V, V],
+                out_blocks=[V, V],
+            )
     gate = call(
         gate_kernel,
         held(wide),
@@ -456,31 +448,20 @@
         ins=[K, K, K, V],
         out_blocks=V,
     )
-    own_carried = call(
-        scan_kernel,
-        shape((N, width), BF16),
-        arrived,
-        name="scan",
-        flops=1000,
-        ins=[V],
-        out_blocks=V,
-    )
-    carried = lax.all_to_all(
-        own_carried, "sp", split_axis=0, concat_axis=0, tiled=True, axis_index_groups=ranks
-    )
     kept, sent = call(
         blend_kernel,
         (held((part, width), BF16), shape((part, width), BF16)),
         side,
         out_maps,
-        carried,
+        before,
+        arrived,
         reach_wide,
         base,
         gate,
         norm_scale_factor[None],
         name="blend",
         flops=2 * length * N * width,
-        ins=[S, K, V, K, K, K, V],
+        ins=[S, K, V, V, K, K, K, V],
         out_blocks=[V, V],
         scratch=[pltpu.VMEM(wide, BF16)],
     )

time: 162 us -> 153 us (0.944)
  the two profiles are of different devices: /device:TPU:66 before, /device:TPU:65 now
where the time goes in v6:
time: 153 us; the launch traced here: 152 us
  waiting for transfers between devices  85 us (56%)
  starting transfers between devices  23 us (15%)
  Pallas kernels  17.7 us (12%)
  between operations  13.9 us (9%)
  local copies, waits for them, and re-layouts  13 us (8%)
    all_gather x1, waiting for transfers between devices, shards(): w_xz = lax.all_gather(picked, 'dp', axis=0, tiled=False)  55.4 us
    all_gather x1, waiting for transfers between devices, shards(): w_o = lax.all_gather(final_projection, 'dp', axis=0, tiled=False)  21.1 us
    pallas_call x14, Pallas kernels, call(): pl.pallas_call(kernel, out_shape=outs, name=name, in_specs=ins, out_specs...  17.7 us
    unnamed x43, local copies, waits for them, and re-layouts  9.85 us
    ppermute x7, starting transfers between devices, shards(): arrived = lax.ppermute(passed, 'sp', links)  8.55 us
    ppermute x1, starting transfers between devices, shards(): other = lax.ppermute(own, 'sp', swap)  6.57 us
    ppermute x1, starting transfers between devices, shards(): arrived_half = lax.ppermute(sent, 'sp', swap)  6.4 us
    ppermute x1, waiting for transfers between devices, shards(): other = lax.ppermute(own, 'sp', swap)  5.03 us
  transfers between devices with their start and end apart: 13, of which 4 were waited for; matrix products, arithmetic and copies ran while one was open for 2% of the time, Pallas kernels for 10%

profile of v6, /device:TPU:65, one launch (start us, length us, event | category | flops | bytes accessed | tf_op | source)
XLA Modules:
  0.0 152.5 jit_solution(17167681433483706159)
XLA Ops:
  6.6 1.7 %pick.1 = bf16[256,512]{1,0:T(8,128)(2,1)} custom-call(s32[1]{0:T(128)} %bitcast.side, bf16[128,1024]{1,0:T(8,128)(2,1)} %w_x.1, bf16[128,1024]{1,0:T(8,128)(2,1)} %w_z.1), custom_call_target="tpu_custom_call" | custom-call | bytes 4194304 | tf_op jit(solution)/shard_map/pick/pallas_call | solution.py:273
  8.4 0.1 all-gather.7.cloned.1.call-start
  8.5 0.7 all-gather.7.cloned.1.call-update
  9.2 6.6 %collective-permute-start.2 = (bf16[192,2048]{1,0:T(8,128)(2,1)}, bf16[192,2048]{1,0:T(8,128)(2,1)S(1)}, u32[]{:S(2)}, u32[]{:S(2)}) collective-permute-start(bf16[192,2048]{1,0:T(8,128)(2,1)} %bitcast.15), channel_id=1, source_target_pairs={{0,16},{16,0},{32,48},{48,32},{64,80},{80,64},{96,112},{112,96},{1... | collective-permute-start | bytes 2359304 | tf_op jit(solution)/shard_map/ppermute | solution.py:335
  15.8 0.9 slice_bitcast_fusion
  16.7 0.7 collective-permute-start
  17.3 0.7 collective-permute-start.1
  18.0 0.8 constant_dynamic-slice_fusion.1
  18.8 0.3 copy.22
  19.1 0.1 copy.20
  19.3 0.7 dynamic-slice_bitcast_fusion
  19.9 0.1 copy.21.stride
  20.1 0.1 dynamic_slice.21
  20.2 0.1 dynamic_slice.22
  20.3 0.1 pad.15.w_step
  20.4 5.0 %collective-permute-done.2.other = bf16[192,2048]{1,0:T(8,128)(2,1)S(1)} collective-permute-done((bf16[192,2048]{1,0:T(8,128)(2,1)}, bf16[192,2048]{1,0:T(8,128)(2,1)S(1)}, u32[]{:S(2)}, u32[]{:S(2)}) %collective-permute-start.2) | collective-permute-done | bytes 786464 | tf_op jit(solution)/shard_map/ppermute | solution.py:335
  25.5 0.9 copy-done.14
  26.3 1.1 copy-done.12
  27.5 1.1 copy-done.15
  28.6 4.8 %maps.1 = (bf16[400,2048]{1,0:T(8,128)(2,1)S(1)}, bf16[128,384]{1,0:T(8,128)(2,1)S(1)}, bf16[384,128]{1,0:T(8,128)(2,1)S(1)}, bf16[8,384,384]{2,1,0:T(8,128)(2,1...) custom-call(s32[1]{0:T(128)} %bitcast.side, ...), custom_call_target="tpu_custom_call" | custom-call | flops 4026531840 | bytes 4194304 | tf_op jit(solution)/shard_map/maps/pallas_call | solution.py:273
  33.4 1.4 copy-done.1
  34.8 0.9 copy-done.3
  35.7 0.9 copy-done.5
  36.6 0.6 copy-done.9
  37.2 55.4 %all-gather.5.cloned.1.call-done = bf16[4096,512]{1,0:T(8,128)(2,1)} async-done(((bf16[256,512]{1,0:T(8,128)(2,1)}), bf16[4096,512]{1,0:T(8,128)(2,1)}) %all-gather.5.cloned.1.call-update) | async-done | bytes 4194320 | tf_op jit(solution)/shard_map/all_gather | solution.py:332
  92.7 1.1 copy-done.4
  93.8 1.1 copy-done.6
  94.9 3.1 %source.1 = (bf16[384,512]{1,0:T(8,128)(2,1)S(1)}, bf16[384,512]{1,0:T(8,128)(2,1)S(1)}, f32[128,512]{1,0:T(8,128)S(1)}, bf16[128,512]{1,0:T(8,128)(2,1)S(1)}) custom-call(s32[1]{0:T(128)} %bitcast.side, bf16[400,2048]{1,0:T(8,128)(2,1)S(1)} %get-tuple-element.33.rows, bf16[16,256,512]{2,1,0:T(8,128)(2,1)} %bitcast.18, f32[4,1024]{1,0:T(4,128)S(1)} %copy-done.11, ...), custom_call_target="tpu_custom_call" | custom-call | flops 805306368 | bytes 4194304 | tf_op jit(solution)/shard_map/source/pallas_call | solution.py:273
  98.1 4.4 %collective-permute-start.3 = (bf16[128,512]{1,0:T(8,128)(2,1)S(1)}, bf16[128,512]{1,0:T(8,128)(2,1)S(1)}, u32[]{:S(2)}, u32[]{:S(2)}) collective-permute-start(bf16[128,512]{1,0:T(8,128)(2,1)S(1)} %get-tuple-element.39), channel_id=1, source_target_pairs={{0,32},{16,48},{1,33},{17,49},{2,34},{18,50},{3,35},{19,51},{4,36}... | collective-permute-start | bytes 393224 | tf_op jit(solution)/shard_map/ppermute | solution.py:411
  102.5 2.6 %collective-permute-done.3.arrived = bf16[128,512]{1,0:T(8,128)(2,1)S(1)} collective-permute-done((bf16[128,512]{1,0:T(8,128)(2,1)S(1)}, bf16[128,512]{1,0:T(8,128)(2,1)S(1)}, u32[]{:S(2)}, u32[]{:S(2)}) %collective-permute-start.3) | collective-permute-done | bytes 131104 | tf_op jit(solution)/shard_map/ppermute | solution.py:411
  105.1 0.7 collective-permute-start.4
  105.9 0.7 collective-permute-start.5
  106.6 0.7 collective-permute-start.6
  107.4 0.7 collective-permute-start.7
  108.1 0.7 pass.10
  108.8 0.7 collective-permute-start.8
  109.4 0.1 dynamic_slice.26
  109.5 0.1 broadcast_in_dim.29
  109.6 0.1 broadcast_in_dim_reshape.3.skip
  109.7 0.8 collective-permute-start.9
  110.6 2.5 %gate.1 = f32[384,512]{1,0:T(8,128)S(1)} custom-call(bf16[400,2048]{1,0:T(8,128)(2,1)S(1)} %get-tuple-element.33.rows, bf16[16,256,512]{2,1,0:T(8,128)(2,1)} %bitcast.19), custom_call_target="tpu_custom_call" | custom-call | flops 805306368 | bytes 4194304 | tf_op jit(solution)/shard_map/gate/pallas_call | solution.py:273
  113.1 0.6 inner.1.base
  113.7 0.3 copy-done.10
  114.0 0.5 blend.1
  114.5 6.4 %collective-permute-start.10 = (bf16[192,512]{1,0:T(8,128)(2,1)S(1)}, bf16[192,512]{1,0:T(8,128)(2,1)S(1)}, u32[]{:S(2)}, u32[]{:S(2)}) collective-permute-start(bf16[192,512]{1,0:T(8,128)(2,1)S(1)} %get-tuple-element.55), channel_id=1, source_target_pairs={{0,16},{16,0},{32,48},{48,32},{64,80},{80,64},{96,112},{112,96},{1... | collective-permute-start | bytes 589832 | tf_op jit(solution)/shard_map/ppermute | solution.py:468
  120.9 21.1 %all-gather.7.cloned.1.call-done = bf16[16384,128]{1,0:T(8,128)(2,1)} async-done(((bf16[1024,128]{1,0:T(8,128)(2,1)}), bf16[16384,128]{1,0:T(8,128)(2,1)}) %all-gather.7.cloned.1.call-update) | async-done | bytes 4194320 | tf_op jit(solution)/shard_map/all_gather | solution.py:333
  142.0 2.3 %own_half.1 = (f32[192,2048]{1,0:T(8,128)S(1)}, bf16[16,512,128]{2,1,0:T(8,128)(2,1)S(1)}) custom-call(s32[1]{0:T(128)} %bitcast.side, bf16[192,512]{1,0:T(8,128)(2,1)S(1)} %get-tuple-element.56.kept, bf16[16,1024,128]{2,1,0:T(8,128)(2,1)} %bitcast.20), custom_call_target="tpu_custom_call" | custom-call | flops 402653184 | bytes 4194304 | tf_op jit(solution)/shard_map/own_half/pallas_call | solution.py:273
  144.3 1.3 output.1
  (52 shorter events, 0.5 us)
Async XLA Ops:
  6.5 12.5 %copy-start = (f32[1,3072,16]{1,2,0:T(8,128)S(1)}, f32[1,3072,16]{1,2,0:T(8,128)}, u32[]{:S(2)}) copy-start(f32[1,3072,16]{1,2,0:T(8,128)} %param.29) | copy-start | bytes 589828
  6.6 13.5 %copy-start.18 = (f32[16]{0:T(128)S(1)}, f32[16]{0:T(128)}, u32[]{:S(2)}) copy-start(f32[16]{0:T(128)} %param.25) | copy-start | bytes 196
  6.6 13.6 %copy-start.19 = (f32[16]{0:T(128)S(1)}, f32[16]{0:T(128)}, u32[]{:S(2)}) copy-start(f32[16]{0:T(128)} %param.26) | copy-start | bytes 196
  6.6 19.8 %copy-start.16 = (f32[4,256]{1,0:T(4,128)S(1)}, f32[4,256]{1,0:T(4,128)}, u32[]{:S(2)}) copy-start(f32[4,256]{1,0:T(4,128)} %taps_in.1) | copy-start | bytes 12292
  6.6 19.8 %copy-start.17 = (f32[4,256]{1,0:T(4,128)S(1)}, f32[4,256]{1,0:T(4,128)}, u32[]{:S(2)}) copy-start(f32[4,256]{1,0:T(4,128)} %taps_out.1) | copy-start | bytes 12292
  6.6 86.1 %all-gather.5.cloned.1.call-start = ((), (), s32[]{:S(2)}) async-start(), calls=%async_computation | async-start | bytes 4456448 | tf_op jit(solution)/shard_map/all_gather | solution.py:332
  8.4 133.6 %all-gather.7.cloned.1.call-start = ((), (), s32[]{:S(2)}) async-start(), calls=%async_computation.1 | async-start | bytes 4456448 | tf_op jit(solution)/shard_map/all_gather | solution.py:333
  9.2 16.2 %collective-permute-start.2 = (bf16[192,2048]{1,0:T(8,128)(2,1)}, bf16[192,2048]{1,0:T(8,128)(2,1)S(1)}, u32[]{:S(2)}, u32[]{:S(2)}) collective-permute-start(bf16[192,2048]{1,0:T(8,128)(2,1)} %bitcast.15), channel_id=1, source_target_pairs={{0,16},{16,0},{32,48},{48,32},{64,80},{80,64},{96,112},{112,96},{1... | collective-permute-start | bytes 2359304 | tf_op jit(solution)/shard_map/ppermute | solution.py:335
  16.7 3.7 %collective-permute-start = (bf16[16,2048]{1,0:T(8,128)(2,1)S(1)}, bf16[16,2048]{1,0:T(8,128)(2,1)S(1)}, u32[]{:S(2)}, u32[]{:S(2)}) collective-permute-start(bf16[16,2048]{1,0:T(8,128)(2,1)S(1)} %slice_bitcast_fusion), channel_id=1, source_target_pairs={{16,32},{48,64},{80,96},{112,128},{144,160},{176,192},{208,224},{1... | collective-permute-start | bytes 196616 | tf_op jit(solution)/shard_map/ppermute | solution.py:337
  17.3 3.1 %collective-permute-start.1 = (bf16[16,2048]{1,0:T(8,128)(2,1)S(1)}, bf16[16,2048]{1,0:T(8,128)(2,1)S(1)}, u32[]{:S(2)}, u32[]{:S(2)}) collective-permute-start(bf16[16,2048]{1,0:T(8,128)(2,1)S(1)} %slice_bitcast_fusion), channel_id=1, source_target_pairs={{16,48},{48,80},{80,112},{112,144},{144,176},{176,208},{208,240},{... | collective-permute-start | bytes 196616 | tf_op jit(solution)/shard_map/ppermute | solution.py:338
  25.5 0.9 copy-start.14
  26.3 1.1 copy-start.12
  27.5 1.1 copy-start.15
  28.6 64.1 %copy-start.11 = (f32[4,1024]{1,0:T(4,128)S(1)}, f32[4,1024]{1,0:T(4,128)}, u32[]{:S(2)}) copy-start(f32[4,1024]{1,0:T(4,128)} %taps.1) | copy-start | bytes 49156
  33.4 1.4 copy-start.1
  34.8 0.9 copy-start.3
  35.7 0.9 copy-start.5
  36.6 0.6 copy-start.9
  92.7 1.1 copy-start.4
  93.8 1.1 copy-start.6
  98.0 9.3 %copy-start.7 = (bf16[384,512]{1,0:T(8,128)(2,1)}, bf16[384,512]{1,0:T(8,128)(2,1)S(1)}, u32[]{:S(2)}) copy-start(bf16[384,512]{1,0:T(8,128)(2,1)S(1)} %get-tuple-element.53.scaled) | copy-start | bytes 1179652
  98.1 7.0 %collective-permute-start.3 = (bf16[128,512]{1,0:T(8,128)(2,1)S(1)}, bf16[128,512]{1,0:T(8,128)(2,1)S(1)}, u32[]{:S(2)}, u32[]{:S(2)}) collective-permute-start(bf16[128,512]{1,0:T(8,128)(2,1)S(1)} %get-tuple-element.39), channel_id=1, source_target_pairs={{0,32},{16,48},{1,33},{17,49},{2,34},{18,50},{3,35},{19,51},{4,36}... | collective-permute-start | bytes 393224 | tf_op jit(solution)/shard_map/ppermute | solution.py:411
  105.1 0.7 collective-permute-start.4
  105.8 3.6 %copy-start.20 = (f32[16]{0:T(128)S(1)}, f32[16]{0:T(128)}, u32[]{:S(2)}) copy-start(f32[16]{0:T(128)} %param.27) | copy-start | bytes 196
  105.9 0.7 collective-permute-start.5
  106.6 0.7 collective-permute-start.6
  107.4 0.7 collective-permute-start.7
  108.8 0.9 collective-permute-start.8
  109.7 3.4 %copy-start.2 = (bf16[8,384,384]{2,1,0:T(8,128)(2,1)S(1)}, bf16[8,384,384]{2,1,0:T(8,128)(2,1)}, u32[]{:S(2)}) copy-start(bf16[8,384,384]{2,1,0:T(8,128)(2,1)} %copy-done.1) | copy-start | bytes 7077892
  109.7 3.4 %copy-start.8 = (bf16[384,512]{1,0:T(8,128)(2,1)S(1)}, bf16[384,512]{1,0:T(8,128)(2,1)}, u32[]{:S(2)}) copy-start(bf16[384,512]{1,0:T(8,128)(2,1)} %copy-done.7) | copy-start | bytes 1179652
  109.7 4.0 %collective-permute-start.9 = (bf16[128,512]{1,0:T(8,128)(2,1)S(1)}, bf16[128,512]{1,0:T(8,128)(2,1)S(1)}, u32[]{:S(2)}, u32[]{:S(2)}) collective-permute-start(bf16[128,512]{1,0:T(8,128)(2,1)S(1)} %get-tuple-element.51), channel_id=1, source_target_pairs={{192,224},{208,240},{193,225},{209,241},{194,226},{210,242},{195,2... | collective-permute-start | bytes 393224 | tf_op jit(solution)/shard_map/ppermute | solution.py:411
  113.1 0.9 copy-start.10
  113.1 0.9 copy-start.13
  114.5 29.8 %collective-permute-start.10 = (bf16[192,512]{1,0:T(8,128)(2,1)S(1)}, bf16[192,512]{1,0:T(8,128)(2,1)S(1)}, u32[]{:S(2)}, u32[]{:S(2)}) collective-permute-start(bf16[192,512]{1,0:T(8,128)(2,1)S(1)} %get-tuple-element.55), channel_id=1, source_target_pairs={{0,16},{16,0},{32,48},{48,32},{64,80},{80,64},{96,112},{112,96},{1... | collective-permute-start | bytes 589832 | tf_op jit(solution)/shard_map/ppermute | solution.py:468
Sparse Core Ops, SparseCore 0:
  9.5 83.0 all-gather.4
  94.8 47.1 all-gather.6

commit v7 on v6

--- a/solution.py
+++ b/solution.py
@@ -41,24 +41,30 @@
     )
 
 
-def pick_kernel(side, w_x, w_z, picked, x, z, sem):
-    rows, width = x.shape
+def pick_kernel(side, w_x, w_z, w_o, picked, held_rows, sem):
+    rows = w_x.shape[0]
+    width = picked.shape[1]
+    tall = picked.shape[0] - 2 * rows
     at = pl.ds(pl.multiple_of(side[0] * width, LANES), width)
     arrive = [
-        pltpu.make_async_copy(w.at[:, at], own, sem.at[k])
-        for k, (w, own) in enumerate(((w_x, x), (w_z, z)))
-    ]
-    leave = [
-        pltpu.make_async_copy(own, picked.at[pl.ds(k * rows, rows)], sem.at[2 + k])
-        for k, own in enumerate((x, z))
-    ]
+        pltpu.make_async_copy(w.at[:, at], held_rows.at[pl.ds(k * rows, rows)], sem.at[k])
+        for k, w in enumerate((w_x, w_z))
+    ]
+    for b in range(w_o.shape[0] // tall):
+        arrive.append(
+            pltpu.make_async_copy(
+                w_o.at[pl.ds(b * tall, tall)],
+                held_rows.at[pl.ds(2 * rows, tall), pl.ds(b * LANES, LANES)],
+                sem.at[2 + b],
+            )
+        )
     for c in arrive:
         c.start()
-    for c_in, c_out in zip(arrive, leave, strict=True):
-        c_in.wait()
-        c_out.start()
-    for c in leave:
+    for c in arrive:
         c.wait()
+    leave = pltpu.make_async_copy(held_rows, picked, sem.at[0])
+    leave.start()
+    leave.wait()
 
 
 def maps_kernel(
@@ -120,7 +126,7 @@
                 mixing[h, to, frm] = (inter * jnp.exp(gap)).astype(BF16)
 
 
-def streamed_dot(rows, first, w_all, half, w, sem):
+def streamed_dot(rows, first, w_all, half, w, sem, others=()):
     parts = sem.shape[0]
     count = w_all.shape[0] // parts
     k_rows = w.shape[1]
@@ -132,7 +138,7 @@
         )
         for p in range(parts)
     ]
-    for c in copies:
+    for c in [*copies, *others]:
         c.start()
     acc = None
     for p in range(parts):
@@ -145,19 +151,25 @@
 
 
 def source_kernel(
-    side, rows, w_xz, taps, step_wide, end_wide, in_t, xs_out, scaled_out, states, passed,
-    w, sem,
+    side, rows, w_xz, taps, step_all, end_all, in_t, xs_out, scaled_out, states, passed,
+    w, step_wide, end_wide, sem, sem_wide,
 ):
     length, width = step_wide.shape
-    raw = streamed_dot(rows, 0, w_xz, 0, w, sem)
+    wides = [
+        pltpu.make_async_copy(src, dst, sem_wide.at[k])
+        for k, (src, dst) in enumerate(((end_all, end_wide), (step_all, step_wide)))
+    ]
+    raw = streamed_dot(rows, 0, w_xz, 0, w, sem, wides)
     group = pl.ds(pl.multiple_of(side[0] * width, LANES), width)
     xs = conv_silu(raw, taps[:, group]).astype(BF16)
     xs_out[...] = xs
     xs = xs.astype(F32)
+    wides[0].wait()
     weighted = (xs * end_wide[...]).astype(BF16)
     state = jnp.dot(in_t[...], weighted, preferred_element_type=F32)
     states[...] = state
     passed[...] = state.astype(BF16)
+    wides[1].wait()
     scaled_out[...] = (xs * step_wide[...]).astype(BF16)
 
 
@@ -205,22 +217,29 @@
 
 
 def joined(w, first, count):
-    return jnp.concatenate([w[d] for d in range(first, first + count)], axis=1)
-
-
-def own_half_kernel(side, kept, w_o, partial, w_other, w, sem):
+    tall = [
+        jnp.concatenate([w[d, :, :LANES], w[d, :, LANES:]], axis=0)
+        for d in range(first, first + count)
+    ]
+    return jnp.concatenate(tall, axis=1)
+
+
+def own_half_kernel(side, kept, w_all, partial, w_other, w, sem):
     parts = sem.shape[0] - 1
-    count = w_o.shape[0] // parts
-    width = kept.shape[1]
-    mine = pl.ds(pl.multiple_of(side[0] * width, LANES), width)
-    others = pl.ds(pl.multiple_of((1 - side[0]) * width, LANES), width)
+    count = w_all.shape[0] // parts
+    tall, wide = w.shape[1:]
+    low = pl.ds(w_all.shape[1] - tall, tall)
+    mine = pl.ds(pl.multiple_of(side[0] * wide, LANES), wide)
+    others = pl.ds(pl.multiple_of((1 - side[0]) * wide, LANES), wide)
     copies = [
         pltpu.make_async_copy(
-            w_o.at[pl.ds(p * count, count), mine], w.at[pl.ds(p * count, count)], sem.at[p]
+            w_all.at[pl.ds(p * count, count), low, mine],
+            w.at[pl.ds(p * count, count)],
+            sem.at[p],
         )
         for p in range(parts)
     ]
-    copies.append(pltpu.make_async_copy(w_o.at[:, others], w_other, sem.at[parts]))
+    copies.append(pltpu.make_async_copy(w_all.at[:, low, others], w_other, sem.at[parts]))
     for c in copies:
         c.start()
     for p in range(parts):
@@ -317,20 +336,23 @@
     side = side_index.astype(jnp.int32)[None]
     swap = [(i, i ^ 1) for i in range(sp)]
 
+    o_blocks = width // LANES
+    tall = final_projection.shape[0] // o_blocks
+    all_rows = 2 * k_rows + tall
     picked = call(
         pick_kernel,
-        shape((2 * k_rows, width), BF16),
+        shape((all_rows, width), BF16),
         side,
         source_projection,
         gating_projection,
+        final_projection,
         name="pick",
         flops=0,
-        ins=[S, H, H],
+        ins=[S, H, H, H],
         out_blocks=H,
-        scratch=[pltpu.VMEM((k_rows, width), BF16), pltpu.VMEM((k_rows, width), BF16), copies(4)],
-    )
-    w_xz = lax.all_gather(picked, "dp", axis=0, tiled=False)
-    w_o = lax.all_gather(final_projection, "dp", axis=0, tiled=False)
+        scratch=[pltpu.VMEM((all_rows, width), BF16), copies(2 + o_blocks)],
+    )
+    w_all = lax.all_gather(picked, "dp", axis=0, tiled=False)
 
     other = lax.ppermute(own, "sp", swap)
     edge = own[part - HALO :]
@@ -357,8 +379,8 @@
         held((N, length), BF16),
         held((length, N), BF16),
         held((heads, length, length), BF16),
-        held(wide),
-        held(wide),
+        shape(wide),
+        shape(wide),
         held(wide),
     )
     rows, in_t, out_maps, mixing, step_wide, end_wide, reach_wide = call(
@@ -393,16 +415,16 @@
         (held(wide, BF16), held(wide, BF16), held(carry), shape(carry, BF16)),
         side,
         rows,
-        w_xz,
+        w_all,
         source_conv_taps,
         step_wide,
         end_wide,
         in_t,
         name="source",
         flops=2 * length * d_model * width,
-        ins=[S, K, H, V, K, K, K],
+        ins=[S, K, H, V, H, H, K],
         out_blocks=[V, V, V, V],
-        scratch=[w_half, copies(4)],
+        scratch=[w_half, pltpu.VMEM(wide, F32), pltpu.VMEM(wide, F32), copies(4), copies(2)],
         limit=20,
     )
     before = jnp.zeros(carry, BF16)
@@ -426,7 +448,7 @@
         gate_kernel,
         held(wide),
         rows,
-        w_xz,
+        w_all,
         name="gate",
         flops=2 * length * d_model * width,
         ins=[K, H],
@@ -467,13 +489,13 @@
     )
     arrived_half = lax.ppermute(sent, "sp", swap)
     out_dims = (part, dp * final_projection.shape[1])
-    w_o_half = (dp, width, final_projection.shape[1])
+    w_o_half = (dp, tall, width // G)
     partial, w_other = call(
         own_half_kernel,
         (held(out_dims), held(w_o_half, BF16)),
         side,
         kept,
-        w_o,
+        w_all,
         name="own_half",
         flops=2 * part * width * d_model,
         ins=[S, K, H],

time: 153 us -> 146 us (0.954)
  waiting for transfers between devices: 85 us -> 79.9 us
  local copies, waits for them, and re-layouts: 13 us -> 10.7 us
    all_gather x2 -> x1, waiting for transfers between devices: 76.5 us -> 69.7 us  [shards(): w_all = lax.all_gather(picked, 'dp', axis=0, tiled=False)]
    ppermute x1, waiting for transfers between devices: 0.01 us -> 2.42 us  [shards(): arrived_half = lax.ppermute(sent, 'sp', swap)]
    unnamed x43 -> x39, local copies, waits for them, and re-layouts: 9.85 us -> 7.56 us
  transfers between devices with their start and end apart: 13 -> 12, of which waited for: 4 -> 4; matrix products, arithmetic and copies ran while one was open for 2% -> 2% of each run, Pallas kernels for 10% -> 7%
where the time goes in v7:
time: 146 us; the launch traced here: 145 us
  waiting for transfers between devices  79.9 us (55%)
  starting transfers between devices  22.9 us (16%)
  Pallas kernels  17.9 us (12%)
  between operations  13.9 us (10%)
  local copies, waits for them, and re-layouts  10.7 us (7%)
    all_gather x1, waiting for transfers between devices, shards(): w_all = lax.all_gather(picked, 'dp', axis=0, tiled=False)  69.7 us
    pallas_call x14, Pallas kernels, call(): pl.pallas_call(kernel, out_shape=outs, name=name, in_specs=ins, out_specs...  17.9 us
    ppermute x7, starting transfers between devices, shards(): arrived = lax.ppermute(passed, 'sp', links)  8.49 us
    unnamed x39, local copies, waits for them, and re-layouts  7.56 us
    ppermute x1, starting transfers between devices, shards(): other = lax.ppermute(own, 'sp', swap)  6.57 us
    ppermute x1, starting transfers between devices, shards(): arrived_half = lax.ppermute(sent, 'sp', swap)  6.55 us
    ppermute x1, waiting for transfers between devices, shards(): other = lax.ppermute(own, 'sp', swap)  5.07 us
  transfers between devices with their start and end apart: 12, of which 4 were waited for; matrix products, arithmetic and copies ran while one was open for 2% of the time, Pallas kernels for 7%

profile of v7, /device:TPU:65, one launch (start us, length us, event | category | flops | bytes accessed | tf_op | source)
XLA Modules:
  0.0 145.4 jit_solution(341950565719098498)
XLA Ops:
  6.6 2.0 %pick.1 = bf16[512,512]{1,0:T(8,128)(2,1)} custom-call(s32[1]{0:T(128)} %bitcast.side, bf16[128,1024]{1,0:T(8,128)(2,1)} %w_x.1, bf16[128,1024]{1,0:T(8,128)(2,1)} %w_z.1, bf16[1024,128]{1,0:T(8,128)(2,1)} %w_o.1), custom_call_target="tpu_custom_call" | custom-call | bytes 4194304 | tf_op jit(solution)/shard_map/pick/pallas_call | solution.py:292
  8.6 0.1 all-gather.3.cloned.1.call-update
  8.7 6.6 %collective-permute-start.2 = (bf16[192,2048]{1,0:T(8,128)(2,1)}, bf16[192,2048]{1,0:T(8,128)(2,1)S(1)}, u32[]{:S(2)}, u32[]{:S(2)}) collective-permute-start(bf16[192,2048]{1,0:T(8,128)(2,1)} %bitcast.14), channel_id=1, source_target_pairs={{0,16},{16,0},{32,48},{48,32},{64,80},{80,64},{96,112},{112,96},{1... | collective-permute-start | bytes 2359304 | tf_op jit(solution)/shard_map/ppermute | solution.py:357
  15.3 0.9 slice_bitcast_fusion
  16.1 0.7 collective-permute-start
  16.8 0.7 collective-permute-start.1
  17.5 0.8 constant_dynamic-slice_fusion.1
  18.2 0.3 copy.22
  18.6 0.1 copy.20
  18.7 0.7 dynamic-slice_bitcast_fusion
  19.4 0.1 copy.21.stride
  19.5 0.1 dynamic_slice.21
  19.6 0.1 dynamic_slice.22
  19.7 0.1 pad.15.w_step
  19.9 5.1 %collective-permute-done.2.other = bf16[192,2048]{1,0:T(8,128)(2,1)S(1)} collective-permute-done((bf16[192,2048]{1,0:T(8,128)(2,1)}, bf16[192,2048]{1,0:T(8,128)(2,1)S(1)}, u32[]{:S(2)}, u32[]{:S(2)}) %collective-permute-start.2) | collective-permute-done | bytes 786464 | tf_op jit(solution)/shard_map/ppermute | solution.py:357
  24.9 0.9 copy-done.12
  25.8 1.1 copy-done.10
  26.9 1.1 copy-done.13
  28.1 4.8 %maps.1 = (bf16[400,2048]{1,0:T(8,128)(2,1)S(1)}, bf16[128,384]{1,0:T(8,128)(2,1)S(1)}, bf16[384,128]{1,0:T(8,128)(2,1)S(1)}, bf16[8,384,384]{2,1,0:T(8,128)(2,1...) custom-call(s32[1]{0:T(128)} %bitcast.side, ...), custom_call_target="tpu_custom_call" | custom-call | flops 4026531840 | bytes 4194304 | tf_op jit(solution)/shard_map/maps/pallas_call | solution.py:292
  32.9 1.4 copy-done.1
  34.3 0.9 copy-done.3
  35.2 0.9 copy-done.4
  36.1 0.6 copy-done.7
  36.7 69.7 %all-gather.3.cloned.1.call-done = bf16[8192,512]{1,0:T(8,128)(2,1)} async-done(((bf16[512,512]{1,0:T(8,128)(2,1)}), bf16[8192,512]{1,0:T(8,128)(2,1)}) %all-gather.3.cloned.1.call-update) | async-done | bytes 8388624 | tf_op jit(solution)/shard_map/all_gather | solution.py:355
  106.4 3.1 %source.1 = (bf16[384,512]{1,0:T(8,128)(2,1)S(1)}, bf16[384,512]{1,0:T(8,128)(2,1)S(1)}, f32[128,512]{1,0:T(8,128)S(1)}, bf16[128,512]{1,0:T(8,128)(2,1)S(1)}) custom-call(s32[1]{0:T(128)} %bitcast.side, bf16[400,2048]{1,0:T(8,128)(2,1)S(1)} %get-tuple-element.33.rows, bf16[16,512,512]{2,1,0:T(8,128)(2,1)} %bitcast.17, f32[4,1024]{1,0:T(4,128)S(1)} %copy-done.9, ...), custom_call_target="tpu_custom_call" | custom-call | flops 805306368 | bytes 4194304 | tf_op jit(solution)/shard_map/source/pallas_call | solution.py:292
  109.6 0.0 copy-start.5
  109.6 4.4 %collective-permute-start.3 = (bf16[128,512]{1,0:T(8,128)(2,1)S(1)}, bf16[128,512]{1,0:T(8,128)(2,1)S(1)}, u32[]{:S(2)}, u32[]{:S(2)}) collective-permute-start(bf16[128,512]{1,0:T(8,128)(2,1)S(1)} %get-tuple-element.39), channel_id=1, source_target_pairs={{0,32},{16,48},{1,33},{17,49},{2,34},{18,50},{3,35},{19,51},{4,36}... | collective-permute-start | bytes 393224 | tf_op jit(solution)/shard_map/ppermute | solution.py:433
  114.0 2.6 %collective-permute-done.3.arrived = bf16[128,512]{1,0:T(8,128)(2,1)S(1)} collective-permute-done((bf16[128,512]{1,0:T(8,128)(2,1)S(1)}, bf16[128,512]{1,0:T(8,128)(2,1)S(1)}, u32[]{:S(2)}, u32[]{:S(2)}) %collective-permute-start.3) | collective-permute-done | bytes 131104 | tf_op jit(solution)/shard_map/ppermute | solution.py:433
  116.6 0.7 collective-permute-start.4
  117.4 0.7 collective-permute-start.5
  118.1 0.7 collective-permute-start.6
  118.9 0.7 collective-permute-start.7
  119.6 0.7 pass.10
  120.2 0.7 collective-permute-start.8
  120.9 0.1 dynamic_slice.26
  121.0 0.1 broadcast_in_dim.29
  121.1 0.1 broadcast_in_dim_reshape.3.skip
  121.2 0.0 copy-start.6
  121.2 0.8 collective-permute-start.9
  122.0 2.4 %gate.1 = f32[384,512]{1,0:T(8,128)S(1)} custom-call(bf16[400,2048]{1,0:T(8,128)(2,1)S(1)} %get-tuple-element.33.rows, bf16[16,512,512]{2,1,0:T(8,128)(2,1)} %bitcast.18), custom_call_target="tpu_custom_call" | custom-call | flops 805306368 | bytes 4194304 | tf_op jit(solution)/shard_map/gate/pallas_call | solution.py:292
  124.4 0.0 copy-start.11
  124.5 0.6 inner.1.base
  125.0 0.3 copy-done.8
  125.3 0.5 blend.1
  125.8 6.5 %collective-permute-start.10 = (bf16[192,512]{1,0:T(8,128)(2,1)S(1)}, bf16[192,512]{1,0:T(8,128)(2,1)S(1)}, u32[]{:S(2)}, u32[]{:S(2)}) collective-permute-start(bf16[192,512]{1,0:T(8,128)(2,1)S(1)} %get-tuple-element.55), channel_id=1, source_target_pairs={{0,16},{16,0},{32,48},{48,32},{64,80},{80,64},{96,112},{112,96},{1... | collective-permute-start | bytes 589832 | tf_op jit(solution)/shard_map/ppermute | solution.py:490
  132.3 2.4 %own_half.1 = (f32[192,2048]{1,0:T(8,128)S(1)}, bf16[16,256,256]{2,1,0:T(8,128)(2,1)S(1)}) custom-call(s32[1]{0:T(128)} %bitcast.side, bf16[192,512]{1,0:T(8,128)(2,1)S(1)} %get-tuple-element.56.kept, bf16[16,512,512]{2,1,0:T(8,128)(2,1)} %bitcast.19), custom_call_target="tpu_custom_call" | custom-call | flops 402653184 | bytes 4194304 | tf_op jit(solution)/shard_map/own_half/pallas_call | solution.py:292
  134.7 2.4 %collective-permute-done.10.arrived = bf16[192,512]{1,0:T(8,128)(2,1)S(1)} collective-permute-done((bf16[192,512]{1,0:T(8,128)(2,1)S(1)}, bf16[192,512]{1,0:T(8,128)(2,1)S(1)}, u32[]{:S(2)}, u32[]{:S(2)}) %collective-permute-start.10) | collective-permute-done | bytes 196640 | tf_op jit(solution)/shard_map/ppermute | solution.py:490
  137.1 1.3 output.1
  (45 shorter events, 0.4 us)
Async XLA Ops:
  6.5 12.0 %copy-start = (f32[1,3072,16]{1,2,0:T(8,128)S(1)}, f32[1,3072,16]{1,2,0:T(8,128)}, u32[]{:S(2)}) copy-start(f32[1,3072,16]{1,2,0:T(8,128)} %param.29) | copy-start | bytes 589828
  6.6 13.0 %copy-start.16 = (f32[16]{0:T(128)S(1)}, f32[16]{0:T(128)}, u32[]{:S(2)}) copy-start(f32[16]{0:T(128)} %param.25) | copy-start | bytes 196
  6.6 13.1 %copy-start.17 = (f32[16]{0:T(128)S(1)}, f32[16]{0:T(128)}, u32[]{:S(2)}) copy-start(f32[16]{0:T(128)} %param.26) | copy-start | bytes 196
  6.6 99.9 %all-gather.3.cloned.1.call-start = ((), (), s32[]{:S(2)}) async-start(), calls=%async_computation | async-start | bytes 8912896 | tf_op jit(solution)/shard_map/all_gather | solution.py:355
  6.6 19.2 %copy-start.14 = (f32[4,256]{1,0:T(4,128)S(1)}, f32[4,256]{1,0:T(4,128)}, u32[]{:S(2)}) copy-start(f32[4,256]{1,0:T(4,128)} %taps_in.1) | copy-start | bytes 12292
  6.6 19.2 %copy-start.15 = (f32[4,256]{1,0:T(4,128)S(1)}, f32[4,256]{1,0:T(4,128)}, u32[]{:S(2)}) copy-start(f32[4,256]{1,0:T(4,128)} %taps_out.1) | copy-start | bytes 12292
  8.7 16.2 %collective-permute-start.2 = (bf16[192,2048]{1,0:T(8,128)(2,1)}, bf16[192,2048]{1,0:T(8,128)(2,1)S(1)}, u32[]{:S(2)}, u32[]{:S(2)}) collective-permute-start(bf16[192,2048]{1,0:T(8,128)(2,1)} %bitcast.14), channel_id=1, source_target_pairs={{0,16},{16,0},{32,48},{48,32},{64,80},{80,64},{96,112},{112,96},{1... | collective-permute-start | bytes 2359304 | tf_op jit(solution)/shard_map/ppermute | solution.py:357
  16.1 3.7 %collective-permute-start = (bf16[16,2048]{1,0:T(8,128)(2,1)S(1)}, bf16[16,2048]{1,0:T(8,128)(2,1)S(1)}, u32[]{:S(2)}, u32[]{:S(2)}) collective-permute-start(bf16[16,2048]{1,0:T(8,128)(2,1)S(1)} %slice_bitcast_fusion), channel_id=1, source_target_pairs={{16,32},{48,64},{80,96},{112,128},{144,160},{176,192},{208,224},{1... | collective-permute-start | bytes 196616 | tf_op jit(solution)/shard_map/ppermute | solution.py:359
  16.8 3.1 %collective-permute-start.1 = (bf16[16,2048]{1,0:T(8,128)(2,1)S(1)}, bf16[16,2048]{1,0:T(8,128)(2,1)S(1)}, u32[]{:S(2)}, u32[]{:S(2)}) collective-permute-start(bf16[16,2048]{1,0:T(8,128)(2,1)S(1)} %slice_bitcast_fusion), channel_id=1, source_target_pairs={{16,48},{48,80},{80,112},{112,144},{144,176},{176,208},{208,240},{... | collective-permute-start | bytes 196616 | tf_op jit(solution)/shard_map/ppermute | solution.py:360
  24.9 0.9 copy-start.12
  25.8 1.1 copy-start.10
  26.9 1.1 copy-start.13
  28.1 78.3 %copy-start.9 = (f32[4,1024]{1,0:T(4,128)S(1)}, f32[4,1024]{1,0:T(4,128)}, u32[]{:S(2)}) copy-start(f32[4,1024]{1,0:T(4,128)} %taps.1) | copy-start | bytes 49156
  32.9 1.4 copy-start.1
  34.3 0.9 copy-start.3
  35.2 0.9 copy-start.4
  36.1 0.6 copy-start.7
  109.6 9.3 %copy-start.5 = (bf16[384,512]{1,0:T(8,128)(2,1)}, bf16[384,512]{1,0:T(8,128)(2,1)S(1)}, u32[]{:S(2)}) copy-start(bf16[384,512]{1,0:T(8,128)(2,1)S(1)} %get-tuple-element.53.scaled) | copy-start | bytes 1179652
  109.6 7.0 %collective-permute-start.3 = (bf16[128,512]{1,0:T(8,128)(2,1)S(1)}, bf16[128,512]{1,0:T(8,128)(2,1)S(1)}, u32[]{:S(2)}, u32[]{:S(2)}) collective-permute-start(bf16[128,512]{1,0:T(8,128)(2,1)S(1)} %get-tuple-element.39), channel_id=1, source_target_pairs={{0,32},{16,48},{1,33},{17,49},{2,34},{18,50},{3,35},{19,51},{4,36}... | collective-permute-start | bytes 393224 | tf_op jit(solution)/shard_map/ppermute | solution.py:433
  116.6 0.7 collective-permute-start.4
  117.4 3.5 %copy-start.18 = (f32[16]{0:T(128)S(1)}, f32[16]{0:T(128)}, u32[]{:S(2)}) copy-start(f32[16]{0:T(128)} %param.27) | copy-start | bytes 196
  117.4 0.7 collective-permute-start.5
  118.1 0.7 collective-permute-start.6
  118.9 0.7 collective-permute-start.7
  120.2 0.9 collective-permute-start.8
  121.2 3.2 %copy-start.2 = (bf16[8,384,384]{2,1,0:T(8,128)(2,1)S(1)}, bf16[8,384,384]{2,1,0:T(8,128)(2,1)}, u32[]{:S(2)}) copy-start(bf16[8,384,384]{2,1,0:T(8,128)(2,1)} %copy-done.1) | copy-start | bytes 7077892
  121.2 3.2 %copy-start.6 = (bf16[384,512]{1,0:T(8,128)(2,1)S(1)}, bf16[384,512]{1,0:T(8,128)(2,1)}, u32[]{:S(2)}) copy-start(bf16[384,512]{1,0:T(8,128)(2,1)} %copy-done.5) | copy-start | bytes 1179652
  121.2 3.8 %collective-permute-start.9 = (bf16[128,512]{1,0:T(8,128)(2,1)S(1)}, bf16[128,512]{1,0:T(8,128)(2,1)S(1)}, u32[]{:S(2)}, u32[]{:S(2)}) collective-permute-start(bf16[128,512]{1,0:T(8,128)(2,1)S(1)} %get-tuple-element.51), channel_id=1, source_target_pairs={{192,224},{208,240},{193,225},{209,241},{194,226},{210,242},{195,2... | collective-permute-start | bytes 393224 | tf_op jit(solution)/shard_map/ppermute | solution.py:433
  124.4 0.9 copy-start.8
  124.4 0.9 copy-start.11
  125.8 11.3 %collective-permute-start.10 = (bf16[192,512]{1,0:T(8,128)(2,1)S(1)}, bf16[192,512]{1,0:T(8,128)(2,1)S(1)}, u32[]{:S(2)}, u32[]{:S(2)}) collective-permute-start(bf16[192,512]{1,0:T(8,128)(2,1)S(1)} %get-tuple-element.55), channel_id=1, source_target_pairs={{0,16},{16,0},{32,48},{48,32},{64,80},{80,64},{96,112},{112,96},{1... | collective-permute-start | bytes 589832 | tf_op jit(solution)/shard_map/ppermute | solution.py:490
Sparse Core Ops, SparseCore 0:
  9.5 96.8 all-gather.2

commit v8 on v7

--- a/solution.py
+++ b/solution.py
@@ -189,6 +189,12 @@
             ].astype(F32)
 
 
+def first_pass_kernel(states, reach_wide, arrived, gate, base, passed):
+    length = reach_wide.shape[0]
+    decay = reach_wide[length - 1 : length, :]
+    passed[...] = (states[...] + decay * arrived[...].astype(F32)).astype(BF16)
+
+
 def pass_kernel(states, reach_wide, before, arrived, carried, passed):
     length = reach_wide.shape[0]
     entered = before[...] + arrived[...]
@@ -427,23 +433,6 @@
         scratch=[w_half, pltpu.VMEM(wide, F32), pltpu.VMEM(wide, F32), copies(4), copies(2)],
         limit=20,
     )
-    before = jnp.zeros(carry, BF16)
-    for k in range(sp // 2 - 1):
-        links = [(i, i + 2) for i in (2 * k, 2 * k + 1)]
-        arrived = lax.ppermute(passed, "sp", links)
-        if k < sp // 2 - 2:
-            before, passed = call(
-                pass_kernel,
-                (shape(carry, BF16), shape(carry, BF16)),
-                states,
-                reach_wide,
-                before,
-                arrived,
-                name="pass",
-                flops=1000,
-                ins=[K, K, V, V],
-                out_blocks=[V, V],
-            )
     gate = call(
         gate_kernel,
         held(wide),
@@ -470,6 +459,40 @@
         ins=[K, K, K, V],
         out_blocks=V,
     )
+    before = None
+    for k in range(sp // 2 - 1):
+        links = [(i, i + 2) for i in (2 * k, 2 * k + 1)]
+        arrived = lax.ppermute(passed, "sp", links)
+        if k == sp // 2 - 2:
+            break
+        if k == 0:
+            passed = call(
+                first_pass_kernel,
+                shape(carry, BF16),
+                states,
+                reach_wide,
+                arrived,
+                gate,
+                base,
+                name="first_pass",
+                flops=1000,
+                ins=[K, K, V, K, K],
+                out_blocks=V,
+            )
+            before = arrived
+        else:
+            before, passed = call(
+                pass_kernel,
+                (shape(carry, BF16), shape(carry, BF16)),
+                states,
+                reach_wide,
+                before,
+                arrived,
+                name="pass",
+                flops=1000,
+                ins=[K, K, V, V],
+                out_blocks=[V, V],
+            )
     kept, sent = call(
         blend_kernel,
         (held((part, width), BF16), shape((part, width), BF16)),

time: 146 us -> 143 us (0.979)
  waiting for transfers between devices: 79.9 us -> 77.7 us
    ppermute x7, waiting for transfers between devices: 2.62 us -> 0.02 us  [shards(): arrived = lax.ppermute(passed, 'sp', links)]
    unnamed x39 -> x31, local copies, waits for them, and re-layouts: 7.56 us -> 6.65 us
  transfers between devices with their start and end apart: 12 -> 12, of which waited for: 4 -> 3; matrix products, arithmetic and copies ran while one was open for 2% -> 2% of each run, Pallas kernels for 7% -> 7%
where the time goes in v8:
time: 143 us; the launch traced here: 141 us
  waiting for transfers between devices  77.7 us (54%)
  starting transfers between devices  22.6 us (16%)
  Pallas kernels  17.3 us (12%)
  between operations  13.9 us (10%)
  local copies, waits for them, and re-layouts  9.74 us (7%)
    all_gather x1, waiting for transfers between devices, shards(): w_all = lax.all_gather(picked, 'dp', axis=0, tiled=False)  70.4 us
    pallas_call x14, Pallas kernels, call(): pl.pallas_call(kernel, out_shape=outs, name=name, in_specs=ins, out_specs...  17.3 us
    ppermute x7, starting transfers between devices, shards(): arrived = lax.ppermute(passed, 'sp', links)  8.5 us
    unnamed x31, local copies, waits for them, and re-layouts  6.65 us
    ppermute x1, starting transfers between devices, shards(): other = lax.ppermute(own, 'sp', swap)  6.57 us
    ppermute x1, starting transfers between devices, shards(): arrived_half = lax.ppermute(sent, 'sp', swap)  6.15 us
    ppermute x1, waiting for transfers between devices, shards(): other = lax.ppermute(own, 'sp', swap)  4.84 us
  transfers between devices with their start and end apart: 12, of which 3 were waited for; matrix products, arithmetic and copies ran while one was open for 2% of the time, Pallas kernels for 7%

profile of v8, /device:TPU:65, one launch (start us, length us, event | category | flops | bytes accessed | tf_op | source)
XLA Modules:
  0.0 141.2 jit_solution(482973430083855999)
XLA Ops:
  6.6 0.1 all-gather.3.cloned.1.call-start
  6.7 2.0 %pick.1 = bf16[512,512]{1,0:T(8,128)(2,1)} custom-call(s32[1]{0:T(128)} %bitcast.side, bf16[128,1024]{1,0:T(8,128)(2,1)} %w_x.1, bf16[128,1024]{1,0:T(8,128)(2,1)} %w_z.1, bf16[1024,128]{1,0:T(8,128)(2,1)} %w_o.1), custom_call_target="tpu_custom_call" | custom-call | bytes 4194304 | tf_op jit(solution)/shard_map/pick/pallas_call | solution.py:298
  8.6 0.1 all-gather.3.cloned.1.call-update
  8.7 6.6 %collective-permute-start.2 = (bf16[192,2048]{1,0:T(8,128)(2,1)}, bf16[192,2048]{1,0:T(8,128)(2,1)S(1)}, u32[]{:S(2)}, u32[]{:S(2)}) collective-permute-start(bf16[192,2048]{1,0:T(8,128)(2,1)} %bitcast.14), channel_id=1, source_target_pairs={{0,16},{16,0},{32,48},{48,32},{64,80},{80,64},{96,112},{112,96},{1... | collective-permute-start | bytes 2359304 | tf_op jit(solution)/shard_map/ppermute | solution.py:363
  15.3 0.9 slice_bitcast_fusion
  16.1 0.7 collective-permute-start
  16.8 0.7 collective-permute-start.1
  17.5 0.8 constant_dynamic-slice_fusion.1
  18.3 0.3 copy.22
  18.6 0.1 copy.20
  18.7 0.7 dynamic-slice_bitcast_fusion
  19.4 0.1 copy.21.stride
  19.6 0.1 dynamic_slice.21
  19.6 0.1 dynamic_slice.22
  19.7 0.1 dynamic_slice.26
  19.8 0.1 broadcast_in_dim.25
  19.9 0.1 broadcast_in_dim_reshape.3.skip
  19.9 0.1 pad.15.w_step
  20.1 0.0 collective-permute-done.halo_a
  20.1 4.8 %collective-permute-done.2.other = bf16[192,2048]{1,0:T(8,128)(2,1)S(1)} collective-permute-done((bf16[192,2048]{1,0:T(8,128)(2,1)}, bf16[192,2048]{1,0:T(8,128)(2,1)S(1)}, u32[]{:S(2)}, u32[]{:S(2)}) %collective-permute-start.2) | collective-permute-done | bytes 786464 | tf_op jit(solution)/shard_map/ppermute | solution.py:363
  25.0 0.9 copy-done.8
  25.8 1.1 copy-done.6
  27.0 1.1 copy-done.9
  28.1 4.8 %maps.1 = (bf16[400,2048]{1,0:T(8,128)(2,1)S(1)}, bf16[128,384]{1,0:T(8,128)(2,1)S(1)}, bf16[384,128]{1,0:T(8,128)(2,1)S(1)}, bf16[8,384,384]{2,1,0:T(8,128)(2,1...) custom-call(s32[1]{0:T(128)} %bitcast.side, ...), custom_call_target="tpu_custom_call" | custom-call | flops 4026531840 | bytes 4194304 | tf_op jit(solution)/shard_map/maps/pallas_call | solution.py:298
  32.9 1.5 %copy-done.1 = bf16[8,384,384]{2,1,0:T(8,128)(2,1)} copy-done((bf16[8,384,384]{2,1,0:T(8,128)(2,1)}, bf16[8,384,384]{2,1,0:T(8,128)(2,1)S(1)}, u32[]{:S(2)}) %copy-start.1) | copy-done | bytes 2359320
  34.3 0.9 copy-done.3
  35.2 0.9 copy-done.4
  36.1 70.4 %all-gather.3.cloned.1.call-done = bf16[8192,512]{1,0:T(8,128)(2,1)} async-done(((bf16[512,512]{1,0:T(8,128)(2,1)}), bf16[8192,512]{1,0:T(8,128)(2,1)}) %all-gather.3.cloned.1.call-update) | async-done | bytes 8388624 | tf_op jit(solution)/shard_map/all_gather | solution.py:361
  106.5 3.1 %source.1 = (bf16[384,512]{1,0:T(8,128)(2,1)S(1)}, bf16[384,512]{1,0:T(8,128)(2,1)S(1)}, f32[128,512]{1,0:T(8,128)S(1)}, bf16[128,512]{1,0:T(8,128)(2,1)S(1)}) custom-call(s32[1]{0:T(128)} %bitcast.side, bf16[400,2048]{1,0:T(8,128)(2,1)S(1)} %get-tuple-element.31.rows, bf16[16,512,512]{2,1,0:T(8,128)(2,1)} %bitcast.17, f32[4,1024]{1,0:T(4,128)S(1)} %copy-done.5, ...), custom_call_target="tpu_custom_call" | custom-call | flops 805306368 | bytes 4194304 | tf_op jit(solution)/shard_map/source/pallas_call | solution.py:298
  109.6 4.5 %collective-permute-start.3 = (bf16[128,512]{1,0:T(8,128)(2,1)S(1)}, bf16[128,512]{1,0:T(8,128)(2,1)S(1)}, u32[]{:S(2)}, u32[]{:S(2)}) collective-permute-start(bf16[128,512]{1,0:T(8,128)(2,1)S(1)} %get-tuple-element.37), channel_id=1, source_target_pairs={{0,32},{16,48},{1,33},{17,49},{2,34},{18,50},{3,35},{19,51},{4,36}... | collective-permute-start | bytes 393224 | tf_op jit(solution)/shard_map/ppermute | solution.py:465
  114.1 2.4 %gate.1 = f32[384,512]{1,0:T(8,128)S(1)} custom-call(bf16[400,2048]{1,0:T(8,128)(2,1)S(1)} %get-tuple-element.31.rows, bf16[16,512,512]{2,1,0:T(8,128)(2,1)} %bitcast.18), custom_call_target="tpu_custom_call" | custom-call | flops 805306368 | bytes 4194304 | tf_op jit(solution)/shard_map/gate/pallas_call | solution.py:298
  116.5 0.6 inner.1.base
  117.2 0.7 collective-permute-start.4
  117.8 0.0 collective-permute-done.4.arrived
  117.9 0.7 collective-permute-start.5
  118.6 0.0 collective-permute-done.5.arrived
  118.6 0.0 copy-start.7
  118.6 0.7 collective-permute-start.6
  119.4 0.7 collective-permute-start.7
  120.1 0.7 collective-permute-start.8
  120.8 0.0 collective-permute-done.8.arrived
  120.9 0.7 collective-permute-start.9
  121.5 0.0 collective-permute-done.9.arrived
  121.6 0.5 blend.1
  122.1 6.2 %collective-permute-start.10 = (bf16[192,512]{1,0:T(8,128)(2,1)S(1)}, bf16[192,512]{1,0:T(8,128)(2,1)S(1)}, u32[]{:S(2)}, u32[]{:S(2)}) collective-permute-start(bf16[192,512]{1,0:T(8,128)(2,1)S(1)} %get-tuple-element.51), channel_id=1, source_target_pairs={{0,16},{16,0},{32,48},{48,32},{64,80},{80,64},{96,112},{112,96},{1... | collective-permute-start | bytes 589832 | tf_op jit(solution)/shard_map/ppermute | solution.py:513
  128.2 2.4 %own_half.1 = (f32[192,2048]{1,0:T(8,128)S(1)}, bf16[16,256,256]{2,1,0:T(8,128)(2,1)S(1)}) custom-call(s32[1]{0:T(128)} %bitcast.side, bf16[192,512]{1,0:T(8,128)(2,1)S(1)} %get-tuple-element.52.kept, bf16[16,512,512]{2,1,0:T(8,128)(2,1)} %bitcast.19), custom_call_target="tpu_custom_call" | custom-call | flops 402653184 | bytes 4194304 | tf_op jit(solution)/shard_map/own_half/pallas_call | solution.py:298
  130.6 2.4 %collective-permute-done.10.arrived = bf16[192,512]{1,0:T(8,128)(2,1)S(1)} collective-permute-done((bf16[192,512]{1,0:T(8,128)(2,1)S(1)}, bf16[192,512]{1,0:T(8,128)(2,1)S(1)}, u32[]{:S(2)}, u32[]{:S(2)}) %collective-permute-start.10) | collective-permute-done | bytes 196640 | tf_op jit(solution)/shard_map/ppermute | solution.py:513
  133.0 1.3 output.1
  (36 shorter events, 0.4 us)
Async XLA Ops:
  6.5 12.0 %copy-start = (f32[1,3072,16]{1,2,0:T(8,128)S(1)}, f32[1,3072,16]{1,2,0:T(8,128)}, u32[]{:S(2)}) copy-start(f32[1,3072,16]{1,2,0:T(8,128)} %param.29) | copy-start | bytes 589828
  6.6 13.0 %copy-start.12 = (f32[16]{0:T(128)S(1)}, f32[16]{0:T(128)}, u32[]{:S(2)}) copy-start(f32[16]{0:T(128)} %param.25) | copy-start | bytes 196
  6.6 13.1 %copy-start.13 = (f32[16]{0:T(128)S(1)}, f32[16]{0:T(128)}, u32[]{:S(2)}) copy-start(f32[16]{0:T(128)} %param.26) | copy-start | bytes 196
  6.6 13.2 %copy-start.14 = (f32[16]{0:T(128)S(1)}, f32[16]{0:T(128)}, u32[]{:S(2)}) copy-start(f32[16]{0:T(128)} %param.27) | copy-start | bytes 196
  6.6 99.9 %all-gather.3.cloned.1.call-start = ((), (), s32[]{:S(2)}) async-start(), calls=%async_computation | async-start | bytes 8912896 | tf_op jit(solution)/shard_map/all_gather | solution.py:361
  6.6 19.2 %copy-start.10 = (f32[4,256]{1,0:T(4,128)S(1)}, f32[4,256]{1,0:T(4,128)}, u32[]{:S(2)}) copy-start(f32[4,256]{1,0:T(4,128)} %taps_in.1) | copy-start | bytes 12292
  6.6 19.2 %copy-start.11 = (f32[4,256]{1,0:T(4,128)S(1)}, f32[4,256]{1,0:T(4,128)}, u32[]{:S(2)}) copy-start(f32[4,256]{1,0:T(4,128)} %taps_out.1) | copy-start | bytes 12292
  8.7 16.2 %collective-permute-start.2 = (bf16[192,2048]{1,0:T(8,128)(2,1)}, bf16[192,2048]{1,0:T(8,128)(2,1)S(1)}, u32[]{:S(2)}, u32[]{:S(2)}) collective-permute-start(bf16[192,2048]{1,0:T(8,128)(2,1)} %bitcast.14), channel_id=1, source_target_pairs={{0,16},{16,0},{32,48},{48,32},{64,80},{80,64},{96,112},{112,96},{1... | collective-permute-start | bytes 2359304 | tf_op jit(solution)/shard_map/ppermute | solution.py:363
  16.1 4.0 %collective-permute-start = (bf16[16,2048]{1,0:T(8,128)(2,1)S(1)}, bf16[16,2048]{1,0:T(8,128)(2,1)S(1)}, u32[]{:S(2)}, u32[]{:S(2)}) collective-permute-start(bf16[16,2048]{1,0:T(8,128)(2,1)S(1)} %slice_bitcast_fusion), channel_id=1, source_target_pairs={{16,32},{48,64},{80,96},{112,128},{144,160},{176,192},{208,224},{1... | collective-permute-start | bytes 196616 | tf_op jit(solution)/shard_map/ppermute | solution.py:365
  16.8 3.3 %collective-permute-start.1 = (bf16[16,2048]{1,0:T(8,128)(2,1)S(1)}, bf16[16,2048]{1,0:T(8,128)(2,1)S(1)}, u32[]{:S(2)}, u32[]{:S(2)}) collective-permute-start(bf16[16,2048]{1,0:T(8,128)(2,1)S(1)} %slice_bitcast_fusion), channel_id=1, source_target_pairs={{16,48},{48,80},{80,112},{112,144},{144,176},{176,208},{208,240},{... | collective-permute-start | bytes 196616 | tf_op jit(solution)/shard_map/ppermute | solution.py:366
  24.9 0.9 copy-start.8
  25.8 1.1 copy-start.6
  27.0 1.1 copy-start.9
  28.1 78.4 %copy-start.5 = (f32[4,1024]{1,0:T(4,128)S(1)}, f32[4,1024]{1,0:T(4,128)}, u32[]{:S(2)}) copy-start(f32[4,1024]{1,0:T(4,128)} %taps.1) | copy-start | bytes 49156
  32.9 1.5 %copy-start.1 = (bf16[8,384,384]{2,1,0:T(8,128)(2,1)}, bf16[8,384,384]{2,1,0:T(8,128)(2,1)S(1)}, u32[]{:S(2)}) copy-start(bf16[8,384,384]{2,1,0:T(8,128)(2,1)S(1)} %get-tuple-element.38.mixing) | copy-start | bytes 7077892
  34.3 0.9 copy-start.3
  35.2 0.9 copy-start.4
  109.6 6.9 %copy-start.2 = (bf16[8,384,384]{2,1,0:T(8,128)(2,1)S(1)}, bf16[8,384,384]{2,1,0:T(8,128)(2,1)}, u32[]{:S(2)}) copy-start(bf16[8,384,384]{2,1,0:T(8,128)(2,1)} %copy-done.1) | copy-start | bytes 7077892
  109.6 7.5 %collective-permute-start.3 = (bf16[128,512]{1,0:T(8,128)(2,1)S(1)}, bf16[128,512]{1,0:T(8,128)(2,1)S(1)}, u32[]{:S(2)}, u32[]{:S(2)}) collective-permute-start(bf16[128,512]{1,0:T(8,128)(2,1)S(1)} %get-tuple-element.37), channel_id=1, source_target_pairs={{0,32},{16,48},{1,33},{17,49},{2,34},{18,50},{3,35},{19,51},{4,36}... | collective-permute-start | bytes 393224 | tf_op jit(solution)/shard_map/ppermute | solution.py:465
  117.2 0.7 collective-permute-start.4
  117.9 0.7 collective-permute-start.5
  118.6 2.9 %copy-start.7 = (f32[1024]{0:T(1024)S(1)}, f32[1024]{0:T(1024)}, u32[]{:S(2)}) copy-start(f32[1024]{0:T(1024)} %param.30) | copy-start | bytes 12292
  118.6 0.7 collective-permute-start.6
  119.4 0.7 collective-permute-start.7
  120.1 0.7 collective-permute-start.8
  120.9 0.7 collective-permute-start.9
  122.1 11.0 %collective-permute-start.10 = (bf16[192,512]{1,0:T(8,128)(2,1)S(1)}, bf16[192,512]{1,0:T(8,128)(2,1)S(1)}, u32[]{:S(2)}, u32[]{:S(2)}) collective-permute-start(bf16[192,512]{1,0:T(8,128)(2,1)S(1)} %get-tuple-element.51), channel_id=1, source_target_pairs={{0,16},{16,0},{32,48},{48,32},{64,80},{80,64},{96,112},{112,96},{1... | collective-permute-start | bytes 589832 | tf_op jit(solution)/shard_map/ppermute | solution.py:513
Sparse Core Ops, SparseCore 0:
  9.5 96.8 all-gather.2

commit v9 on v8

--- a/solution.py
+++ b/solution.py
@@ -11,6 +11,7 @@
 G = 2
 CONV_W = 4
 HALO = 16
+SIDE_ROWS = 96
 LANES = 128
 EPSILON = 1e-06
 
@@ -50,10 +51,13 @@
         pltpu.make_async_copy(w.at[:, at], held_rows.at[pl.ds(k * rows, rows)], sem.at[k])
         for k, w in enumerate((w_x, w_z))
     ]
-    for b in range(w_o.shape[0] // tall):
+    group_rows = w_o.shape[0] // G
+    blocks = width // LANES
+    per = blocks // G
+    for b in range(blocks):
         arrive.append(
             pltpu.make_async_copy(
-                w_o.at[pl.ds(b * tall, tall)],
+                w_o.at[pl.ds(b // per * group_rows + b % per * tall, tall)],
                 held_rows.at[pl.ds(2 * rows, tall), pl.ds(b * LANES, LANES)],
                 sem.at[2 + b],
             )
@@ -151,7 +155,7 @@
 
 
 def source_kernel(
-    side, rows, w_xz, taps, step_all, end_all, in_t, xs_out, scaled_out, states, passed,
+    side, rows, w_xz, taps, step_all, end_all, in_t, w_side, xs_out, scaled_out, states, passed,
     w, step_wide, end_wide, sem, sem_wide,
 ):
     length, width = step_wide.shape
@@ -222,16 +226,19 @@
     kept[...] = normed[pl.ds(pl.multiple_of(side[0] * part, HALO), part), :]
 
 
-def joined(w, first, count):
+def joined(w, extra, first, count):
     tall = [
-        jnp.concatenate([w[d, :, :LANES], w[d, :, LANES:]], axis=0)
+        jnp.concatenate([w[d, :, :LANES], w[d, :, LANES:], extra[d]], axis=0)
         for d in range(first, first + count)
     ]
     return jnp.concatenate(tall, axis=1)
 
 
-def own_half_kernel(side, kept, w_all, partial, w_other, w, sem):
-    parts = sem.shape[0] - 1
+def own_half_kernel(
+    side, kept, w_all, w_side, partial, w_other, side_other, w, side_w, sem
+):
+    parts = sem.shape[0] - 3
+    extra = side_w.shape[1]
     count = w_all.shape[0] // parts
     tall, wide = w.shape[1:]
     low = pl.ds(w_all.shape[1] - tall, tall)
@@ -245,26 +252,34 @@
         )
         for p in range(parts)
     ]
-    copies.append(pltpu.make_async_copy(w_all.at[:, low, others], w_other, sem.at[parts]))
+    mine_low = pl.ds(pl.multiple_of(side[0] * extra, HALO), extra)
+    others_low = pl.ds(pl.multiple_of((1 - side[0]) * extra, HALO), extra)
+    copies.append(pltpu.make_async_copy(w_side.at[:, mine_low], side_w, sem.at[parts]))
+    copies.append(pltpu.make_async_copy(w_all.at[:, low, others], w_other, sem.at[parts + 1]))
+    copies.append(
+        pltpu.make_async_copy(w_side.at[:, others_low], side_other, sem.at[parts + 2])
+    )
     for c in copies:
         c.start()
+    copies[parts].wait()
     for p in range(parts):
         copies[p].wait()
         at = slice(p * count * LANES, (p + 1) * count * LANES)
         partial[:, at] = jnp.dot(
-            kept[...], joined(w, p * count, count), preferred_element_type=F32
+            kept[...], joined(w, side_w, p * count, count), preferred_element_type=F32
         )
-    copies[parts].wait()
-
-
-def output_kernel(arrived, partial, w_other, output, out, sem):
+    copies[parts + 1].wait()
+    copies[parts + 2].wait()
+
+
+def output_kernel(arrived, partial, w_other, side_other, output, out, sem):
     parts = sem.shape[0]
     count = w_other.shape[0] // parts
     outs = []
     for p in range(parts):
         at = pl.ds(p * count * LANES, count * LANES)
         half = jnp.dot(
-            arrived[...], joined(w_other, p * count, count), preferred_element_type=F32
+            arrived[...], joined(w_other, side_other, p * count, count), preferred_element_type=F32
         )
         out[:, at] = (partial[:, at] + half).astype(BF16)
         outs.append(pltpu.make_async_copy(out.at[:, at], output.at[:, at], sem.at[p]))
@@ -343,7 +358,8 @@
     swap = [(i, i ^ 1) for i in range(sp)]
 
     o_blocks = width // LANES
-    tall = final_projection.shape[0] // o_blocks
+    group_rows = final_projection.shape[0] // G
+    tall = (group_rows - SIDE_ROWS) * G // o_blocks
     all_rows = 2 * k_rows + tall
     picked = call(
         pick_kernel,
@@ -359,6 +375,9 @@
         scratch=[pltpu.VMEM((all_rows, width), BF16), copies(2 + o_blocks)],
     )
     w_all = lax.all_gather(picked, "dp", axis=0, tiled=False)
+    ends = [(g + 1) * group_rows for g in range(G)]
+    side_own = jnp.concatenate([final_projection[e - SIDE_ROWS : e] for e in ends], axis=0)
+    w_side = lax.all_gather(side_own, "dp", axis=0, tiled=False)
 
     other = lax.ppermute(own, "sp", swap)
     edge = own[part - HALO :]
@@ -426,9 +445,10 @@
         step_wide,
         end_wide,
         in_t,
+        w_side,
         name="source",
         flops=2 * length * d_model * width,
-        ins=[S, K, H, V, H, H, K],
+        ins=[S, K, H, V, H, H, K, H],
         out_blocks=[V, V, V, V],
         scratch=[w_half, pltpu.VMEM(wide, F32), pltpu.VMEM(wide, F32), copies(4), copies(2)],
         limit=20,
@@ -513,17 +533,19 @@
     arrived_half = lax.ppermute(sent, "sp", swap)
     out_dims = (part, dp * final_projection.shape[1])
     w_o_half = (dp, tall, width // G)
-    partial, w_other = call(
+    side_dims = (dp, SIDE_ROWS, final_projection.shape[1])
+    partial, w_other, side_other = call(
         own_half_kernel,
-        (held(out_dims), held(w_o_half, BF16)),
+        (held(out_dims), held(w_o_half, BF16), held(side_dims, BF16)),
         side,
         kept,
         w_all,
+        w_side,
         name="own_half",
         flops=2 * part * width * d_model,
-        ins=[S, K, H],
-        out_blocks=[V, V],
-        scratch=[pltpu.VMEM(w_o_half, BF16), copies(5)],
+        ins=[S, K, H, H],
+        out_blocks=[V, V, V],
+        scratch=[pltpu.VMEM(w_o_half, BF16), pltpu.VMEM(side_dims, BF16), copies(7)],
     )
     output = call(
         output_kernel,
@@ -531,9 +553,10 @@
         arrived_half,
         partial,
         w_other,
+        side_other,
         name="output",
         flops=2 * part * width * d_model,
-        ins=[V, K, K],
+        ins=[V, K, K, K],
         out_blocks=H,
         scratch=[pltpu.VMEM(out_dims, BF16), copies(4)],
     )

time: 143 us -> 140 us (0.979)
  waiting for transfers between devices: 77.7 us -> 19.5 us
  blocking collectives: 0 us -> 41.7 us
  starting transfers between devices: 22.6 us -> 35.9 us
    all_gather x1, waiting for transfers between devices: 70.4 us -> 17.4 us  [shards(): w_all = lax.all_gather(picked, 'dp', axis=0, tiled=False)]
    all_gather x0 -> x1, blocking collectives: none -> 41.7 us  [shards(): w_side = lax.all_gather(side_own, 'dp', axis=0, tiled=False)]
    ppermute x1, starting transfers between devices: 6.57 us -> 21.5 us  [shards(): other = lax.ppermute(own, 'sp', swap)]
    ppermute x1, waiting for transfers between devices: 4.84 us -> 0.01 us  [shards(): other = lax.ppermute(own, 'sp', swap)]
    ppermute x7, starting transfers between devices: 8.5 us -> 6.85 us  [shards(): arrived = lax.ppermute(passed, 'sp', links)]
    unnamed x31 -> x35, local copies, waits for them, and re-layouts: 6.65 us -> 6.67 us
  transfers between devices with their start and end apart: 12 -> 12, of which waited for: 3 -> 2; matrix products, arithmetic and copies ran while one was open for 2% -> 2% of each run, Pallas kernels for 7% -> 8%
where the time goes in v9:
time: 140 us; the launch traced here: 138 us
  blocking collectives  41.7 us (30%)
  starting transfers between devices  35.9 us (26%)
  waiting for transfers between devices  19.5 us (14%)
  Pallas kernels  17.5 us (12%)
  between operations  14 us (10%)
  local copies, waits for them, and re-layouts  8.92 us (6%)
    all_gather x1, blocking collectives, shards(): w_side = lax.all_gather(side_own, 'dp', axis=0, tiled=False)  41.7 us
    ppermute x1, starting transfers between devices, shards(): other = lax.ppermute(own, 'sp', swap)  21.5 us
    pallas_call x14, Pallas kernels, call(): pl.pallas_call(kernel, out_shape=outs, name=name, in_specs=ins, out_specs...  17.5 us
    all_gather x1, waiting for transfers between devices, shards(): w_all = lax.all_gather(picked, 'dp', axis=0, tiled=False)  17.4 us
    ppermute x7, starting transfers between devices, shards(): arrived = lax.ppermute(passed, 'sp', links)  6.85 us
    unnamed x35, local copies, waits for them, and re-layouts  6.67 us
    ppermute x1, starting transfers between devices, shards(): arrived_half = lax.ppermute(sent, 'sp', swap)  6.15 us
  transfers between devices with their start and end apart: 12, of which 2 were waited for; matrix products, arithmetic and copies ran while one was open for 2% of the time, Pallas kernels for 8%

profile of v9, /device:TPU:65, one launch (start us, length us, event | category | flops | bytes accessed | tf_op | source)
XLA Modules:
  0.0 137.5 jit_solution(16537594224581811765)
XLA Ops:
  6.6 0.1 all-gather.4.cloned.1.call-start
  6.7 1.9 %pick.1 = bf16[464,512]{1,0:T(8,128)(2,1)} custom-call(s32[1]{0:T(128)} %bitcast.side, bf16[128,1024]{1,0:T(8,128)(2,1)} %w_x.1, bf16[128,1024]{1,0:T(8,128)(2,1)} %w_z.1, bf16[1024,128]{1,0:T(8,128)(2,1)} %w_o.1), custom_call_target="tpu_custom_call" | custom-call | bytes 4194304 | tf_op jit(solution)/shard_map/pick/pallas_call | solution.py:313
  8.6 0.1 all-gather.4.cloned.1.call-update
  8.7 0.7 collective-permute-start
  9.4 0.7 collective-permute-start.1
  10.0 21.5 %collective-permute-start.2 = (bf16[192,2048]{1,0:T(8,128)(2,1)S(1)}, bf16[192,2048]{1,0:T(8,128)(2,1)S(1)}, u32[]{:S(2)}, u32[]{:S(2)}) collective-permute-start(bf16[192,2048]{1,0:T(8,128)(2,1)S(1)} %bitcast.15), channel_id=1, source_target_pairs={{0,16},{16,0},{32,48},{48,32},{64,80},{80,64},{96,112},{112,96},{1... | collective-permute-start | bytes 2359304 | tf_op jit(solution)/shard_map/ppermute | solution.py:382
  31.5 0.0 copy-start.11
  31.6 0.0 copy-start.12
  31.6 0.3 copy.22
  31.9 0.1 copy.20
  32.0 0.7 dynamic-slice_bitcast_fusion
  32.7 0.1 copy.21.stride
  32.9 0.1 dynamic_slice.21
  33.0 0.1 dynamic_slice.22
  33.0 0.1 dynamic_slice.26
  33.1 0.1 broadcast_in_dim.25
  33.2 0.1 broadcast_in_dim_reshape.3.skip
  33.3 0.1 pad.15.w_step
  33.4 0.8 fusion
  34.2 41.7 %all-gather.1 = bf16[3072,128]{1,0:T(8,128)(2,1)} all-gather(bf16[192,128]{1,0:T(8,128)(2,1)S(1)} %pad_maximum_fusion), channel_id=3, replica_groups=mesh['grp'=2,'sp'=16,'dp'=16] {'dp'}, dimensions={0}, use_global_device_ids=true | all-gather | bytes 835584 | tf_op jit(solution)/shard_map/all_gather | solution.py:380
  75.9 0.0 collective-permute-done.1.halo_b
  75.9 0.0 collective-permute-done.2.other
  75.9 0.0 copy-start.9
  75.9 0.9 copy-done.9
  76.8 1.1 copy-done.7
  77.9 1.1 copy-done.10
  79.0 4.8 %maps.1 = (bf16[400,2048]{1,0:T(8,128)(2,1)S(1)}, bf16[128,384]{1,0:T(8,128)(2,1)S(1)}, bf16[384,128]{1,0:T(8,128)(2,1)S(1)}, bf16[8,384,384]{2,1,0:T(8,128)(2,1...) custom-call(s32[1]{0:T(128)} %bitcast.side, ...), custom_call_target="tpu_custom_call" | custom-call | flops 4026531840 | bytes 4194304 | tf_op jit(solution)/shard_map/maps/pallas_call | solution.py:313
  83.8 1.5 %copy-done.1 = bf16[8,384,384]{2,1,0:T(8,128)(2,1)} copy-done((bf16[8,384,384]{2,1,0:T(8,128)(2,1)}, bf16[8,384,384]{2,1,0:T(8,128)(2,1)S(1)}, u32[]{:S(2)}) %copy-start.1) | copy-done | bytes 2359320
  85.3 0.9 copy-done.3
  86.2 0.9 copy-done.4
  87.1 17.4 %all-gather.4.cloned.1.call-done = bf16[7424,512]{1,0:T(8,128)(2,1)} async-done(((bf16[464,512]{1,0:T(8,128)(2,1)}), bf16[7424,512]{1,0:T(8,128)(2,1)}) %all-gather.4.cloned.1.call-update) | async-done | bytes 7602192 | tf_op jit(solution)/shard_map/all_gather | solution.py:377
  104.4 3.1 %source.1 = (bf16[384,512]{1,0:T(8,128)(2,1)S(1)}, bf16[384,512]{1,0:T(8,128)(2,1)S(1)}, f32[128,512]{1,0:T(8,128)S(1)}, bf16[128,512]{1,0:T(8,128)(2,1)S(1)}) custom-call(s32[1]{0:T(128)} %bitcast.side, bf16[400,2048]{1,0:T(8,128)(2,1)S(1)} %get-tuple-element.32.rows, bf16[16,464,512]{2,1,0:T(8,128)(2,1)} %bitcast.18, f32[4,1024]{1,0:T(4,128)S(1)} %copy-done.5, ...), custom_call_target="tpu_custom_call" | custom-call | flops 805306368 | bytes 4194304 | tf_op jit(solution)/shard_map/source/pallas_call | solution.py:313
  107.6 2.8 %collective-permute-start.3 = (bf16[128,512]{1,0:T(8,128)(2,1)S(1)}, bf16[128,512]{1,0:T(8,128)(2,1)S(1)}, u32[]{:S(2)}, u32[]{:S(2)}) collective-permute-start(bf16[128,512]{1,0:T(8,128)(2,1)S(1)} %get-tuple-element.38), channel_id=1, source_target_pairs={{0,32},{16,48},{1,33},{17,49},{2,34},{18,50},{3,35},{19,51},{4,36}... | collective-permute-start | bytes 393224 | tf_op jit(solution)/shard_map/ppermute | solution.py:485
  110.4 2.4 %gate.1 = f32[384,512]{1,0:T(8,128)S(1)} custom-call(bf16[400,2048]{1,0:T(8,128)(2,1)S(1)} %get-tuple-element.32.rows, bf16[16,464,512]{2,1,0:T(8,128)(2,1)} %bitcast.19), custom_call_target="tpu_custom_call" | custom-call | flops 805306368 | bytes 4194304 | tf_op jit(solution)/shard_map/gate/pallas_call | solution.py:313
  112.8 0.6 inner.1.base
  113.5 0.7 collective-permute-start.4
  114.1 0.0 collective-permute-done.4.arrived
  114.2 0.7 collective-permute-start.5
  114.9 0.7 collective-permute-start.6
  115.6 0.0 copy-start.8
  115.7 0.7 collective-permute-start.7
  116.4 0.7 collective-permute-start.8
  117.2 0.7 collective-permute-start.9
  117.9 0.5 blend.1
  118.4 6.2 %collective-permute-start.10 = (bf16[192,512]{1,0:T(8,128)(2,1)S(1)}, bf16[192,512]{1,0:T(8,128)(2,1)S(1)}, u32[]{:S(2)}, u32[]{:S(2)}) collective-permute-start(bf16[192,512]{1,0:T(8,128)(2,1)S(1)} %get-tuple-element.52), channel_id=1, source_target_pairs={{0,16},{16,0},{32,48},{48,32},{64,80},{80,64},{96,112},{112,96},{1... | collective-permute-start | bytes 589832 | tf_op jit(solution)/shard_map/ppermute | solution.py:533
  124.5 2.7 %own_half.1 = (f32[192,2048]{1,0:T(8,128)S(1)}, bf16[16,208,256]{2,1,0:T(8,128)(2,1)S(1)}, bf16[16,96,128]{2,1,0:T(8,128)(2,1)S(1)}) custom-call(s32[1]{0:T(128)} %bitcast.side, bf16[192,512]{1,0:T(8,128)(2,1)S(1)} %get-tuple-element.53.kept, bf16[16,464,512]{2,1,0:T(8,128)(2,1)} %bitcast.20, bf16[16,192,128]{2,1,0:T(8,128)(2,1)} %bitcast.22), custom_call_target="tpu_custom_call" | custom-call | flops 402653184 | bytes 4194304 | tf_op jit(solution)/shard_map/own_half/pallas_call | solution.py:313
  127.2 2.1 %collective-permute-done.10.arrived = bf16[192,512]{1,0:T(8,128)(2,1)S(1)} collective-permute-done((bf16[192,512]{1,0:T(8,128)(2,1)S(1)}, bf16[192,512]{1,0:T(8,128)(2,1)S(1)}, u32[]{:S(2)}, u32[]{:S(2)}) %collective-permute-start.10) | collective-permute-done | bytes 196640 | tf_op jit(solution)/shard_map/ppermute | solution.py:533
  129.3 1.3 output.1
  (43 shorter events, 0.4 us)
Async XLA Ops:
  6.5 25.3 %copy-start = (f32[1,3072,16]{1,2,0:T(8,128)S(1)}, f32[1,3072,16]{1,2,0:T(8,128)}, u32[]{:S(2)}) copy-start(f32[1,3072,16]{1,2,0:T(8,128)} %param.29) | copy-start | bytes 589828
  6.6 2.1 %copy-start.6 = (bf16[1,192,2048]{2,1,0:T(8,128)(2,1)S(1)}, bf16[1,192,2048]{2,1,0:T(8,128)(2,1)}, u32[]{:S(2)}) copy-start(bf16[1,192,2048]{2,1,0:T(8,128)(2,1)} %param.16) | copy-start | bytes 2359300
  6.6 25.0 %copy-start.13 = (bf16[2048,16]{0,1:T(8,128)(2,1)S(1)}, bf16[2048,16]{0,1:T(8,128)(2,1)}, u32[]{:S(2)}) copy-start(bf16[2048,16]{0,1:T(8,128)(2,1)} %param.21) | copy-start | bytes 196612
  6.6 26.3 %copy-start.14 = (f32[16]{0:T(128)S(1)}, f32[16]{0:T(128)}, u32[]{:S(2)}) copy-start(f32[16]{0:T(128)} %param.25) | copy-start | bytes 196
  6.6 26.4 %copy-start.15 = (f32[16]{0:T(128)S(1)}, f32[16]{0:T(128)}, u32[]{:S(2)}) copy-start(f32[16]{0:T(128)} %param.26) | copy-start | bytes 196
  6.6 26.5 %copy-start.16 = (f32[16]{0:T(128)S(1)}, f32[16]{0:T(128)}, u32[]{:S(2)}) copy-start(f32[16]{0:T(128)} %param.27) | copy-start | bytes 196
  6.6 97.8 %all-gather.4.cloned.1.call-start = ((), (), s32[]{:S(2)}) async-start(), calls=%async_computation | async-start | bytes 8077312 | tf_op jit(solution)/shard_map/all_gather | solution.py:377
  8.7 67.2 %collective-permute-start = (bf16[16,2048]{1,0:T(8,128)(2,1)S(1)}, bf16[16,2048]{1,0:T(8,128)(2,1)S(1)}, u32[]{:S(2)}, u32[]{:S(2)}) collective-permute-start(bf16[16,2048]{1,0:T(8,128)(2,1)S(1)} %slice_bitcast_fusion), channel_id=1, source_target_pairs={{16,32},{48,64},{80,96},{112,128},{144,160},{176,192},{208,224},{1... | collective-permute-start | bytes 196616 | tf_op jit(solution)/shard_map/ppermute | solution.py:384
  9.4 66.5 %collective-permute-start.1 = (bf16[16,2048]{1,0:T(8,128)(2,1)S(1)}, bf16[16,2048]{1,0:T(8,128)(2,1)S(1)}, u32[]{:S(2)}, u32[]{:S(2)}) collective-permute-start(bf16[16,2048]{1,0:T(8,128)(2,1)S(1)} %slice_bitcast_fusion), channel_id=1, source_target_pairs={{16,48},{48,80},{80,112},{112,144},{144,176},{176,208},{208,240},{... | collective-permute-start | bytes 196616 | tf_op jit(solution)/shard_map/ppermute | solution.py:385
  10.0 65.9 %collective-permute-start.2 = (bf16[192,2048]{1,0:T(8,128)(2,1)S(1)}, bf16[192,2048]{1,0:T(8,128)(2,1)S(1)}, u32[]{:S(2)}, u32[]{:S(2)}) collective-permute-start(bf16[192,2048]{1,0:T(8,128)(2,1)S(1)} %bitcast.15), channel_id=1, source_target_pairs={{0,16},{16,0},{32,48},{48,32},{64,80},{80,64},{96,112},{112,96},{1... | collective-permute-start | bytes 2359304 | tf_op jit(solution)/shard_map/ppermute | solution.py:382
  31.5 45.2 %copy-start.11 = (f32[4,256]{1,0:T(4,128)S(1)}, f32[4,256]{1,0:T(4,128)}, u32[]{:S(2)}) copy-start(f32[4,256]{1,0:T(4,128)} %taps_in.1) | copy-start | bytes 12292
  31.6 45.2 %copy-start.12 = (f32[4,256]{1,0:T(4,128)S(1)}, f32[4,256]{1,0:T(4,128)}, u32[]{:S(2)}) copy-start(f32[4,256]{1,0:T(4,128)} %taps_out.1) | copy-start | bytes 12292
  75.9 0.9 copy-start.9
  76.8 1.1 copy-start.7
  77.9 1.1 copy-start.10
  79.0 25.4 %copy-start.5 = (f32[4,1024]{1,0:T(4,128)S(1)}, f32[4,1024]{1,0:T(4,128)}, u32[]{:S(2)}) copy-start(f32[4,1024]{1,0:T(4,128)} %taps.1) | copy-start | bytes 49156
  83.8 1.5 %copy-start.1 = (bf16[8,384,384]{2,1,0:T(8,128)(2,1)}, bf16[8,384,384]{2,1,0:T(8,128)(2,1)S(1)}, u32[]{:S(2)}) copy-start(bf16[8,384,384]{2,1,0:T(8,128)(2,1)S(1)} %get-tuple-element.39.mixing) | copy-start | bytes 7077892
  85.3 0.9 copy-start.3
  86.2 0.9 copy-start.4
  107.6 5.2 %copy-start.2 = (bf16[8,384,384]{2,1,0:T(8,128)(2,1)S(1)}, bf16[8,384,384]{2,1,0:T(8,128)(2,1)}, u32[]{:S(2)}) copy-start(bf16[8,384,384]{2,1,0:T(8,128)(2,1)} %copy-done.1) | copy-start | bytes 7077892
  107.6 5.8 %collective-permute-start.3 = (bf16[128,512]{1,0:T(8,128)(2,1)S(1)}, bf16[128,512]{1,0:T(8,128)(2,1)S(1)}, u32[]{:S(2)}, u32[]{:S(2)}) collective-permute-start(bf16[128,512]{1,0:T(8,128)(2,1)S(1)} %get-tuple-element.38), channel_id=1, source_target_pairs={{0,32},{16,48},{1,33},{17,49},{2,34},{18,50},{3,35},{19,51},{4,36}... | collective-permute-start | bytes 393224 | tf_op jit(solution)/shard_map/ppermute | solution.py:485
  113.5 0.7 collective-permute-start.4
  114.2 0.7 collective-permute-start.5
  114.9 0.7 collective-permute-start.6
  115.6 2.2 %copy-start.8 = (f32[1024]{0:T(1024)S(1)}, f32[1024]{0:T(1024)}, u32[]{:S(2)}) copy-start(f32[1024]{0:T(1024)} %param.30) | copy-start | bytes 12292
  115.7 0.7 collective-permute-start.7
  116.4 0.7 collective-permute-start.8
  117.2 0.7 collective-permute-start.9
  118.4 11.0 %collective-permute-start.10 = (bf16[192,512]{1,0:T(8,128)(2,1)S(1)}, bf16[192,512]{1,0:T(8,128)(2,1)S(1)}, u32[]{:S(2)}, u32[]{:S(2)}) collective-permute-start(bf16[192,512]{1,0:T(8,128)(2,1)S(1)} %get-tuple-element.52), channel_id=1, source_target_pairs={{0,16},{16,0},{32,48},{48,32},{64,80},{80,64},{96,112},{112,96},{1... | collective-permute-start | bytes 589832 | tf_op jit(solution)/shard_map/ppermute | solution.py:533
Sparse Core Ops, SparseCore 0:
  9.5 94.8 all-gather.3

commit v10 on v9

--- a/solution.py
+++ b/solution.py
@@ -199,12 +199,10 @@
     passed[...] = (states[...] + decay * arrived[...].astype(F32)).astype(BF16)
 
 
-def pass_kernel(states, reach_wide, before, arrived, carried, passed):
+def pass_kernel(states, reach_wide, arrived, passed):
     length = reach_wide.shape[0]
-    entered = before[...] + arrived[...]
-    carried[...] = entered
     decay = reach_wide[length - 1 : length, :]
-    passed[...] = (states[...] + decay * entered.astype(F32)).astype(BF16)
+    passed[...] = (states[...] + decay * arrived[...].astype(F32)).astype(BF16)
 
 
 def gate_kernel(rows, w_xz, gate, w, sem):
@@ -212,10 +210,11 @@
 
 
 def blend_kernel(
-    side, out_maps, before, arrived, reach_wide, base, gate, gain, kept, sent, normed
+    side, out_maps, reach_wide, base, gate, gain, *rest
 ):
+    *hops, kept, sent, normed = rest
     part = kept.shape[0]
-    carried = before[...] + arrived[...]
+    carried = sum((h[...] for h in hops[1:]), hops[0][...])
     reached = jnp.dot(out_maps[...], carried, preferred_element_type=F32)
     mixed = (base[...] + reached * reach_wide[...]).astype(BF16).astype(F32)
     gated = mixed * gate[...]
@@ -479,54 +478,38 @@
         ins=[K, K, K, V],
         out_blocks=V,
     )
-    before = None
+    hops = []
     for k in range(sp // 2 - 1):
         links = [(i, i + 2) for i in (2 * k, 2 * k + 1)]
-        arrived = lax.ppermute(passed, "sp", links)
+        hops.append(lax.ppermute(passed, "sp", links))
         if k == sp // 2 - 2:
             break
-        if k == 0:
-            passed = call(
-                first_pass_kernel,
-                shape(carry, BF16),
-                states,
-                reach_wide,
-                arrived,
-                gate,
-                base,
-                name="first_pass",
-                flops=1000,
-                ins=[K, K, V, K, K],
-                out_blocks=V,
-            )
-            before = arrived
-        else:
-            before, passed = call(
-                pass_kernel,
-                (shape(carry, BF16), shape(carry, BF16)),
-                states,
-                reach_wide,
-                before,
-                arrived,
-                name="pass",
-                flops=1000,
-                ins=[K, K, V, V],
-                out_blocks=[V, V],
-            )
+        unread = (gate, base) if k == 0 else ()
+        passed = call(
+            pass_kernel if k else first_pass_kernel,
+            shape(carry, BF16),
+            states,
+            reach_wide,
+            hops[k],
+            *unread,
+            name="pass",
+            flops=1000,
+            ins=[K, K, V] + [K] * len(unread),
+            out_blocks=V,
+        )
     kept, sent = call(
         blend_kernel,
         (held((part, width), BF16), shape((part, width), BF16)),
         side,
         out_maps,
-        before,
-        arrived,
         reach_wide,
         base,
         gate,
         norm_scale_factor[None],
+        *hops,
         name="blend",
         flops=2 * length * N * width,
-        ins=[S, K, V, V, K, K, K, V],
+        ins=[S, K, K, K, K, V] + [V] * len(hops),
         out_blocks=[V, V],
         scratch=[pltpu.VMEM(wide, BF16)],
     )

time: 140 us -> 140 us (level)
  no operation moved by 1% of the time
where the time goes in v10:
time: 140 us; the launch traced here: 138 us
  blocking collectives  41.7 us (30%)
  starting transfers between devices  35.9 us (26%)
  waiting for transfers between devices  19.6 us (14%)
  Pallas kernels  17.5 us (12%)
  between operations  13.9 us (10%)
  local copies, waits for them, and re-layouts  8.9 us (6%)
    all_gather x1, blocking collectives, shards(): w_side = lax.all_gather(side_own, 'dp', axis=0, tiled=False)  41.7 us
    ppermute x1, starting transfers between devices, shards(): other = lax.ppermute(own, 'sp', swap)  21.5 us
    pallas_call x14, Pallas kernels, call(): pl.pallas_call(kernel, out_shape=outs, name=name, in_specs=ins, out_specs...  17.5 us
    all_gather x1, waiting for transfers between devices, shards(): w_all = lax.all_gather(picked, 'dp', axis=0, tiled=False)  17.4 us
    ppermute x7, starting transfers between devices, shards(): hops.append(lax.ppermute(passed, 'sp', links))  6.87 us
    unnamed x35, local copies, waits for them, and re-layouts  6.66 us
    ppermute x1, starting transfers between devices, shards(): arrived_half = lax.ppermute(sent, 'sp', swap)  6.16 us
  transfers between devices with their start and end apart: 12, of which 2 were waited for; matrix products, arithmetic and copies ran while one was open for 2% of the time, Pallas kernels for 8%

profile of v10, /device:TPU:65, one launch (start us, length us, event | category | flops | bytes accessed | tf_op | source)
XLA Modules:
  0.0 137.5 jit_solution(12065024722077363003)
XLA Ops:
  6.6 0.1 all-gather.4.cloned.1.call-start
  6.7 1.9 %pick.1 = bf16[464,512]{1,0:T(8,128)(2,1)} custom-call(s32[1]{0:T(128)} %bitcast.side, bf16[128,1024]{1,0:T(8,128)(2,1)} %w_x.1, bf16[128,1024]{1,0:T(8,128)(2,1)} %w_z.1, bf16[1024,128]{1,0:T(8,128)(2,1)} %w_o.1), custom_call_target="tpu_custom_call" | custom-call | bytes 4194304 | tf_op jit(solution)/shard_map/pick/pallas_call | solution.py:312
  8.6 0.1 all-gather.4.cloned.1.call-update
  8.7 0.7 collective-permute-start
  9.3 0.7 collective-permute-start.1
  10.0 21.5 %collective-permute-start.2 = (bf16[192,2048]{1,0:T(8,128)(2,1)S(1)}, bf16[192,2048]{1,0:T(8,128)(2,1)S(1)}, u32[]{:S(2)}, u32[]{:S(2)}) collective-permute-start(bf16[192,2048]{1,0:T(8,128)(2,1)S(1)} %bitcast.15), channel_id=1, source_target_pairs={{0,16},{16,0},{32,48},{48,32},{64,80},{80,64},{96,112},{112,96},{1... | collective-permute-start | bytes 2359304 | tf_op jit(solution)/shard_map/ppermute | solution.py:381
  31.5 0.0 copy-start.11
  31.5 0.0 copy-start.12
  31.6 0.3 copy.22
  31.8 0.1 dynamic_slice.22
  31.9 0.1 dynamic_slice.21
  32.0 0.7 dynamic-slice_bitcast_fusion
  32.7 0.1 copy.21.stride
  32.9 0.1 copy.20
  33.0 0.1 dynamic_slice.26
  33.1 0.1 broadcast_in_dim.25
  33.2 0.1 broadcast_in_dim_reshape.3.skip
  33.2 0.1 pad.15.w_step
  33.4 0.8 fusion
  34.1 41.7 %all-gather.1 = bf16[3072,128]{1,0:T(8,128)(2,1)} all-gather(bf16[192,128]{1,0:T(8,128)(2,1)S(1)} %pad_maximum_fusion), channel_id=3, replica_groups=mesh['grp'=2,'sp'=16,'dp'=16] {'dp'}, dimensions={0}, use_global_device_ids=true | all-gather | bytes 835584 | tf_op jit(solution)/shard_map/all_gather | solution.py:379
  75.8 0.0 collective-permute-done.halo_a
  75.9 0.0 collective-permute-done.1.halo_b
  75.9 0.0 collective-permute-done.2.other
  75.9 0.0 copy-start.9
  75.9 0.9 copy-done.9
  76.8 1.1 copy-done.7
  77.9 1.1 copy-done.10
  79.0 4.8 %maps.1 = (bf16[400,2048]{1,0:T(8,128)(2,1)S(1)}, bf16[128,384]{1,0:T(8,128)(2,1)S(1)}, bf16[384,128]{1,0:T(8,128)(2,1)S(1)}, bf16[8,384,384]{2,1,0:T(8,128)(2,1...) custom-call(s32[1]{0:T(128)} %bitcast.side, ...), custom_call_target="tpu_custom_call" | custom-call | flops 4026531840 | bytes 4194304 | tf_op jit(solution)/shard_map/maps/pallas_call | solution.py:312
  83.8 1.5 %copy-done.1 = bf16[8,384,384]{2,1,0:T(8,128)(2,1)} copy-done((bf16[8,384,384]{2,1,0:T(8,128)(2,1)}, bf16[8,384,384]{2,1,0:T(8,128)(2,1)S(1)}, u32[]{:S(2)}) %copy-start.1) | copy-done | bytes 2359320
  85.3 0.9 copy-done.3
  86.2 0.9 copy-done.4
  87.0 17.4 %all-gather.4.cloned.1.call-done = bf16[7424,512]{1,0:T(8,128)(2,1)} async-done(((bf16[464,512]{1,0:T(8,128)(2,1)}), bf16[7424,512]{1,0:T(8,128)(2,1)}) %all-gather.4.cloned.1.call-update) | async-done | bytes 7602192 | tf_op jit(solution)/shard_map/all_gather | solution.py:376
  104.4 3.1 %source.1 = (bf16[384,512]{1,0:T(8,128)(2,1)S(1)}, bf16[384,512]{1,0:T(8,128)(2,1)S(1)}, f32[128,512]{1,0:T(8,128)S(1)}, bf16[128,512]{1,0:T(8,128)(2,1)S(1)}) custom-call(s32[1]{0:T(128)} %bitcast.side, bf16[400,2048]{1,0:T(8,128)(2,1)S(1)} %get-tuple-element.24.rows, bf16[16,464,512]{2,1,0:T(8,128)(2,1)} %bitcast.18, f32[4,1024]{1,0:T(4,128)S(1)} %copy-done.5, ...), custom_call_target="tpu_custom_call" | custom-call | flops 805306368 | bytes 4194304 | tf_op jit(solution)/shard_map/source/pallas_call | solution.py:312
  107.6 2.9 %collective-permute-start.3 = (bf16[128,512]{1,0:T(8,128)(2,1)S(1)}, bf16[128,512]{1,0:T(8,128)(2,1)S(1)}, u32[]{:S(2)}, u32[]{:S(2)}) collective-permute-start(bf16[128,512]{1,0:T(8,128)(2,1)S(1)} %get-tuple-element.30), channel_id=1, source_target_pairs={{0,32},{16,48},{1,33},{17,49},{2,34},{18,50},{3,35},{19,51},{4,36}... | collective-permute-start | bytes 393224 | tf_op jit(solution)/shard_map/ppermute | solution.py:484
  110.4 2.4 %gate.1 = f32[384,512]{1,0:T(8,128)S(1)} custom-call(bf16[400,2048]{1,0:T(8,128)(2,1)S(1)} %get-tuple-element.24.rows, bf16[16,464,512]{2,1,0:T(8,128)(2,1)} %bitcast.19), custom_call_target="tpu_custom_call" | custom-call | flops 805306368 | bytes 4194304 | tf_op jit(solution)/shard_map/gate/pallas_call | solution.py:312
  112.8 0.6 inner.1.base
  113.5 0.7 collective-permute-start.4
  114.2 0.7 collective-permute-start.5
  114.9 0.0 copy-start.8
  114.9 0.7 collective-permute-start.6
  115.7 0.7 collective-permute-start.7
  116.4 0.7 collective-permute-start.8
  117.1 0.7 collective-permute-start.9
  117.8 0.5 blend.1
  118.4 6.2 %collective-permute-start.10 = (bf16[192,512]{1,0:T(8,128)(2,1)S(1)}, bf16[192,512]{1,0:T(8,128)(2,1)S(1)}, u32[]{:S(2)}, u32[]{:S(2)}) collective-permute-start(bf16[192,512]{1,0:T(8,128)(2,1)S(1)} %get-tuple-element.32), channel_id=1, source_target_pairs={{0,16},{16,0},{32,48},{48,32},{64,80},{80,64},{96,112},{112,96},{1... | collective-permute-start | bytes 589832 | tf_op jit(solution)/shard_map/ppermute | solution.py:516
  124.5 2.7 %own_half.1 = (f32[192,2048]{1,0:T(8,128)S(1)}, bf16[16,208,256]{2,1,0:T(8,128)(2,1)S(1)}, bf16[16,96,128]{2,1,0:T(8,128)(2,1)S(1)}) custom-call(s32[1]{0:T(128)} %bitcast.side, bf16[192,512]{1,0:T(8,128)(2,1)S(1)} %get-tuple-element.33.kept, bf16[16,464,512]{2,1,0:T(8,128)(2,1)} %bitcast.20, bf16[16,192,128]{2,1,0:T(8,128)(2,1)} %bitcast.22), custom_call_target="tpu_custom_call" | custom-call | flops 402653184 | bytes 4194304 | tf_op jit(solution)/shard_map/own_half/pallas_call | solution.py:312
  127.2 2.1 %collective-permute-done.10.arrived = bf16[192,512]{1,0:T(8,128)(2,1)S(1)} collective-permute-done((bf16[192,512]{1,0:T(8,128)(2,1)S(1)}, bf16[192,512]{1,0:T(8,128)(2,1)S(1)}, u32[]{:S(2)}, u32[]{:S(2)}) %collective-permute-start.10) | collective-permute-done | bytes 196640 | tf_op jit(solution)/shard_map/ppermute | solution.py:516
  129.3 1.3 output.1
  (43 shorter events, 0.3 us)
Async XLA Ops:
  6.5 26.3 %copy-start = (f32[1,3072,16]{1,2,0:T(8,128)S(1)}, f32[1,3072,16]{1,2,0:T(8,128)}, u32[]{:S(2)}) copy-start(f32[1,3072,16]{1,2,0:T(8,128)} %param.29) | copy-start | bytes 589828
  6.6 2.1 %copy-start.6 = (bf16[1,192,2048]{2,1,0:T(8,128)(2,1)S(1)}, bf16[1,192,2048]{2,1,0:T(8,128)(2,1)}, u32[]{:S(2)}) copy-start(bf16[1,192,2048]{2,1,0:T(8,128)(2,1)} %param.16) | copy-start | bytes 2359300
  6.6 25.0 %copy-start.13 = (bf16[2048,16]{0,1:T(8,128)(2,1)S(1)}, bf16[2048,16]{0,1:T(8,128)(2,1)}, u32[]{:S(2)}) copy-start(bf16[2048,16]{0,1:T(8,128)(2,1)} %param.21) | copy-start | bytes 196612
  6.6 25.3 %copy-start.14 = (f32[16]{0:T(128)S(1)}, f32[16]{0:T(128)}, u32[]{:S(2)}) copy-start(f32[16]{0:T(128)} %param.26) | copy-start | bytes 196
  6.6 25.4 %copy-start.15 = (f32[16]{0:T(128)S(1)}, f32[16]{0:T(128)}, u32[]{:S(2)}) copy-start(f32[16]{0:T(128)} %param.25) | copy-start | bytes 196
  6.6 26.4 %copy-start.16 = (f32[16]{0:T(128)S(1)}, f32[16]{0:T(128)}, u32[]{:S(2)}) copy-start(f32[16]{0:T(128)} %param.27) | copy-start | bytes 196
  6.6 97.8 %all-gather.4.cloned.1.call-start = ((), (), s32[]{:S(2)}) async-start(), calls=%async_computation | async-start | bytes 8077312 | tf_op jit(solution)/shard_map/all_gather | solution.py:376
  8.7 67.2 %collective-permute-start = (bf16[16,2048]{1,0:T(8,128)(2,1)S(1)}, bf16[16,2048]{1,0:T(8,128)(2,1)S(1)}, u32[]{:S(2)}, u32[]{:S(2)}) collective-permute-start(bf16[16,2048]{1,0:T(8,128)(2,1)S(1)} %slice_bitcast_fusion), channel_id=1, source_target_pairs={{16,32},{48,64},{80,96},{112,128},{144,160},{176,192},{208,224},{1... | collective-permute-start | bytes 196616 | tf_op jit(solution)/shard_map/ppermute | solution.py:383
  9.3 66.5 %collective-permute-start.1 = (bf16[16,2048]{1,0:T(8,128)(2,1)S(1)}, bf16[16,2048]{1,0:T(8,128)(2,1)S(1)}, u32[]{:S(2)}, u32[]{:S(2)}) collective-permute-start(bf16[16,2048]{1,0:T(8,128)(2,1)S(1)} %slice_bitcast_fusion), channel_id=1, source_target_pairs={{16,48},{48,80},{80,112},{112,144},{144,176},{176,208},{208,240},{... | collective-permute-start | bytes 196616 | tf_op jit(solution)/shard_map/ppermute | solution.py:384
  10.0 65.9 %collective-permute-start.2 = (bf16[192,2048]{1,0:T(8,128)(2,1)S(1)}, bf16[192,2048]{1,0:T(8,128)(2,1)S(1)}, u32[]{:S(2)}, u32[]{:S(2)}) collective-permute-start(bf16[192,2048]{1,0:T(8,128)(2,1)S(1)} %bitcast.15), channel_id=1, source_target_pairs={{0,16},{16,0},{32,48},{48,32},{64,80},{80,64},{96,112},{112,96},{1... | collective-permute-start | bytes 2359304 | tf_op jit(solution)/shard_map/ppermute | solution.py:381
  31.5 45.2 %copy-start.11 = (f32[4,256]{1,0:T(4,128)S(1)}, f32[4,256]{1,0:T(4,128)}, u32[]{:S(2)}) copy-start(f32[4,256]{1,0:T(4,128)} %taps_in.1) | copy-start | bytes 12292
  31.5 45.2 %copy-start.12 = (f32[4,256]{1,0:T(4,128)S(1)}, f32[4,256]{1,0:T(4,128)}, u32[]{:S(2)}) copy-start(f32[4,256]{1,0:T(4,128)} %taps_out.1) | copy-start | bytes 12292
  75.9 0.9 copy-start.9
  76.8 1.1 copy-start.7
  77.9 1.1 copy-start.10
  79.0 25.4 %copy-start.5 = (f32[4,1024]{1,0:T(4,128)S(1)}, f32[4,1024]{1,0:T(4,128)}, u32[]{:S(2)}) copy-start(f32[4,1024]{1,0:T(4,128)} %taps.1) | copy-start | bytes 49156
  83.8 1.5 %copy-start.1 = (bf16[8,384,384]{2,1,0:T(8,128)(2,1)}, bf16[8,384,384]{2,1,0:T(8,128)(2,1)S(1)}, u32[]{:S(2)}) copy-start(bf16[8,384,384]{2,1,0:T(8,128)(2,1)S(1)} %get-tuple-element.23.mixing) | copy-start | bytes 7077892
  85.3 0.9 copy-start.3
  86.2 0.9 copy-start.4
  107.5 5.3 %copy-start.2 = (bf16[8,384,384]{2,1,0:T(8,128)(2,1)S(1)}, bf16[8,384,384]{2,1,0:T(8,128)(2,1)}, u32[]{:S(2)}) copy-start(bf16[8,384,384]{2,1,0:T(8,128)(2,1)} %copy-done.1) | copy-start | bytes 7077892
  107.6 5.9 %collective-permute-start.3 = (bf16[128,512]{1,0:T(8,128)(2,1)S(1)}, bf16[128,512]{1,0:T(8,128)(2,1)S(1)}, u32[]{:S(2)}, u32[]{:S(2)}) collective-permute-start(bf16[128,512]{1,0:T(8,128)(2,1)S(1)} %get-tuple-element.30), channel_id=1, source_target_pairs={{0,32},{16,48},{1,33},{17,49},{2,34},{18,50},{3,35},{19,51},{4,36}... | collective-permute-start | bytes 393224 | tf_op jit(solution)/shard_map/ppermute | solution.py:484
  113.5 0.7 collective-permute-start.4
  114.2 0.7 collective-permute-start.5
  114.9 2.9 %copy-start.8 = (f32[1024]{0:T(1024)S(1)}, f32[1024]{0:T(1024)}, u32[]{:S(2)}) copy-start(f32[1024]{0:T(1024)} %param.30) | copy-start | bytes 12292
  114.9 0.7 collective-permute-start.6
  115.7 0.7 collective-permute-start.7
  116.4 0.7 collective-permute-start.8
  117.1 0.7 collective-permute-start.9
  118.4 11.0 %collective-permute-start.10 = (bf16[192,512]{1,0:T(8,128)(2,1)S(1)}, bf16[192,512]{1,0:T(8,128)(2,1)S(1)}, u32[]{:S(2)}, u32[]{:S(2)}) collective-permute-start(bf16[192,512]{1,0:T(8,128)(2,1)S(1)} %get-tuple-element.32), channel_id=1, source_target_pairs={{0,16},{16,0},{32,48},{48,32},{64,80},{80,64},{96,112},{112,96},{1... | collective-permute-start | bytes 589832 | tf_op jit(solution)/shard_map/ppermute | solution.py:516
Sparse Core Ops, SparseCore 0:
  9.5 94.8 all-gather.3

commit v11 on v9

--- a/solution.py
+++ b/solution.py
@@ -155,14 +155,11 @@
 
 
 def source_kernel(
-    side, rows, w_xz, taps, step_all, end_all, in_t, w_side, xs_out, scaled_out, states, passed,
-    w, step_wide, end_wide, sem, sem_wide,
+    side, rows, w_xz, taps, end_all, in_t, w_side, xs_out, states, passed,
+    w, end_wide, sem, sem_wide,
 ):
-    length, width = step_wide.shape
-    wides = [
-        pltpu.make_async_copy(src, dst, sem_wide.at[k])
-        for k, (src, dst) in enumerate(((end_all, end_wide), (step_all, step_wide)))
-    ]
+    width = end_wide.shape[1]
+    wides = [pltpu.make_async_copy(end_all, end_wide, sem_wide.at[0])]
     raw = streamed_dot(rows, 0, w_xz, 0, w, sem, wides)
     group = pl.ds(pl.multiple_of(side[0] * width, LANES), width)
     xs = conv_silu(raw, taps[:, group]).astype(BF16)
@@ -173,19 +170,18 @@
     state = jnp.dot(in_t[...], weighted, preferred_element_type=F32)
     states[...] = state
     passed[...] = state.astype(BF16)
-    wides[1].wait()
-    scaled_out[...] = (xs * step_wide[...]).astype(BF16)
-
-
-def inner_kernel(mixing, scaled, xs, skip, base):
-    length = scaled.shape[0]
+
+
+def inner_kernel(mixing, step_wide, xs, skip, base):
+    length = xs.shape[0]
     lane = lax.broadcasted_iota(jnp.int32, (LANES, LANES), 1)
-    for pair in range(scaled.shape[1] // LANES):
+    for pair in range(xs.shape[1] // LANES):
         at = slice(pair * LANES, (pair + 1) * LANES)
+        scaled = (xs[:, at].astype(F32) * step_wide[:, at]).astype(BF16)
         for i in range(length // LANES):
             to = slice(i * LANES, (i + 1) * LANES)
             seen = (i + 1) * LANES
-            both = scaled[:seen, at]
+            both = scaled[:seen, :]
             first = jnp.dot(mixing[2 * pair, to, :seen], both, preferred_element_type=F32)
             second = jnp.dot(mixing[2 * pair + 1, to, :seen], both, preferred_element_type=F32)
             base[to, at] = jnp.where(lane < P_SIZE, first, second) + skip[:, at] * xs[
@@ -404,7 +400,7 @@
         held((N, length), BF16),
         held((length, N), BF16),
         held((heads, length, length), BF16),
-        shape(wide),
+        held(wide),
         shape(wide),
         held(wide),
     )
@@ -435,22 +431,21 @@
 
     w_half = pltpu.VMEM((dp, k_rows, width), BF16)
     carry = (N, width)
-    xs, scaled, states, passed = call(
+    xs, states, passed = call(
         source_kernel,
-        (held(wide, BF16), held(wide, BF16), held(carry), shape(carry, BF16)),
+        (held(wide, BF16), held(carry), shape(carry, BF16)),
         side,
         rows,
         w_all,
         source_conv_taps,
-        step_wide,
         end_wide,
         in_t,
         w_side,
         name="source",
         flops=2 * length * d_model * width,
-        ins=[S, K, H, V, H, H, K, H],
-        out_blocks=[V, V, V, V],
-        scratch=[w_half, pltpu.VMEM(wide, F32), pltpu.VMEM(wide, F32), copies(4), copies(2)],
+        ins=[S, K, H, V, H, K, H],
+        out_blocks=[V, V, V],
+        scratch=[w_half, pltpu.VMEM(wide, F32), copies(4), copies(1)],
         limit=20,
     )
     gate = call(
@@ -471,7 +466,7 @@
         inner_kernel,
         held(wide),
         mixing,
-        scaled,
+        step_wide,
         xs,
         skip_wide,
         name="inner",

time: 140 us -> 140 us (level)
  local copies, waits for them, and re-layouts: 8.92 us -> 12.3 us
  waiting for transfers between devices: 19.5 us -> 16.8 us
    all_gather x1, waiting for transfers between devices: 17.4 us -> 14.6 us  [shards(): w_all = lax.all_gather(picked, 'dp', axis=0, tiled=False)]
    unnamed x35 -> x47, local copies, waits for them, and re-layouts: 6.67 us -> 9.38 us
where the time goes in v11:
time: 140 us; the launch traced here: 137 us
  blocking collectives  41.6 us (30%)
  starting transfers between devices  35.4 us (25%)
  Pallas kernels  17.5 us (12%)
  waiting for transfers between devices  16.8 us (12%)
  between operations  13.9 us (10%)
  local copies, waits for them, and re-layouts  12.3 us (9%)
    all_gather x1, blocking collectives, shards(): w_side = lax.all_gather(side_own, 'dp', axis=0, tiled=False)  41.6 us
    ppermute x1, starting transfers between devices, shards(): other = lax.ppermute(own, 'sp', swap)  21.5 us
    pallas_call x14, Pallas kernels, call(): pl.pallas_call(kernel, out_shape=outs, name=name, in_specs=ins, out_specs...  17.5 us
    all_gather x1, waiting for transfers between devices, shards(): w_all = lax.all_gather(picked, 'dp', axis=0, tiled=False)  14.6 us
    unnamed x47, local copies, waits for them, and re-layouts  9.38 us
    ppermute x7, starting transfers between devices, shards(): arrived = lax.ppermute(passed, 'sp', links)  6.39 us
    ppermute x1, starting transfers between devices, shards(): arrived_half = lax.ppermute(sent, 'sp', swap)  6.15 us
  transfers between devices with their start and end apart: 12, of which 2 were waited for; matrix products, arithmetic and copies ran while one was open for 2% of the time, Pallas kernels for 8%

profile of v11, /device:TPU:65, one launch (start us, length us, event | category | flops | bytes accessed | tf_op | source)
XLA Modules:
  0.0 137.5 jit_solution(17319759098635901845)
XLA Ops:
  6.6 0.1 all-gather.4.cloned.1.call-start
  6.7 1.9 %pick.1 = bf16[464,512]{1,0:T(8,128)(2,1)} custom-call(s32[1]{0:T(128)} %bitcast.side, bf16[128,1024]{1,0:T(8,128)(2,1)} %w_x.1, bf16[128,1024]{1,0:T(8,128)(2,1)} %w_z.1, bf16[1024,128]{1,0:T(8,128)(2,1)} %w_o.1), custom_call_target="tpu_custom_call" | custom-call | bytes 4194304 | tf_op jit(solution)/shard_map/pick/pallas_call | solution.py:309
  8.6 0.1 all-gather.4.cloned.1.call-update
  8.7 0.7 collective-permute-start
  9.3 0.7 collective-permute-start.1
  10.0 21.5 %collective-permute-start.2 = (bf16[192,2048]{1,0:T(8,128)(2,1)S(1)}, bf16[192,2048]{1,0:T(8,128)(2,1)S(1)}, u32[]{:S(2)}, u32[]{:S(2)}) collective-permute-start(bf16[192,2048]{1,0:T(8,128)(2,1)S(1)} %bitcast.15), channel_id=1, source_target_pairs={{0,16},{16,0},{32,48},{48,32},{64,80},{80,64},{96,112},{112,96},{1... | collective-permute-start | bytes 2359304 | tf_op jit(solution)/shard_map/ppermute | solution.py:378
  31.5 0.0 copy-start.17
  31.5 0.0 copy-start.18
  31.5 0.3 copy.22
  31.9 0.1 copy.20
  32.0 0.7 dynamic-slice_bitcast_fusion
  32.7 0.8 copy.21.stride
  33.5 0.1 dynamic_slice.21
  33.6 0.1 dynamic_slice.22
  33.7 0.1 dynamic_slice.26
  33.8 0.1 broadcast_in_dim.25
  33.8 0.1 broadcast_in_dim_reshape.3.skip
  33.9 0.1 pad.15.w_step
  34.1 0.8 fusion
  34.8 41.6 %all-gather.1 = bf16[3072,128]{1,0:T(8,128)(2,1)} all-gather(bf16[192,128]{1,0:T(8,128)(2,1)S(1)} %pad_maximum_fusion), channel_id=3, replica_groups=mesh['grp'=2,'sp'=16,'dp'=16] {'dp'}, dimensions={0}, use_global_device_ids=true | all-gather | bytes 835584 | tf_op jit(solution)/shard_map/all_gather | solution.py:376
  76.4 0.6 copy-done.13
  77.0 0.6 copy-done.15
  77.6 0.9 copy-done.11
  78.5 1.1 copy-done.9
  79.7 1.1 copy-done.12
  80.8 0.8 copy-done.14
  81.6 0.9 copy-done.16
  82.5 4.8 %maps.1 = (bf16[400,2048]{1,0:T(8,128)(2,1)S(1)}, bf16[128,384]{1,0:T(8,128)(2,1)S(1)}, bf16[384,128]{1,0:T(8,128)(2,1)S(1)}, bf16[8,384,384]{2,1,0:T(8,128)(2,1...) custom-call(s32[1]{0:T(128)} %bitcast.side, bf16[16,2048]{1,0:T(8,128)(2,1)S(1)} %copy-done.14, ...), custom_call_target="tpu_custom_call" | custom-call | flops 4026531840 | bytes 4194304 | tf_op jit(solution)/shard_map/maps/pallas_call | solution.py:309
  87.3 1.5 %copy-done.1 = bf16[8,384,384]{2,1,0:T(8,128)(2,1)} copy-done((bf16[8,384,384]{2,1,0:T(8,128)(2,1)}, bf16[8,384,384]{2,1,0:T(8,128)(2,1)S(1)}, u32[]{:S(2)}) %copy-start.1) | copy-done | bytes 2359320
  88.8 0.9 copy-done.3
  89.6 0.6 copy-done.5
  90.3 14.6 %all-gather.4.cloned.1.call-done = bf16[7424,512]{1,0:T(8,128)(2,1)} async-done(((bf16[464,512]{1,0:T(8,128)(2,1)}), bf16[7424,512]{1,0:T(8,128)(2,1)}) %all-gather.4.cloned.1.call-update) | async-done | bytes 7602192 | tf_op jit(solution)/shard_map/all_gather | solution.py:373
  104.9 3.1 %source.1 = (bf16[384,512]{1,0:T(8,128)(2,1)S(1)}, f32[128,512]{1,0:T(8,128)S(1)}, bf16[128,512]{1,0:T(8,128)(2,1)S(1)}) custom-call(s32[1]{0:T(128)} %bitcast.side, bf16[400,2048]{1,0:T(8,128)(2,1)S(1)} %get-tuple-element.31.rows, bf16[16,464,512]{2,1,0:T(8,128)(2,1)} %bitcast.18, f32[4,1024]{1,0:T(4,128)S(1)} %copy-done.7, f32[384,512]{1,0:T(8,128)} %copy-done.3, ...), custom_call_target="tpu_custom_call" | custom-call | flops 805306368 | bytes 4194304 | tf_op jit(solution)/shard_map/source/pallas_call | solution.py:309
  108.0 2.4 %collective-permute-start.3 = (bf16[128,512]{1,0:T(8,128)(2,1)S(1)}, bf16[128,512]{1,0:T(8,128)(2,1)S(1)}, u32[]{:S(2)}, u32[]{:S(2)}) collective-permute-start(bf16[128,512]{1,0:T(8,128)(2,1)S(1)} %get-tuple-element.36), channel_id=1, source_target_pairs={{0,32},{16,48},{1,33},{17,49},{2,34},{18,50},{3,35},{19,51},{4,36}... | collective-permute-start | bytes 393224 | tf_op jit(solution)/shard_map/ppermute | solution.py:480
  110.4 2.4 %gate.1 = f32[384,512]{1,0:T(8,128)S(1)} custom-call(bf16[400,2048]{1,0:T(8,128)(2,1)S(1)} %get-tuple-element.31.rows, bf16[16,464,512]{2,1,0:T(8,128)(2,1)} %bitcast.19), custom_call_target="tpu_custom_call" | custom-call | flops 805306368 | bytes 4194304 | tf_op jit(solution)/shard_map/gate/pallas_call | solution.py:309
  112.7 0.6 inner.1.base
  113.4 0.7 collective-permute-start.4
  114.1 0.7 collective-permute-start.5
  114.9 0.7 collective-permute-start.6
  115.6 0.0 copy-start.10
  115.6 0.7 collective-permute-start.7
  116.4 0.7 collective-permute-start.8
  117.1 0.7 collective-permute-start.9
  117.8 0.5 blend.1
  118.3 6.2 %collective-permute-start.10 = (bf16[192,512]{1,0:T(8,128)(2,1)S(1)}, bf16[192,512]{1,0:T(8,128)(2,1)S(1)}, u32[]{:S(2)}, u32[]{:S(2)}) collective-permute-start(bf16[192,512]{1,0:T(8,128)(2,1)S(1)} %get-tuple-element.50), channel_id=1, source_target_pairs={{0,16},{16,0},{32,48},{48,32},{64,80},{80,64},{96,112},{112,96},{1... | collective-permute-start | bytes 589832 | tf_op jit(solution)/shard_map/ppermute | solution.py:528
  124.5 2.7 %own_half.1 = (f32[192,2048]{1,0:T(8,128)S(1)}, bf16[16,208,256]{2,1,0:T(8,128)(2,1)S(1)}, bf16[16,96,128]{2,1,0:T(8,128)(2,1)S(1)}) custom-call(s32[1]{0:T(128)} %bitcast.side, bf16[192,512]{1,0:T(8,128)(2,1)S(1)} %get-tuple-element.51.kept, bf16[16,464,512]{2,1,0:T(8,128)(2,1)} %bitcast.20, bf16[16,192,128]{2,1,0:T(8,128)(2,1)} %bitcast.22), custom_call_target="tpu_custom_call" | custom-call | flops 402653184 | bytes 4194304 | tf_op jit(solution)/shard_map/own_half/pallas_call | solution.py:309
  127.2 2.1 %collective-permute-done.10.arrived = bf16[192,512]{1,0:T(8,128)(2,1)S(1)} collective-permute-done((bf16[192,512]{1,0:T(8,128)(2,1)S(1)}, bf16[192,512]{1,0:T(8,128)(2,1)S(1)}, u32[]{:S(2)}, u32[]{:S(2)}) %collective-permute-start.10) | collective-permute-done | bytes 196640 | tf_op jit(solution)/shard_map/ppermute | solution.py:528
  129.3 1.3 output.1
  (55 shorter events, 0.4 us)
Async XLA Ops:
  6.5 25.3 %copy-start = (f32[1,3072,16]{1,2,0:T(8,128)S(1)}, f32[1,3072,16]{1,2,0:T(8,128)}, u32[]{:S(2)}) copy-start(f32[1,3072,16]{1,2,0:T(8,128)} %param.29) | copy-start | bytes 589828
  6.6 2.1 %copy-start.8 = (bf16[1,192,2048]{2,1,0:T(8,128)(2,1)S(1)}, bf16[1,192,2048]{2,1,0:T(8,128)(2,1)}, u32[]{:S(2)}) copy-start(bf16[1,192,2048]{2,1,0:T(8,128)(2,1)} %param.16) | copy-start | bytes 2359300
  6.6 24.9 %copy-start.19 = (bf16[2048,16]{0,1:T(8,128)(2,1)S(1)}, bf16[2048,16]{0,1:T(8,128)(2,1)}, u32[]{:S(2)}) copy-start(bf16[2048,16]{0,1:T(8,128)(2,1)} %param.21) | copy-start | bytes 196612
  6.6 27.0 %copy-start.20 = (f32[16]{0:T(128)S(1)}, f32[16]{0:T(128)}, u32[]{:S(2)}) copy-start(f32[16]{0:T(128)} %param.25) | copy-start | bytes 196
  6.6 27.1 %copy-start.21 = (f32[16]{0:T(128)S(1)}, f32[16]{0:T(128)}, u32[]{:S(2)}) copy-start(f32[16]{0:T(128)} %param.26) | copy-start | bytes 196
  6.6 27.1 %copy-start.22 = (f32[16]{0:T(128)S(1)}, f32[16]{0:T(128)}, u32[]{:S(2)}) copy-start(f32[16]{0:T(128)} %param.27) | copy-start | bytes 196
  6.6 98.3 %all-gather.4.cloned.1.call-start = ((), (), s32[]{:S(2)}) async-start(), calls=%async_computation | async-start | bytes 8077312 | tf_op jit(solution)/shard_map/all_gather | solution.py:373
  8.7 67.7 %collective-permute-start = (bf16[16,2048]{1,0:T(8,128)(2,1)S(1)}, bf16[16,2048]{1,0:T(8,128)(2,1)S(1)}, u32[]{:S(2)}, u32[]{:S(2)}) collective-permute-start(bf16[16,2048]{1,0:T(8,128)(2,1)S(1)} %slice_bitcast_fusion), channel_id=1, source_target_pairs={{16,32},{48,64},{80,96},{112,128},{144,160},{176,192},{208,224},{1... | collective-permute-start | bytes 196616 | tf_op jit(solution)/shard_map/ppermute | solution.py:380
  9.3 67.7 %collective-permute-start.1 = (bf16[16,2048]{1,0:T(8,128)(2,1)S(1)}, bf16[16,2048]{1,0:T(8,128)(2,1)S(1)}, u32[]{:S(2)}, u32[]{:S(2)}) collective-permute-start(bf16[16,2048]{1,0:T(8,128)(2,1)S(1)} %slice_bitcast_fusion), channel_id=1, source_target_pairs={{16,48},{48,80},{80,112},{112,144},{144,176},{176,208},{208,240},{... | collective-permute-start | bytes 196616 | tf_op jit(solution)/shard_map/ppermute | solution.py:381
  10.0 67.6 %collective-permute-start.2 = (bf16[192,2048]{1,0:T(8,128)(2,1)S(1)}, bf16[192,2048]{1,0:T(8,128)(2,1)S(1)}, u32[]{:S(2)}, u32[]{:S(2)}) collective-permute-start(bf16[192,2048]{1,0:T(8,128)(2,1)S(1)} %bitcast.15), channel_id=1, source_target_pairs={{0,16},{16,0},{32,48},{48,32},{64,80},{80,64},{96,112},{112,96},{1... | collective-permute-start | bytes 2359304 | tf_op jit(solution)/shard_map/ppermute | solution.py:378
  31.5 47.0 %copy-start.17 = (f32[4,256]{1,0:T(4,128)S(1)}, f32[4,256]{1,0:T(4,128)}, u32[]{:S(2)}) copy-start(f32[4,256]{1,0:T(4,128)} %taps_in.1) | copy-start | bytes 12292
  31.5 47.0 %copy-start.18 = (f32[4,256]{1,0:T(4,128)S(1)}, f32[4,256]{1,0:T(4,128)}, u32[]{:S(2)}) copy-start(f32[4,256]{1,0:T(4,128)} %taps_out.1) | copy-start | bytes 12292
  33.9 44.6 %copy-start.4 = (f32[384,1]{1,0:T(8,128)S(1)}, f32[384,1]{1,0:T(8,128)}, u32[]{:S(2)}) copy-start(f32[384,1]{1,0:T(8,128)} %copy.21.stride) | copy-start | bytes 4612
  76.4 0.6 copy-start.13
  77.0 0.6 copy-start.15
  77.6 0.9 copy-start.11
  78.5 1.1 copy-start.9
  79.7 1.1 copy-start.12
  80.8 0.8 copy-start.14
  81.6 0.9 copy-start.16
  82.5 22.4 %copy-start.7 = (f32[4,1024]{1,0:T(4,128)S(1)}, f32[4,1024]{1,0:T(4,128)}, u32[]{:S(2)}) copy-start(f32[4,1024]{1,0:T(4,128)} %taps.1) | copy-start | bytes 49156
  87.3 1.5 %copy-start.1 = (bf16[8,384,384]{2,1,0:T(8,128)(2,1)}, bf16[8,384,384]{2,1,0:T(8,128)(2,1)S(1)}, u32[]{:S(2)}) copy-start(bf16[8,384,384]{2,1,0:T(8,128)(2,1)S(1)} %get-tuple-element.37.mixing) | copy-start | bytes 7077892
  88.8 0.9 copy-start.3
  89.6 0.6 copy-start.5
  108.0 4.8 %copy-start.2 = (bf16[8,384,384]{2,1,0:T(8,128)(2,1)S(1)}, bf16[8,384,384]{2,1,0:T(8,128)(2,1)}, u32[]{:S(2)}) copy-start(bf16[8,384,384]{2,1,0:T(8,128)(2,1)} %copy-done.1) | copy-start | bytes 7077892
  108.0 5.4 %collective-permute-start.3 = (bf16[128,512]{1,0:T(8,128)(2,1)S(1)}, bf16[128,512]{1,0:T(8,128)(2,1)S(1)}, u32[]{:S(2)}, u32[]{:S(2)}) collective-permute-start(bf16[128,512]{1,0:T(8,128)(2,1)S(1)} %get-tuple-element.36), channel_id=1, source_target_pairs={{0,32},{16,48},{1,33},{17,49},{2,34},{18,50},{3,35},{19,51},{4,36}... | collective-permute-start | bytes 393224 | tf_op jit(solution)/shard_map/ppermute | solution.py:480
  113.4 0.7 collective-permute-start.4
  114.1 0.7 collective-permute-start.5
  114.9 0.7 collective-permute-start.6
  115.6 2.2 %copy-start.6 = (bf16[384,128]{1,0:T(8,128)(2,1)S(1)}, bf16[384,128]{1,0:T(8,128)(2,1)}, u32[]{:S(2)}) copy-start(bf16[384,128]{1,0:T(8,128)(2,1)} %copy-done.5) | copy-start | bytes 294916
  115.6 2.2 %copy-start.10 = (f32[1024]{0:T(1024)S(1)}, f32[1024]{0:T(1024)}, u32[]{:S(2)}) copy-start(f32[1024]{0:T(1024)} %param.30) | copy-start | bytes 12292
  115.6 0.7 collective-permute-start.7
  116.4 0.7 collective-permute-start.8
  117.1 0.7 collective-permute-start.9
  118.3 11.0 %collective-permute-start.10 = (bf16[192,512]{1,0:T(8,128)(2,1)S(1)}, bf16[192,512]{1,0:T(8,128)(2,1)S(1)}, u32[]{:S(2)}, u32[]{:S(2)}) collective-permute-start(bf16[192,512]{1,0:T(8,128)(2,1)S(1)} %get-tuple-element.50), channel_id=1, source_target_pairs={{0,16},{16,0},{32,48},{48,32},{64,80},{80,64},{96,112},{112,96},{1... | collective-permute-start | bytes 589832 | tf_op jit(solution)/shard_map/ppermute | solution.py:528
Sparse Core Ops, SparseCore 0:
  9.5 95.2 all-gather.3

commit v12 on v9

--- a/solution.py
+++ b/solution.py
@@ -42,13 +42,13 @@
     )
 
 
-def pick_kernel(side, w_x, w_z, w_o, picked, held_rows, sem):
+def pick_kernel(side, w_x, w_z, w_o, picked, held_rows, sem, sem_out):
     rows = w_x.shape[0]
     width = picked.shape[1]
     tall = picked.shape[0] - 2 * rows
-    at = pl.ds(pl.multiple_of(side[0] * width, LANES), width)
+    own = pl.ds(pl.multiple_of(side[0] * width, LANES), width)
     arrive = [
-        pltpu.make_async_copy(w.at[:, at], held_rows.at[pl.ds(k * rows, rows)], sem.at[k])
+        pltpu.make_async_copy(w.at[:, own], held_rows.at[pl.ds(k * rows, rows)], sem.at[k])
         for k, w in enumerate((w_x, w_z))
     ]
     group_rows = w_o.shape[0] // G
@@ -64,11 +64,21 @@
         )
     for c in arrive:
         c.start()
-    for c in arrive:
+    spans = ((0, rows, 1), (rows, rows, 1), (2 * rows, tall, blocks))
+    leave = [
+        pltpu.make_async_copy(
+            held_rows.at[pl.ds(at, size)], picked.at[pl.ds(at, size)], sem_out.at[k]
+        )
+        for k, (at, size, _) in enumerate(spans)
+    ]
+    done = 0
+    for (_, _, count), c in zip(spans, leave, strict=True):
+        for k in range(count):
+            arrive[done + k].wait()
+        done += count
+        c.start()
+    for c in leave:
         c.wait()
-    leave = pltpu.make_async_copy(held_rows, picked, sem.at[0])
-    leave.start()
-    leave.wait()
 
 
 def maps_kernel(
@@ -372,7 +382,7 @@
         flops=0,
         ins=[S, H, H, H],
         out_blocks=H,
-        scratch=[pltpu.VMEM((all_rows, width), BF16), copies(2 + o_blocks)],
+        scratch=[pltpu.VMEM((all_rows, width), BF16), copies(2 + o_blocks), copies(3)],
     )
     w_all = lax.all_gather(picked, "dp", axis=0, tiled=False)
     ends = [(g + 1) * group_rows for g in range(G)]

time: 140 us -> 140 us (level)
  no operation moved by 1% of the time
where the time goes in v12:
time: 140 us; the launch traced here: 138 us
  blocking collectives  41.7 us (30%)
  starting transfers between devices  35.9 us (26%)
  waiting for transfers between devices  19.5 us (14%)
  Pallas kernels  17.5 us (12%)
  between operations  14 us (10%)
  local copies, waits for them, and re-layouts  8.92 us (6%)
    all_gather x1, blocking collectives, shards(): w_side = lax.all_gather(side_own, 'dp', axis=0, tiled=False)  41.7 us
    ppermute x1, starting transfers between devices, shards(): other = lax.ppermute(own, 'sp', swap)  21.5 us
    pallas_call x14, Pallas kernels, call(): pl.pallas_call(kernel, out_shape=outs, name=name, in_specs=ins, out_specs...  17.5 us
    all_gather x1, waiting for transfers between devices, shards(): w_all = lax.all_gather(picked, 'dp', axis=0, tiled=False)  17.3 us
    ppermute x7, starting transfers between devices, shards(): arrived = lax.ppermute(passed, 'sp', links)  6.92 us
    unnamed x35, local copies, waits for them, and re-layouts  6.67 us
    ppermute x1, starting transfers between devices, shards(): arrived_half = lax.ppermute(sent, 'sp', swap)  6.15 us
  transfers between devices with their start and end apart: 12, of which 2 were waited for; matrix products, arithmetic and copies ran while one was open for 2% of the time, Pallas kernels for 8%

profile of v12, /device:TPU:65, one launch (start us, length us, event | category | flops | bytes accessed | tf_op | source)
XLA Modules:
  0.0 137.5 jit_solution(9086124499032780479)
XLA Ops:
  6.6 0.1 all-gather.4.cloned.1.call-start
  6.7 1.9 %pick.1 = bf16[464,512]{1,0:T(8,128)(2,1)} custom-call(s32[1]{0:T(128)} %bitcast.side, bf16[128,1024]{1,0:T(8,128)(2,1)} %w_x.1, bf16[128,1024]{1,0:T(8,128)(2,1)} %w_z.1, bf16[1024,128]{1,0:T(8,128)(2,1)} %w_o.1), custom_call_target="tpu_custom_call" | custom-call | bytes 4194304 | tf_op jit(solution)/shard_map/pick/pallas_call | solution.py:323
  8.5 0.1 all-gather.4.cloned.1.call-update
  8.6 0.7 collective-permute-start
  9.3 0.7 collective-permute-start.1
  10.0 21.5 %collective-permute-start.2 = (bf16[192,2048]{1,0:T(8,128)(2,1)S(1)}, bf16[192,2048]{1,0:T(8,128)(2,1)S(1)}, u32[]{:S(2)}, u32[]{:S(2)}) collective-permute-start(bf16[192,2048]{1,0:T(8,128)(2,1)S(1)} %bitcast.15), channel_id=1, source_target_pairs={{0,16},{16,0},{32,48},{48,32},{64,80},{80,64},{96,112},{112,96},{1... | collective-permute-start | bytes 2359304 | tf_op jit(solution)/shard_map/ppermute | solution.py:392
  31.5 0.0 copy-start.11
  31.5 0.0 copy-start.12
  31.5 0.3 copy.22
  31.8 0.1 copy.20
  32.0 0.7 dynamic-slice_bitcast_fusion
  32.6 0.1 copy.21.stride
  32.8 0.1 dynamic_slice.21
  32.9 0.1 dynamic_slice.22
  33.0 0.1 dynamic_slice.26
  33.0 0.1 broadcast_in_dim.25
  33.1 0.1 broadcast_in_dim_reshape.3.skip
  33.2 0.1 pad.15.w_step
  33.3 0.8 fusion
  34.1 41.7 %all-gather.1 = bf16[3072,128]{1,0:T(8,128)(2,1)} all-gather(bf16[192,128]{1,0:T(8,128)(2,1)S(1)} %pad_maximum_fusion), channel_id=3, replica_groups=mesh['grp'=2,'sp'=16,'dp'=16] {'dp'}, dimensions={0}, use_global_device_ids=true | all-gather | bytes 835584 | tf_op jit(solution)/shard_map/all_gather | solution.py:390
  75.8 0.0 collective-permute-done.halo_a
  75.9 0.0 collective-permute-done.2.other
  75.9 0.0 copy-start.9
  75.9 0.9 copy-done.9
  76.8 1.1 copy-done.7
  77.9 1.1 copy-done.10
  79.0 4.8 %maps.1 = (bf16[400,2048]{1,0:T(8,128)(2,1)S(1)}, bf16[128,384]{1,0:T(8,128)(2,1)S(1)}, bf16[384,128]{1,0:T(8,128)(2,1)S(1)}, bf16[8,384,384]{2,1,0:T(8,128)(2,1...) custom-call(s32[1]{0:T(128)} %bitcast.side, ...), custom_call_target="tpu_custom_call" | custom-call | flops 4026531840 | bytes 4194304 | tf_op jit(solution)/shard_map/maps/pallas_call | solution.py:323
  83.8 1.5 %copy-done.1 = bf16[8,384,384]{2,1,0:T(8,128)(2,1)} copy-done((bf16[8,384,384]{2,1,0:T(8,128)(2,1)}, bf16[8,384,384]{2,1,0:T(8,128)(2,1)S(1)}, u32[]{:S(2)}) %copy-start.1) | copy-done | bytes 2359320
  85.3 0.9 copy-done.3
  86.1 0.9 copy-done.4
  87.0 17.3 %all-gather.4.cloned.1.call-done = bf16[7424,512]{1,0:T(8,128)(2,1)} async-done(((bf16[464,512]{1,0:T(8,128)(2,1)}), bf16[7424,512]{1,0:T(8,128)(2,1)}) %all-gather.4.cloned.1.call-update) | async-done | bytes 7602192 | tf_op jit(solution)/shard_map/all_gather | solution.py:387
  104.4 3.1 %source.1 = (bf16[384,512]{1,0:T(8,128)(2,1)S(1)}, bf16[384,512]{1,0:T(8,128)(2,1)S(1)}, f32[128,512]{1,0:T(8,128)S(1)}, bf16[128,512]{1,0:T(8,128)(2,1)S(1)}) custom-call(s32[1]{0:T(128)} %bitcast.side, bf16[400,2048]{1,0:T(8,128)(2,1)S(1)} %get-tuple-element.32.rows, bf16[16,464,512]{2,1,0:T(8,128)(2,1)} %bitcast.18, f32[4,1024]{1,0:T(4,128)S(1)} %copy-done.5, ...), custom_call_target="tpu_custom_call" | custom-call | flops 805306368 | bytes 4194304 | tf_op jit(solution)/shard_map/source/pallas_call | solution.py:323
  107.5 2.9 %collective-permute-start.3 = (bf16[128,512]{1,0:T(8,128)(2,1)S(1)}, bf16[128,512]{1,0:T(8,128)(2,1)S(1)}, u32[]{:S(2)}, u32[]{:S(2)}) collective-permute-start(bf16[128,512]{1,0:T(8,128)(2,1)S(1)} %get-tuple-element.38), channel_id=1, source_target_pairs={{0,32},{16,48},{1,33},{17,49},{2,34},{18,50},{3,35},{19,51},{4,36}... | collective-permute-start | bytes 393224 | tf_op jit(solution)/shard_map/ppermute | solution.py:495
  110.4 2.4 %gate.1 = f32[384,512]{1,0:T(8,128)S(1)} custom-call(bf16[400,2048]{1,0:T(8,128)(2,1)S(1)} %get-tuple-element.32.rows, bf16[16,464,512]{2,1,0:T(8,128)(2,1)} %bitcast.19), custom_call_target="tpu_custom_call" | custom-call | flops 805306368 | bytes 4194304 | tf_op jit(solution)/shard_map/gate/pallas_call | solution.py:323
  112.8 0.6 inner.1.base
  113.5 0.7 collective-permute-start.4
  114.1 0.0 collective-permute-done.4.arrived
  114.2 0.7 collective-permute-start.5
  114.9 0.7 collective-permute-start.6
  115.6 0.0 copy-start.8
  115.7 0.7 collective-permute-start.7
  116.4 0.7 collective-permute-start.8
  117.2 0.7 collective-permute-start.9
  117.9 0.5 blend.1
  118.4 6.2 %collective-permute-start.10 = (bf16[192,512]{1,0:T(8,128)(2,1)S(1)}, bf16[192,512]{1,0:T(8,128)(2,1)S(1)}, u32[]{:S(2)}, u32[]{:S(2)}) collective-permute-start(bf16[192,512]{1,0:T(8,128)(2,1)S(1)} %get-tuple-element.52), channel_id=1, source_target_pairs={{0,16},{16,0},{32,48},{48,32},{64,80},{80,64},{96,112},{112,96},{1... | collective-permute-start | bytes 589832 | tf_op jit(solution)/shard_map/ppermute | solution.py:543
  124.5 2.7 %own_half.1 = (f32[192,2048]{1,0:T(8,128)S(1)}, bf16[16,208,256]{2,1,0:T(8,128)(2,1)S(1)}, bf16[16,96,128]{2,1,0:T(8,128)(2,1)S(1)}) custom-call(s32[1]{0:T(128)} %bitcast.side, bf16[192,512]{1,0:T(8,128)(2,1)S(1)} %get-tuple-element.53.kept, bf16[16,464,512]{2,1,0:T(8,128)(2,1)} %bitcast.20, bf16[16,192,128]{2,1,0:T(8,128)(2,1)} %bitcast.22), custom_call_target="tpu_custom_call" | custom-call | flops 402653184 | bytes 4194304 | tf_op jit(solution)/shard_map/own_half/pallas_call | solution.py:323
  127.2 2.1 %collective-permute-done.10.arrived = bf16[192,512]{1,0:T(8,128)(2,1)S(1)} collective-permute-done((bf16[192,512]{1,0:T(8,128)(2,1)S(1)}, bf16[192,512]{1,0:T(8,128)(2,1)S(1)}, u32[]{:S(2)}, u32[]{:S(2)}) %collective-permute-start.10) | collective-permute-done | bytes 196640 | tf_op jit(solution)/shard_map/ppermute | solution.py:543
  129.3 1.3 output.1
  (43 shorter events, 0.4 us)
Async XLA Ops:
  6.5 25.2 %copy-start = (f32[1,3072,16]{1,2,0:T(8,128)S(1)}, f32[1,3072,16]{1,2,0:T(8,128)}, u32[]{:S(2)}) copy-start(f32[1,3072,16]{1,2,0:T(8,128)} %param.29) | copy-start | bytes 589828
  6.6 2.0 %copy-start.6 = (bf16[1,192,2048]{2,1,0:T(8,128)(2,1)S(1)}, bf16[1,192,2048]{2,1,0:T(8,128)(2,1)}, u32[]{:S(2)}) copy-start(bf16[1,192,2048]{2,1,0:T(8,128)(2,1)} %param.16) | copy-start | bytes 2359300
  6.6 24.9 %copy-start.13 = (bf16[2048,16]{0,1:T(8,128)(2,1)S(1)}, bf16[2048,16]{0,1:T(8,128)(2,1)}, u32[]{:S(2)}) copy-start(bf16[2048,16]{0,1:T(8,128)(2,1)} %param.21) | copy-start | bytes 196612
  6.6 26.2 %copy-start.14 = (f32[16]{0:T(128)S(1)}, f32[16]{0:T(128)}, u32[]{:S(2)}) copy-start(f32[16]{0:T(128)} %param.25) | copy-start | bytes 196
  6.6 26.3 %copy-start.15 = (f32[16]{0:T(128)S(1)}, f32[16]{0:T(128)}, u32[]{:S(2)}) copy-start(f32[16]{0:T(128)} %param.26) | copy-start | bytes 196
  6.6 26.4 %copy-start.16 = (f32[16]{0:T(128)S(1)}, f32[16]{0:T(128)}, u32[]{:S(2)}) copy-start(f32[16]{0:T(128)} %param.27) | copy-start | bytes 196
  6.6 97.8 %all-gather.4.cloned.1.call-start = ((), (), s32[]{:S(2)}) async-start(), calls=%async_computation | async-start | bytes 8077312 | tf_op jit(solution)/shard_map/all_gather | solution.py:387
  8.6 67.2 %collective-permute-start = (bf16[16,2048]{1,0:T(8,128)(2,1)S(1)}, bf16[16,2048]{1,0:T(8,128)(2,1)S(1)}, u32[]{:S(2)}, u32[]{:S(2)}) collective-permute-start(bf16[16,2048]{1,0:T(8,128)(2,1)S(1)} %slice_bitcast_fusion), channel_id=1, source_target_pairs={{16,32},{48,64},{80,96},{112,128},{144,160},{176,192},{208,224},{1... | collective-permute-start | bytes 196616 | tf_op jit(solution)/shard_map/ppermute | solution.py:394
  9.3 66.6 %collective-permute-start.1 = (bf16[16,2048]{1,0:T(8,128)(2,1)S(1)}, bf16[16,2048]{1,0:T(8,128)(2,1)S(1)}, u32[]{:S(2)}, u32[]{:S(2)}) collective-permute-start(bf16[16,2048]{1,0:T(8,128)(2,1)S(1)} %slice_bitcast_fusion), channel_id=1, source_target_pairs={{16,48},{48,80},{80,112},{112,144},{144,176},{176,208},{208,240},{... | collective-permute-start | bytes 196616 | tf_op jit(solution)/shard_map/ppermute | solution.py:395
  10.0 65.9 %collective-permute-start.2 = (bf16[192,2048]{1,0:T(8,128)(2,1)S(1)}, bf16[192,2048]{1,0:T(8,128)(2,1)S(1)}, u32[]{:S(2)}, u32[]{:S(2)}) collective-permute-start(bf16[192,2048]{1,0:T(8,128)(2,1)S(1)} %bitcast.15), channel_id=1, source_target_pairs={{0,16},{16,0},{32,48},{48,32},{64,80},{80,64},{96,112},{112,96},{1... | collective-permute-start | bytes 2359304 | tf_op jit(solution)/shard_map/ppermute | solution.py:392
  31.5 45.3 %copy-start.11 = (f32[4,256]{1,0:T(4,128)S(1)}, f32[4,256]{1,0:T(4,128)}, u32[]{:S(2)}) copy-start(f32[4,256]{1,0:T(4,128)} %taps_in.1) | copy-start | bytes 12292
  31.5 45.3 %copy-start.12 = (f32[4,256]{1,0:T(4,128)S(1)}, f32[4,256]{1,0:T(4,128)}, u32[]{:S(2)}) copy-start(f32[4,256]{1,0:T(4,128)} %taps_out.1) | copy-start | bytes 12292
  75.9 0.9 copy-start.9
  76.8 1.1 copy-start.7
  77.9 1.1 copy-start.10
  79.0 25.3 %copy-start.5 = (f32[4,1024]{1,0:T(4,128)S(1)}, f32[4,1024]{1,0:T(4,128)}, u32[]{:S(2)}) copy-start(f32[4,1024]{1,0:T(4,128)} %taps.1) | copy-start | bytes 49156
  83.8 1.5 %copy-start.1 = (bf16[8,384,384]{2,1,0:T(8,128)(2,1)}, bf16[8,384,384]{2,1,0:T(8,128)(2,1)S(1)}, u32[]{:S(2)}) copy-start(bf16[8,384,384]{2,1,0:T(8,128)(2,1)S(1)} %get-tuple-element.39.mixing) | copy-start | bytes 7077892
  85.3 0.9 copy-start.3
  86.1 0.9 copy-start.4
  107.5 5.3 %copy-start.2 = (bf16[8,384,384]{2,1,0:T(8,128)(2,1)S(1)}, bf16[8,384,384]{2,1,0:T(8,128)(2,1)}, u32[]{:S(2)}) copy-start(bf16[8,384,384]{2,1,0:T(8,128)(2,1)} %copy-done.1) | copy-start | bytes 7077892
  107.5 5.9 %collective-permute-start.3 = (bf16[128,512]{1,0:T(8,128)(2,1)S(1)}, bf16[128,512]{1,0:T(8,128)(2,1)S(1)}, u32[]{:S(2)}, u32[]{:S(2)}) collective-permute-start(bf16[128,512]{1,0:T(8,128)(2,1)S(1)} %get-tuple-element.38), channel_id=1, source_target_pairs={{0,32},{16,48},{1,33},{17,49},{2,34},{18,50},{3,35},{19,51},{4,36}... | collective-permute-start | bytes 393224 | tf_op jit(solution)/shard_map/ppermute | solution.py:495
  113.5 0.7 collective-permute-start.4
  114.2 0.7 collective-permute-start.5
  114.9 0.7 collective-permute-start.6
  115.6 2.2 %copy-start.8 = (f32[1024]{0:T(1024)S(1)}, f32[1024]{0:T(1024)}, u32[]{:S(2)}) copy-start(f32[1024]{0:T(1024)} %param.30) | copy-start | bytes 12292
  115.7 0.7 collective-permute-start.7
  116.4 0.7 collective-permute-start.8
  117.2 0.7 collective-permute-start.9
  118.4 11.0 %collective-permute-start.10 = (bf16[192,512]{1,0:T(8,128)(2,1)S(1)}, bf16[192,512]{1,0:T(8,128)(2,1)S(1)}, u32[]{:S(2)}, u32[]{:S(2)}) collective-permute-start(bf16[192,512]{1,0:T(8,128)(2,1)S(1)} %get-tuple-element.52), channel_id=1, source_target_pairs={{0,16},{16,0},{32,48},{48,32},{64,80},{80,64},{96,112},{112,96},{1... | collective-permute-start | bytes 589832 | tf_op jit(solution)/shard_map/ppermute | solution.py:543
Sparse Core Ops, SparseCore 0:
  9.5 94.7 all-gather.3
